TPU v7x, 32 devices: a whole 2x2x4 slice. The times are simulated.
32 devices in a mesh: grp: 2 (over y), sp: 4 (over z), fs: 2 (over x), tp: 2 (over core).
Axes of the slice: x: 2, y: 2, z: 4, core: 2. Of those that a mesh axis runs over, the one named last changes fastest.
Arguments:
- tokens: bfloat16 [4, 512, 2048], P(('grp', 'fs'), 'sp'), parts along dimension 0, may hold values from -6 to 6
- norm_gain: float32 [2048], replicated, may hold values from 0.1 to 1.9
- query_attend: bfloat16 [2048, 8, 128], P(None, ('fs', 'tp')), may hold values from -0.125 to 0.125
- key_attend: bfloat16 [2048, 8, 128], P(None, ('fs', 'tp')), may hold values from -0.125 to 0.125
- value_attend: bfloat16 [2048, 8, 128], P(None, ('fs', 'tp')), may hold values from -0.125 to 0.125
- query_linear: bfloat16 [2048, 8, 128], P(None, ('fs', 'tp')), may hold values from -0.125 to 0.125
- key_linear: bfloat16 [2048, 8, 128], P(None, ('fs', 'tp')), may hold values from -0.125 to 0.125
- value_linear: bfloat16 [2048, 8, 256], P(None, ('fs', 'tp')), may hold values from -0.125 to 0.125
- decay_down: bfloat16 [2048, 32], replicated, may hold values from -0.125 to 0.125
- decay_up: bfloat16 [32, 8, 128], replicated, may hold values from -2.109375 to 2.109375
- decay_bias: float32 [8, 128], replicated, may hold values from -1.5 to 7.5
- log_retain: float32 [4, 512, 8], P(('grp', 'fs'), 'sp'), parts along dimension 0, may hold values from -1.5 to 0
- query_gain: float32 [64], replicated, may hold values from 0.6 to 4
- key_gain: float32 [8, 2, 64], replicated, may hold values from 0.8 to 14
- diff_lambda: float32 [8], replicated, may hold values from 0.3 to 0.8
- mix_gain: float32 [128], replicated, may hold values from 0.1 to 1.9
- state_gain: float32 [256], replicated, may hold values from 0.1 to 1.9
- init_state: float32 [4, 8, 128, 256], P('grp', ('fs', 'tp')), parts along dimension 0, may hold values from -80 to 80
- output_attend: bfloat16 [1024, 2048], P(None, 'tp'), may hold values from -0.109375 to 0.109375
- output_linear: bfloat16 [2048, 2048], P(None, 'tp'), may hold values from -0.109375 to 0.109375
Outputs:
- mixed_out: bfloat16 [4, 512, 2048], P(('grp', 'fs'), 'sp', 'tp'), parts along dimension 0
There are 2 independent parts, one for each index of `grp`. A program takes and returns all parts, laid end to end along the dimension named above; an argument that names none is the same for every part. Nothing has to cross between parts.
All inputs are finite; a program needn't handle non-finite values.
Results may differ from a plain program's by a relative error of at most 0.018.
The roundings to bfloat16 on the way count: a program that leaves them out, or rounds other values in their place, can miss the bound.
Values may be sent and summed in bfloat16 or wider, within the bound.
No kernel may reach another device: no remote copies, remote signals or barrier semaphores. Data moves between devices by JAX's collectives and lax.ppermute only.
A program may use at most 128 MiB of HBM per device.

v0:
```python
import jax
import jax.numpy as jnp
from jax import lax
from jax.sharding import PartitionSpec as P

MIXER_HEADS = 8
HD_A = 64
DV_A = 128
HDK = 128
HDV = 256
BLK = 64


norm_eps = 1e-06
decay_tau = 16.0


def entering(part, axis, combine, identity):
    place = lax.axis_index(axis)
    gathered = jax.tree.map(lambda a: lax.all_gather(a, axis), part)
    state = jax.tree.map(lambda a, e: jnp.zeros_like(a) + jnp.asarray(e, a.dtype), part, identity)

    def one(hop, state):
        return combine(
            state, jax.tree.map(lambda a: lax.dynamic_index_in_dim(a, hop, 0, False), gathered)
        )

    return lax.fori_loop(0, place, one, state)


def rms_scale(values, gain):
    widened = values.astype(jnp.float32)
    return (
        widened * lax.rsqrt(jnp.mean(widened * widened, axis=-1, keepdims=True) + norm_eps) * gain
    )


def head_order(fs_size, tp_size, tp_rank):
    per_device = MIXER_HEADS // (fs_size * tp_size)
    owners = jnp.arange(fs_size, dtype=jnp.int32)[:, None] * tp_size + tp_rank
    return (owners * per_device + jnp.arange(per_device, dtype=jnp.int32)[None, :]).reshape(-1)


def linear_blocks(queries, keys_in, values_in, log_decay):
    tok_rows, head_count, key_dim = queries.shape
    value_dim = values_in.shape[-1]
    block_count = tok_rows // BLK
    highest_precision = lax.Precision.HIGHEST

    def split_blocks(source):
        return source.reshape(block_count, BLK, head_count, source.shape[-1])

    causal = (
        jnp.arange(BLK, dtype=jnp.int32)[:, None] >= jnp.arange(BLK, dtype=jnp.int32)[None, :]
    )[None]

    def advance(carry, inputs_now):
        recurrent_state, offset = carry
        question_patch_lines, block_k, value_tile_width, block_log = inputs_now
        running_state = jnp.cumsum(block_log, axis=0)
        pivot = running_state[BLK // 2]
        q_scaled = question_patch_lines * jnp.exp(running_state - pivot[None])
        k_scaled = block_k * jnp.exp(pivot[None] - running_state)
        scores = jnp.einsum("thk,shk->hts", q_scaled, k_scaled, precision=highest_precision)
        scores = jnp.where(causal, scores, 0.0)
        inside_block = jnp.einsum(
            "hts,shv->thv", scores, value_tile_width, precision=highest_precision
        )
        inside_block = inside_block + jnp.einsum(
            "jwo,wos->jws",
            question_patch_lines * jnp.exp(running_state),
            recurrent_state,
            precision=highest_precision,
        )
        final_state = running_state[-1]
        faded_memory_matrix = block_k * jnp.exp(final_state[None] - running_state)
        recurrent_state = recurrent_state * jnp.exp(final_state)[:, :, None] + jnp.einsum(
            "zcb,zcw->cbw", faded_memory_matrix, value_tile_width, precision=highest_precision
        )
        reaching_keys = question_patch_lines * jnp.exp(offset[None] + running_state)
        return ((recurrent_state, offset + final_state), (inside_block, reaching_keys))

    start_carry = (
        jnp.zeros((head_count, key_dim, value_dim), jnp.float32),
        jnp.zeros((head_count, key_dim), jnp.float32),
    )
    (recurrent_state, total_decay), (inside_block, reaching_keys) = lax.scan(
        advance,
        start_carry,
        (
            split_blocks(queries),
            split_blocks(keys_in),
            split_blocks(values_in),
            split_blocks(log_decay),
        ),
    )
    return (
        recurrent_state,
        total_decay,
        inside_block.reshape(tok_rows, head_count, value_dim),
        reaching_keys.reshape(tok_rows, head_count, key_dim),
    )


def body(
    tokens,
    norm_gain,
    query_attend,
    key_attend,
    value_attend,
    query_linear,
    key_linear,
    value_linear,
    decay_down,
    decay_up,
    decay_bias,
    log_retain,
    query_gain,
    key_gain,
    diff_lambda,
    mix_gain,
    state_gain,
    init_state,
    output_attend,
    output_linear,
):
    fs_size = lax.axis_size("fs")
    tp_size = lax.axis_size("tp")
    tp_rank = lax.axis_index("tp")
    tok_rows = tokens.shape[1]
    normed = rms_scale(tokens, norm_gain).astype(jnp.bfloat16)
    normed_rows = normed[0]
    local_weights = (query_attend, key_attend, value_attend, query_linear, key_linear, value_linear)
    widths = [weight.shape[1] * weight.shape[2] for weight in local_weights]
    packed = jnp.concatenate(
        [weight.reshape(weight.shape[0], -1) for weight in local_weights], axis=1
    )
    computed = jnp.einsum(
        "std,dp->stp",
        lax.all_gather(normed, "fs", axis=0, tiled=True),
        packed,
        preferred_element_type=jnp.float32,
    ).astype(jnp.bfloat16)
    arrived = lax.all_to_all(computed, "fs", split_axis=0, concat_axis=2, tiled=True).reshape(
        tok_rows, fs_size, -1
    )
    sections = []
    column_at = 0
    for weight, width_now in zip(local_weights, widths):
        section = arrived[:, :, column_at : column_at + width_now]
        sections.append(section.reshape(tok_rows, fs_size * weight.shape[1], weight.shape[2]))
        column_at = column_at + width_now
    projected = tuple(sections)
    q_pair, k_pair, v_attend, q_lin, k_lin, v_lin = projected
    head_ids = head_order(fs_size, tp_size, tp_rank)
    head_count = head_ids.shape[0]
    q_unit = rms_scale(q_pair.reshape(tok_rows, head_count, 2, HD_A), query_gain).astype(
        jnp.bfloat16
    )
    k_unit = rms_scale(
        k_pair.reshape(tok_rows, head_count, 2, HD_A), jnp.take(key_gain, head_ids, axis=0)
    ).astype(jnp.bfloat16)
    sp_start = lax.axis_index("sp") * tok_rows
    query_block = (sp_start + jnp.arange(tok_rows, dtype=jnp.int32)) // BLK
    score_scale = HD_A ** (-0.5)
    blank_attend = (
        jnp.full((head_count, 2, tok_rows), -jnp.inf, jnp.float32),
        jnp.zeros((head_count, 2, tok_rows), jnp.float32),
        jnp.zeros((head_count, 2, tok_rows, DV_A), jnp.float32),
    )
    carry = blank_attend
    seg_keys = lax.all_gather(k_unit, "sp", axis=0, tiled=True)
    seg_values = lax.all_gather(v_attend, "sp", axis=0, tiled=True)
    span = seg_keys.shape[0]
    stride_token_lines = 2 * tok_rows
    step_count = span // stride_token_lines
    key_steps = seg_keys.reshape(step_count, stride_token_lines, head_count, 2, HD_A)
    value_steps = seg_values.reshape(step_count, stride_token_lines, head_count, DV_A)

    def one_step(running_state, inputs_now):
        step_index, key_step, value_step = inputs_now
        key_start = step_index * stride_token_lines

        def compute(current):
            run_max, run_total, run_acc = current
            scores = (
                jnp.einsum("qhmd,khmd->hmqk", q_unit, key_step, preferred_element_type=jnp.float32)
                * score_scale
            )
            key_block = (key_start + jnp.arange(stride_token_lines, dtype=jnp.int32)) // BLK
            allowed = query_block[:, None] >= key_block[None, :]
            scores = jnp.where(allowed, scores, -jnp.inf)
            new_max = jnp.maximum(run_max, jnp.max(scores, axis=-1))
            factor = jnp.exp(run_max - new_max)
            raised = jnp.exp(scores - new_max[..., None])
            run_total = run_total * factor + jnp.sum(raised, axis=-1)
            run_acc = run_acc * factor[..., None] + jnp.einsum(
                "hmqk,khv->hmqv",
                raised.astype(jnp.bfloat16),
                value_step,
                preferred_element_type=jnp.float32,
            )
            return (new_max, run_total, run_acc)

        def unchanged(current):
            return current

        return (lax.cond(key_start <= sp_start, compute, unchanged, running_state), None)

    carry, _ = lax.scan(
        one_step, carry, (jnp.arange(step_count, dtype=jnp.int32), key_steps, value_steps)
    )
    run_max, run_total, run_acc = carry
    lambda_heads = jnp.take(diff_lambda, head_ids, axis=0)
    diff_raw = (
        run_acc[:, 0] / run_total[:, 0, :, None]
        - lambda_heads[:, None, None] * run_acc[:, 1] / run_total[:, 1, :, None]
    )
    attend_out = rms_scale(jnp.transpose(diff_raw, (1, 0, 2)), mix_gain).astype(jnp.bfloat16)
    low_rank = jnp.dot(normed_rows, decay_down, preferred_element_type=jnp.float32).astype(
        jnp.bfloat16
    )
    up_columns = jnp.take(decay_up, head_ids, axis=1)
    pre_act = jnp.einsum(
        "tr,rhk->thk", low_rank, up_columns, preferred_element_type=jnp.float32
    ) + jnp.take(decay_bias, head_ids, axis=0)
    retain_heads = jnp.take(log_retain[0], head_ids, axis=1)
    log_decay = jax.nn.log_sigmoid(pre_act) / decay_tau + retain_heads[:, :, None]
    local_state, local_decay, inside_block, reaching_keys = linear_blocks(
        q_lin.astype(jnp.float32) * HDK ** (-0.5),
        k_lin.astype(jnp.float32),
        v_lin.astype(jnp.float32),
        log_decay,
    )

    def chain(earlier, later):
        return (earlier[0] + later[0], earlier[1] * jnp.exp(later[0])[:, :, None] + later[1])

    zero_chain = (jnp.zeros_like(local_decay), jnp.zeros_like(local_state))
    prior_decay, prior_state = entering((local_decay, local_state), "sp", chain, zero_chain)
    start_state = lax.all_to_all(init_state, "fs", split_axis=0, concat_axis=1, tiled=True)[0]
    incoming_state = start_state * jnp.exp(prior_decay)[:, :, None] + prior_state
    linear_raw = inside_block + jnp.einsum(
        "jwo,wos->jws", reaching_keys, incoming_state, precision=lax.Precision.HIGHEST
    )
    linear_out = rms_scale(linear_raw, state_gain).astype(jnp.bfloat16)
    out_cols = output_attend.shape[1]
    per_device = MIXER_HEADS // (fs_size * tp_size)
    attend_view = output_attend.reshape(fs_size, tp_size, per_device * DV_A, out_cols)
    linear_view = output_linear.reshape(fs_size, tp_size, per_device * HDV, out_cols)
    blank_out = jnp.zeros((tok_rows, out_cols), jnp.float32)
    running_out = blank_out
    seg_attend = lax.all_gather(attend_out, "tp", axis=1, tiled=True)
    seg_linear = lax.all_gather(linear_out, "tp", axis=1, tiled=True)
    shard_count = seg_attend.shape[1] // head_count
    first_rank = jnp.int32(0) // head_count
    for shard_step in range(shard_count):
        owner_rank = first_rank + shard_step
        rows_attend = lax.dynamic_index_in_dim(attend_view, owner_rank, 1, keepdims=False).reshape(
            -1, out_cols
        )
        rows_linear = lax.dynamic_index_in_dim(linear_view, owner_rank, 1, keepdims=False).reshape(
            -1, out_cols
        )
        part_attend = seg_attend[
            :, shard_step * head_count : (shard_step + 1) * head_count
        ].reshape(tok_rows, -1)
        part_linear = seg_linear[
            :, shard_step * head_count : (shard_step + 1) * head_count
        ].reshape(tok_rows, -1)
        running_out = running_out + jnp.dot(
            part_attend, rows_attend, preferred_element_type=jnp.float32
        )
        running_out = running_out + jnp.dot(
            part_linear, rows_linear, preferred_element_type=jnp.float32
        )
    return running_out.astype(jnp.bfloat16).reshape(1, tok_rows, out_cols)


def solution(mesh):
    in_specs = (
        P(("grp", "fs"), "sp", None),
        P(),
        P(None, ("fs", "tp"), None),
        P(None, ("fs", "tp"), None),
        P(None, ("fs", "tp"), None),
        P(None, ("fs", "tp"), None),
        P(None, ("fs", "tp"), None),
        P(None, ("fs", "tp"), None),
        P(),
        P(),
        P(),
        P(("grp", "fs"), "sp", None),
        P(),
        P(),
        P(),
        P(),
        P(),
        P("grp", ("fs", "tp"), None, None),
        P(None, "tp"),
        P(None, "tp"),
    )
    out_specs = P(("grp", "fs"), "sp", "tp")
    return jax.shard_map(body, mesh=mesh, in_specs=in_specs, out_specs=out_specs, check_vma=False)
```

profile of v0, /device:TPU:31, one launch (start us, length us, event | category | flops | bytes accessed | tf_op | source)
XLA Modules:
  0.0 174.8 jit_solution(11387450350925184077)
XLA Ops:
  7.9 2.0 %fusion.48 = bf16[1,128,2048]{2,1,0:T(8,128)(2,1)} fusion(bf16[1,128,2048]{2,1,0:T(8,128)(2,1)} %param.28, f32[2048]{0:T(1024)} %param.29, f32[128]{0:T(128)S(1)} %add_rsqrt_fusion.4), kind=kLoop, calls=%fused_computation.92 | loop fusion | flops 1048576 | bytes 1057280 | tf_op jit(solution)/shard_map/convert_element_type | solution.py:131
  12.8 2.4 %bitcast_dynamic-update-slice_fusion.4 = bf16[2048,1792]{1,0:T(8,128)(2,1)} fusion(bf16[256,8,2,128]{3,2,1,0:T(2,128)(2,1)} %bitcast.243), kind=kLoop, calls=%fused_computation.97 | loop fusion | bytes 2097152
  15.2 2.0 %copy.128 = bf16[256,8,2,256]{3,1,2,0:T(8,128)(2,1)S(1)} copy(bf16[256,8,2,256]{3,2,1,0:T(2,128)(2,1)} %bitcast.240) | data formatting | bytes 4194304
  19.1 2.5 %bitcast_dynamic-update-slice_fusion.3 = bf16[2048,1792]{1,0:T(8,128)(2,1)} fusion(bf16[2048,1792]{1,0:T(8,128)(2,1)} %bitcast_dynamic-update-slice_fusion.4, bf16[256,8,2,128]{3,2,1,0:T(2,128)(2,1)} %bitcast.244), kind=kLoop, calls=%fused_computation.96 | loop fusion | bytes 2097152
  21.6 2.4 %bitcast_dynamic-update-slice_fusion.2 = bf16[2048,1792]{1,0:T(8,128)(2,1)} fusion(bf16[2048,1792]{1,0:T(8,128)(2,1)} %bitcast_dynamic-update-slice_fusion.3, bf16[256,8,2,128]{3,2,1,0:T(2,128)(2,1)} %bitcast.245), kind=kLoop, calls=%fused_computation.95 | loop fusion | bytes 2097152
  24.0 2.5 %bitcast_dynamic-update-slice_fusion.1 = bf16[2048,1792]{1,0:T(8,128)(2,1)} fusion(bf16[2048,1792]{1,0:T(8,128)(2,1)} %bitcast_dynamic-update-slice_fusion.2, bf16[256,8,2,128]{3,2,1,0:T(2,128)(2,1)} %bitcast.246), kind=kLoop, calls=%fused_computation.94 | loop fusion | bytes 2097152
  28.0 2.6 %bitcast_dynamic-update-slice_fusion = bf16[2048,1792]{1,0:T(8,128)(2,1)} fusion(bf16[2048,1792]{1,0:T(8,128)(2,1)} %bitcast_dynamic-update-slice_fusion.1, bf16[256,8,2,128]{3,2,1,0:T(2,128)(2,1)} %bitcast.247), kind=kLoop, calls=%fused_computation.93 | loop fusion | bytes 2097152
  33.7 6.4 %fusion.37 = bf16[2,128,1792]{2,1,0:T(8,128)(2,1)} fusion(bf16[2,128,2048]{2,1,0:T(8,128)(2,1)} %all-gather.6.cloned.1.call-done, bf16[2048,1792]{1,0:T(8,128)(2,1)} %constant_dynamic-update-slice_fusion), kind=kOutput, calls=%fused_computation.76 | convolution fusion | flops 1879506944 | bytes 9306112 | tf_op jit(solution)/shard_map/std,dp->stp/dot_general | solution.py:138
  40.1 3.8 %all-to-all-start = ((bf16[2,128,1792]{2,1,0:T(8,128)(2,1)}), bf16[2,128,1792]{2,1,0:T(8,128)(2,1)S(1)}, u32[]{:S(2)}, u32[]{:S(2)}) async-start(bf16[2,128,1792]{2,1,0:T(8,128)(2,1)} %fusion.37), calls=%async_computation | async-start | bytes 1835008 | tf_op jit(solution)/shard_map/all_to_all | solution.py:144
  44.0 4.6 %fusion.67 = (bf16[2,1,512,1024]{3,2,1,0:T(8,128)(2,1)}, bf16[2,1,512,1024]{3,2,1,0:T(8,128)(2,1)}) fusion(bf16[2,2,512,1024]{3,2,1,0:T(8,128)(2,1)} %bitcast.227), kind=kLoop, calls=%fused_computation.147 | loop fusion | bytes 8388608 | tf_op jit(solution)/shard_map/jit(dynamic_index_in_dim)/dynamic_slice | solution.py:262
  48.6 5.8 %all-to-all-done = bf16[2,128,1792]{2,1,0:T(8,128)(2,1)S(1)} async-done(((bf16[2,128,1792]{2,1,0:T(8,128)(2,1)}), bf16[2,128,1792]{2,1,0:T(8,128)(2,1)S(1)}, u32[]{:S(2)}, u32[]{:S(2)}) %all-to-all-start) | async-done | bytes 917536 | tf_op jit(solution)/shard_map/all_to_all | solution.py:144
  54.4 4.7 %all-to-all-start.1 = ((f32[2,2,128,256]{3,2,1,0:T(8,128)}), f32[2,2,128,256]{3,2,1,0:T(8,128)S(1)}, u32[]{:S(2)}, u32[]{:S(2)}) async-start(f32[2,2,128,256]{3,2,1,0:T(8,128)} %param.45), calls=%async_computation.1 | async-start | bytes 1048576 | tf_op jit(solution)/shard_map/all_to_all | solution.py:241
  64.8 9.1 %while.46 = (s32[]{:T(128)}, f32[4,128,256]{2,1,0:T(8,128)S(1)}, f32[4,128]{1,0:T(4,128)S(1)}, f32[2,64,4,256]{3,1,0,2:T(8,128)}, f32[2,64,4,128]{3,2,1,0:T(4,12...) while((s32[]{:T(128)}, f32[4,128,256]{2,1,0:T(8,128)S(1)}, ...), condition=%wide.region_12.13_spmd.clone, body=%wide.region_10.12_spmd.clone.sunk | while | flops 279794688 | bytes 5934213 | solution.py:87
  75.0 13.2 %all_gather.28 = bf16[512,4,2,64]{0,3,2,1:T(8,128)(2,1)S(1)} all-gather(bf16[128,4,2,64]{0,3,2,1:T(8,128)(2,1)S(1)} %multiply_convert_fusion.3), channel_id=1, replica_groups=mesh['grp'=2,'sp'=4,'fs'=2,'tp'=2] {'sp'}, dimensions={0}, use_global_device_ids=true | all-gather | bytes 655360 | tf_op jit(solution)/shard_map/all_gather | solution.py:172
  89.4 28.4 %all_gather.29 = bf16[512,4,128]{0,2,1:T(8,128)(2,1)S(1)} all-gather(bf16[128,4,128]{0,2,1:T(8,128)(2,1)S(1)} %bitcast.252), channel_id=1, replica_groups=mesh['grp'=2,'sp'=4,'fs'=2,'tp'=2] {'sp'}, dimensions={0}, use_global_device_ids=true | all-gather | bytes 655360 | tf_op jit(solution)/shard_map/all_gather | solution.py:173
  119.0 4.9 %while.47 = (s32[]{:T(128)}, f32[4,2,128]{2,1,0:T(2,128)S(1)}, f32[4,2,128]{2,1,0:T(2,128)S(1)}, f32[4,2,128,128]{3,2,1,0:T(8,128)S(1)}, s32[2]{0:T(128)S(1)}, /...) while((s32[]{:T(128)}, f32[4,2,128]{2,1,0:T(2,128)S(1)}, ...), condition=%wide.region_8.9_spmd.clone.clone, body=%wide.region_3.8_spmd.clone.clone.sunk | while | flops 102802176 | bytes 4989555 | solution.py:210
  124.5 10.0 %all_gather.30 = bf16[128,8,128]{2,0,1:T(8,128)(2,1)S(1)} all-gather(bf16[128,4,128]{2,0,1:T(8,128)(2,1)S(1)} %multiply_convert_fusion.1), channel_id=1, replica_groups=mesh['grp'=2,'sp'=4,'fs'=2,'tp'=2] {'tp'}, dimensions={1}, use_global_device_ids=true | all-gather | bytes 393216 | tf_op jit(solution)/shard_map/all_gather | solution.py:253
  137.1 8.3 %all-gather.2 = f32[4,4,128]{2,1,0:T(4,128)S(1)} all-gather(f32[1,4,128]{2,1,0:T(4,128)S(1)} %bitcast.260), channel_id=2, replica_groups=mesh['grp'=2,'sp'=4,'fs'=2,'tp'=2] {'sp'}, dimensions={0}, use_global_device_ids=true | all-gather | bytes 10240 | tf_op jit(solution)/shard_map/all_gather | solution.py:20
  145.5 3.9 %while.45 = (s32[]{:T(128)}, f32[4,128]{1,0:T(4,128)S(1)}, f32[4,128,256]{2,1,0:T(8,128)S(1)}, s32[]{:T(128)}, f32[4,4,128]{2,1,0:T(4,128)S(1)}, /*index=5*/f32[...) while((s32[]{:T(128)}, f32[4,128]{1,0:T(4,128)S(1)}, f32[4,128,256]{2,1,0:T(8,128)S(1)}, s32[]{:T(128)}, ...), condition=%wide.region_14.15_spmd, body=%wide.region_13.14_spmd.sunk | while | flops 262661 | bytes 1583239 | solution.py:28
  149.6 2.3 %multiply_reduce_fusion = (f32[128,4]{0,1:T(4,128)S(1)}, f32[128,4,256]{0,2,1:T(8,128)S(1)}) fusion(f32[128,4,256]{0,2,1:T(8,128)} %copy.101, f32[4,128,256]{2,1,0:T(8,128)S(1)} %fusion.49, f32[128,4,128]{2,1,0:T(4,128)} %bitcast.257), kind=kOutput, calls=%fused_computation.104 | convolution fusion | flops 201719296 | bytes 1837056 | tf_op jit(solution)/shard_map/jwo,wos->jws/dot_general | solution.py:243
  153.8 4.5 %all_gather.35 = bf16[128,8,256]{2,0,1:T(8,128)(2,1)S(1)} all-gather(bf16[128,4,256]{2,0,1:T(8,128)(2,1)S(1)} %copy.102), channel_id=1, replica_groups=mesh['grp'=2,'sp'=4,'fs'=2,'tp'=2] {'tp'}, dimensions={1}, use_global_device_ids=true | all-gather | bytes 786432 | tf_op jit(solution)/shard_map/all_gather | solution.py:254
  159.0 1.8 %copy.114 = bf16[128,4,256]{0,2,1:T(8,128)(2,1)} copy(bf16[128,4,256]{2,0,1:T(8,128)(2,1)} %get-tuple-element.513) | data formatting | bytes 524288
  161.6 2.2 %fusion.73 = f32[128,1024]{1,0:T(8,128)S(1)} fusion(bf16[128,1024]{0,1:T(8,128)(2,1)} %bitcast.249, bf16[1024,1024]{1,0:T(8,128)(2,1)} %bitcast.225), kind=kOutput, calls=%fused_computation.153 | convolution fusion | flops 268435456 | bytes 2883584 | tf_op jit(solution)/shard_map/dot_general | solution.py:274
  165.3 1.6 convolution_add_fusion.3
  (161 shorter events, 47.7 us)
Async XLA Ops:
  6.5 20.1 %copy-start = (bf16[2048,32]{0,1:T(8,128)(2,1)S(1)}, bf16[2048,32]{0,1:T(8,128)(2,1)}, u32[]{:S(2)}) copy-start(bf16[2048,32]{0,1:T(8,128)(2,1)} %param.36) | copy-start | bytes 393220
  6.5 10.7 %copy-start.10 = (f32[8,128]{1,0:T(8,128)S(1)}, f32[8,128]{1,0:T(8,128)}, u32[]{:S(2)}) copy-start(f32[8,128]{1,0:T(8,128)} %param.38) | copy-start | bytes 12292
  6.5 11.2 %copy-start.1 = (f32[1,128,8]{1,2,0:T(8,128)S(1)}, f32[1,128,8]{1,2,0:T(8,128)}, u32[]{:S(2)}) copy-start(f32[1,128,8]{1,2,0:T(8,128)} %param.39) | copy-start | bytes 12292
  6.5 11.8 %copy-start.7 = (bf16[32,8,128]{2,1,0:T(8,128)(2,1)S(1)}, bf16[32,8,128]{2,1,0:T(8,128)(2,1)}, u32[]{:S(2)}) copy-start(bf16[32,8,128]{2,1,0:T(8,128)(2,1)} %param.37) | copy-start | bytes 196612
  6.5 27.1 %all-gather.6.cloned.1.call-start = ((), (), s32[]{:S(2)}) async-start(), calls=%async_computation.2 | async-start | bytes 1572864 | tf_op jit(solution)/shard_map/all_gather | solution.py:140
  9.9 16.7 %copy-start.6 = (bf16[1,128,2048]{2,1,0:T(8,128)(2,1)S(1)}, bf16[1,128,2048]{2,1,0:T(8,128)(2,1)}, u32[]{:S(2)}) copy-start(bf16[1,128,2048]{2,1,0:T(8,128)(2,1)} %fusion.48) | copy-start | bytes 1572868
  28.0 4.1 %copy-start.5 = (bf16[1024,1024]{1,0:T(8,128)(2,1)S(1)}, bf16[1024,1024]{1,0:T(8,128)(2,1)}, u32[]{:S(2)}) copy-start(bf16[1024,1024]{1,0:T(8,128)(2,1)} %param.46) | copy-start | bytes 6291460
  40.1 14.3 %all-to-all-start = ((bf16[2,128,1792]{2,1,0:T(8,128)(2,1)}), bf16[2,128,1792]{2,1,0:T(8,128)(2,1)S(1)}, u32[]{:S(2)}, u32[]{:S(2)}) async-start(bf16[2,128,1792]{2,1,0:T(8,128)(2,1)} %fusion.37), calls=%async_computation | async-start | bytes 1835008 | tf_op jit(solution)/shard_map/all_to_all | solution.py:144
  54.4 95.0 %all-to-all-start.1 = ((f32[2,2,128,256]{3,2,1,0:T(8,128)}), f32[2,2,128,256]{3,2,1,0:T(8,128)S(1)}, u32[]{:S(2)}, u32[]{:S(2)}) async-start(f32[2,2,128,256]{3,2,1,0:T(8,128)} %param.45), calls=%async_computation.1 | async-start | bytes 1048576 | tf_op jit(solution)/shard_map/all_to_all | solution.py:241
  59.0 86.4 %all-gather.8.cloned.1.call-start = ((), (), s32[]{:S(2)}) async-start(), calls=%async_computation.3 | async-start | bytes 2621440 | tf_op jit(solution)/shard_map/all_gather | solution.py:20
  74.0 0.8 copy-start.2
  119.0 5.3 %copy-start.12 = (f32[128]{0:T(128)S(1)}, f32[128]{0:T(128)}, u32[]{:S(2)}) copy-start(f32[128]{0:T(128)} %param.43) | copy-start | bytes 1540
  119.0 16.3 %copy-start.9 = (f32[2,64,4,256]{3,1,0,2:T(8,128)S(1)}, f32[2,64,4,256]{3,1,0,2:T(8,128)}, u32[]{:S(2)}) copy-start(f32[2,64,4,256]{3,1,0,2:T(8,128)} %get-tuple-element.232) | copy-start | bytes 1572868
  124.5 27.4 %copy-start.11 = (f32[256]{0:T(256)S(1)}, f32[256]{0:T(256)}, u32[]{:S(2)}) copy-start(f32[256]{0:T(256)} %param.44) | copy-start | bytes 3076
  145.5 18.4 %copy-start.3 = (bf16[2,1,512,1024]{3,2,1,0:T(8,128)(2,1)S(1)}, bf16[2,1,512,1024]{3,2,1,0:T(8,128)(2,1)}, u32[]{:S(2)}) copy-start(bf16[2,1,512,1024]{3,2,1,0:T(8,128)(2,1)} %get-tuple-element.506) | copy-start | bytes 6291460
  149.6 17.4 %copy-start.4 = (bf16[2,1,256,1024]{3,2,1,0:T(8,128)(2,1)S(1)}, bf16[2,1,256,1024]{3,2,1,0:T(8,128)(2,1)}, u32[]{:S(2)}) copy-start(bf16[2,1,256,1024]{3,2,1,0:T(8,128)(2,1)} %get-tuple-element.507) | copy-start | bytes 3145732
  161.6 5.3 %copy-start.8 = (bf16[128,4,128]{0,2,1:T(8,128)(2,1)S(1)}, bf16[128,4,128]{0,2,1:T(8,128)(2,1)}, u32[]{:S(2)}) copy-start(bf16[128,4,128]{0,2,1:T(8,128)(2,1)} %copy.115) | copy-start | bytes 393220
Sparse Core Ops, SparseCore 0:
  10.1 21.0 all-gather.5
  74.9 55.7 all-gather.7
where the time goes:
time: 176 us; the launch traced here: 175 us
  blocking collectives  64.4 us (37%)
  local copies, waits for them, and re-layouts  44 us (25%)
  matrix products  23.2 us (13%)
  between operations  13.8 us (8%)
  other arithmetic  13.4 us (8%)
  starting transfers between devices  8.49 us (5%)
  waiting for transfers between devices  5.8 us (3%)
    all_gather x1, blocking collectives, body(): seg_values = lax.all_gather(v_attend, 'sp', axis=0, tiled=True)  28.4 us
    unnamed x37, local copies, waits for them, and re-layouts  19.5 us
    all_gather x1, blocking collectives, body(): seg_keys = lax.all_gather(k_unit, 'sp', axis=0, tiled=True)  13.2 us
    all_gather x1, blocking collectives, body(): seg_attend = lax.all_gather(attend_out, 'tp', axis=1, tiled=True)  10 us
    all_gather x1, blocking collectives, entering(): gathered = jax.tree.map(lambda a: lax.all_gather(a, axis), part)  8.34 us
    dot_general x1, matrix products, body(): jnp.einsum('std,dp->stp', lax.all_gather(normed, 'fs', axis=0, tiled=True...  6.43 us
    all_to_all x1, waiting for transfers between devices, body(): lax.all_to_all(computed, 'fs', split_axis=0, concat_axis=2, tiled=True)  5.76 us
    all_to_all x1, starting transfers between devices, body(): lax.all_to_all(init_state, 'fs', split_axis=0, concat_axis=1, tiled=True)[0]  4.65 us
  transfers between devices with their start and end apart: 4, of which 1 were waited for; matrix products, arithmetic and copies ran while one was open for 32% of the time, Pallas kernels for 0%

commit v1 on v0

v1 whole, which is shorter than its diff:
```python
import functools

import jax
import jax.numpy as jnp
from jax import lax
from jax.experimental import pallas as pl
from jax.experimental.pallas import tpu as pltpu
from jax.sharding import PartitionSpec as P

EPS = 1e-06
TAU = 16.0
BLK = 64
F32 = jnp.float32
BF16 = jnp.bfloat16
HIGH = lax.Precision.HIGHEST


def dot(a, b, dims=((1,), (0,)), precision=None):
    return lax.dot_general(a, b, (dims, ((), ())), precision=precision, preferred_element_type=F32)


def rms(x, gain):
    return x * lax.rsqrt(jnp.mean(x * x, axis=-1, keepdims=True) + EPS) * gain


def rms_halves(x, gain):
    rows, width = x.shape
    half = width // 2
    first = lax.broadcasted_iota(jnp.int32, x.shape, 1) < half
    sq = x * x
    low = jnp.sum(jnp.where(first, sq, 0.0), axis=-1, keepdims=True) / half
    high = jnp.sum(jnp.where(first, 0.0, sq), axis=-1, keepdims=True) / half
    return x * jnp.where(first, lax.rsqrt(low + EPS), lax.rsqrt(high + EPS)) * gain


def whole(shape, memory_space=pltpu.VMEM):
    return pl.BlockSpec(shape, lambda *_: (0,) * len(shape), memory_space=memory_space)


SMEM = pl.BlockSpec(memory_space=pltpu.SMEM)


def unpack_weight(w_ref, wide_ref, heads, parts, out_ref, column):
    rows = w_ref.shape[0] // (heads * parts)
    if heads * parts == 1:
        out_ref[:, column : column + 128] = w_ref[...]
        return
    wide_ref[: w_ref.shape[0], :] = w_ref[...].astype(F32)
    for head in range(heads):
        for part in range(parts):
            piece = wide_ref[pl.ds(part * heads + head, rows, stride=heads * parts), :]
            at = column + (head * parts + part) * 128
            out_ref[:, at : at + 128] = piece.astype(BF16)


class Dims:
    def __init__(self, tokens, query_attend, value_attend, key_linear, value_linear, decay_up):
        self.rows = tokens.shape[1]
        self.model = tokens.shape[2]
        self.heads = query_attend.shape[1]
        self.ca = query_attend.shape[2]
        self.va = value_attend.shape[2]
        self.ck = key_linear.shape[2]
        self.cv = value_linear.shape[2]
        self.all_heads = decay_up.shape[1]
        self.rank = decay_up.shape[0]
        self.kv = self.heads * (self.ca + self.va)
        self.rest = self.heads * (self.ca + 2 * self.ck + self.cv)
        self.steps = 4
        self.chunk = self.model // self.steps


def norm_into(parts, start_of, gain, normed_ref):
    for index, part in enumerate(parts):
        values = rms(part[...].astype(F32), gain[...]).astype(BF16)
        normed_ref[pl.ds(start_of(index), part.shape[0]), :] = values


def write_kv(acc, key_gain, meta, dims, out):
    for h in range(dims.heads):
        k = acc[:, h * dims.ca : (h + 1) * dims.ca].astype(BF16).astype(F32)
        row = 2 * (meta[1] + h)
        gain = jnp.concatenate([key_gain[pl.ds(row, 1), :], key_gain[pl.ds(row + 1, 1), :]], axis=1)
        out[:, h * dims.ca : (h + 1) * dims.ca] = rms_halves(k, gain).astype(BF16)
    at = dims.heads * dims.ca
    out[:, at:] = acc[:, at:].astype(BF16)


def kv_first(dims, tokens, gain, wk, wv, key_gain, meta):
    hd = dims.heads

    def body(meta_ref, tok, gain_ref, wk_ref, wv_ref, kg, kv_out, normed_out, w_out, acc, wide):
        step = pl.program_id(0)

        @pl.when(step == 0)
        def _():
            norm_into([tok], lambda i: 0, gain_ref, normed_out)
            acc[...] = jnp.zeros_like(acc)

        unpack_weight(wk_ref, wide, hd, dims.ca // 128, w_out, 0)
        unpack_weight(wv_ref, wide, hd, dims.va // 128, w_out, hd * dims.ca)
        at = pl.multiple_of(step * dims.chunk, dims.chunk)
        acc[...] += dot(normed_out[:, pl.ds(at, dims.chunk)], w_out[...])

        @pl.when(step == dims.steps - 1)
        def _():
            write_kv(acc[...], kg, meta_ref, dims, kv_out)

    return pl.pallas_call(
        body,
        grid=(dims.steps,),
        in_specs=[
            SMEM,
            whole(tokens.shape),
            whole(gain.shape),
            pl.BlockSpec((wk.shape[0] // dims.steps, 128), lambda i: (i, 0)),
            pl.BlockSpec((wv.shape[0] // dims.steps, 128), lambda i: (i, 0)),
            whole(key_gain.shape),
        ],
        out_specs=[
            whole((dims.rows, dims.kv)),
            whole((dims.rows, dims.model)),
            pl.BlockSpec((dims.chunk, dims.kv), lambda i: (i, 0)),
        ],
        out_shape=[
            jax.ShapeDtypeStruct((dims.rows, dims.kv), BF16),
            jax.ShapeDtypeStruct((dims.rows, dims.model), BF16),
            jax.ShapeDtypeStruct((dims.model, dims.kv), BF16),
        ],
        scratch_shapes=[
            pltpu.VMEM((dims.rows, dims.kv), F32),
            pltpu.VMEM((wk.shape[0] // dims.steps, 128), F32),
        ],
        name="kv_first",
    )(meta, tokens, gain, wk, wv, key_gain)


def kv_other(dims, parts, gain, weights, key_gain, meta):
    count = len(parts)
    piece = parts[0].shape[0]

    def body(meta_ref, *refs):
        toks, (gain_ref, w_ref, kg, kv_out, normed_out) = refs[:count], refs[count:]
        norm_into(toks, lambda i: lax.rem(meta_ref[2] + i, count) * piece, gain_ref, normed_out)
        write_kv(dot(normed_out[...], w_ref[...]), kg, meta_ref, dims, kv_out)

    return pl.pallas_call(
        body,
        in_specs=[SMEM] + [whole(p.shape) for p in parts] + [whole(gain.shape), whole(weights.shape), whole(key_gain.shape)],
        out_specs=[whole((dims.rows, dims.kv)), whole((dims.rows, dims.model))],
        out_shape=[
            jax.ShapeDtypeStruct((dims.rows, dims.kv), BF16),
            jax.ShapeDtypeStruct((dims.rows, dims.model), BF16),
        ],
        name="kv_other",
    )(meta, *parts, gain, weights, key_gain)


def rest_outputs(dims):
    hd, rows = dims.heads, dims.rows
    return [
        jax.ShapeDtypeStruct((rows, hd * dims.ca), BF16),
        jax.ShapeDtypeStruct((rows, hd * dims.ck), BF16),
        jax.ShapeDtypeStruct((rows, hd * dims.cv), F32),
        jax.ShapeDtypeStruct((hd * dims.ck + 16, dims.cv), BF16),
        jax.ShapeDtypeStruct((hd * dims.ck, dims.cv), F32),
        jax.ShapeDtypeStruct((16, dims.ck), F32),
    ]


def local_part(dims, acc, low_rank, meta, slot_state, up, up_wide, bias, retain, query_gain, outs):
    q_out, reach_out, inside_out, send_out, state_out, decay_out = outs
    hd, rows, ck, cv = dims.heads, dims.rows, dims.ck, dims.cv
    gain = jnp.concatenate([query_gain[...], query_gain[...]], axis=1)
    up_wide[...] = up[...].astype(F32)
    retain_columns = jnp.transpose(retain[...])
    head_lane = lax.broadcasted_iota(jnp.int32, retain_columns.shape, 1)
    row_id = lax.broadcasted_iota(jnp.int32, (rows, rows), 0)
    col_id = lax.broadcasted_iota(jnp.int32, (rows, rows), 1)
    same_block = row_id // BLK == col_id // BLK
    lower = row_id >= col_id
    summing = jnp.where(same_block & lower, 1.0, 0.0).astype(F32)
    blocks = rows // BLK
    first = meta[0] == 0
    send_out[hd * ck :, :] = jnp.zeros((16, cv), BF16)
    decay_out[...] = jnp.ones((16, ck), F32)
    for h in range(hd):
        q = acc[:, h * dims.ca : (h + 1) * dims.ca].astype(BF16).astype(F32)
        q_out[:, h * dims.ca : (h + 1) * dims.ca] = rms_halves(q, gain).astype(BF16)
        at = hd * dims.ca + h * ck
        ql = acc[:, at : at + ck].astype(BF16).astype(F32) * ck ** (-0.5)
        at = hd * (dims.ca + ck) + h * ck
        kl = acc[:, at : at + ck].astype(BF16).astype(F32)
        at = hd * (dims.ca + 2 * ck) + h * cv
        vl = acc[:, at : at + cv].astype(BF16)
        head = meta[1] + h
        up_head = up_wide[pl.ds(head, dims.rank, stride=dims.all_heads), :].astype(BF16)
        pre = dot(low_rank, up_head) + bias[pl.ds(head, 1), :]
        gate = jnp.minimum(pre, 0.0) - jnp.log1p(jnp.exp(-jnp.abs(pre)))
        kept = jnp.sum(jnp.where(head_lane == head, retain_columns, 0.0), axis=1, keepdims=True)
        log_decay = gate / TAU + kept
        running = dot(summing, log_decay, precision=HIGH)
        finals = [running[(b + 1) * BLK - 1 : (b + 1) * BLK, :] for b in range(blocks)]
        pivots = [running[b * BLK + BLK // 2 : b * BLK + BLK // 2 + 1, :] for b in range(blocks)]
        q_blocks, reach_blocks, k_ends, inside = [], [], [], []
        before = jnp.zeros_like(finals[0])
        for b in range(blocks):
            here = slice(b * BLK, (b + 1) * BLK)
            run = running[here]
            q_edge = ql[here] * jnp.exp(run)
            q_piv = (ql[here] * jnp.exp(run - pivots[b])).astype(BF16)
            k_piv = (kl[here] * jnp.exp(pivots[b] - run)).astype(BF16)
            own = dot(q_piv, k_piv, ((1,), (1,)))
            own = jnp.where(lower[:BLK, :BLK], own, 0.0).astype(BF16)
            result = dot(own, vl[here])
            gap = jnp.zeros_like(finals[0])
            for c in range(b - 1, -1, -1):
                across = dot(q_edge.astype(BF16), (k_ends[c] * jnp.exp(gap)).astype(BF16), ((1,), (1,)))
                result = result + dot(across.astype(BF16), vl[c * BLK : (c + 1) * BLK])
                gap = gap + finals[c]
            inside.append(result)
            reach_blocks.append((q_edge * jnp.exp(before)).astype(BF16))
            k_ends.append(kl[here] * jnp.exp(finals[b] - run))
            before = before + finals[b]
        for b in range(blocks):
            here = slice(b * BLK, (b + 1) * BLK)
            inside_out[here, h * cv : (h + 1) * cv] = inside[b]
            reach_out[here, h * ck : (h + 1) * ck] = reach_blocks[b]
        later = jnp.zeros_like(finals[0])
        faded = [None] * blocks
        for b in range(blocks - 1, -1, -1):
            faded[b] = (k_ends[b] * jnp.exp(later)).astype(BF16)
            later = later + finals[b]
        state = dot(jnp.concatenate(faded, axis=0), vl, ((0,), (0,)))
        decay = jnp.exp(before)
        columns = dot(decay, jnp.ones((1, cv), F32), ((0,), (0,)), precision=HIGH)
        begin = jnp.where(first, slot_state[h * ck : (h + 1) * ck, :], 0.0)
        state = state + columns * begin
        state_out[h * ck : (h + 1) * ck, :] = state
        send_out[h * ck : (h + 1) * ck, :] = state.astype(BF16)
        send_out[hd * ck + h : hd * ck + h + 1, :ck] = decay.astype(BF16)
        decay_out[h : h + 1, :] = decay


def rest_specs(dims, consts):
    return [whole(c.shape) for c in consts], [whole(s.shape) for s in rest_outputs(dims)]


def rest_first(dims, normed, weights, down, consts, meta):
    hd = dims.heads
    const_specs, out_specs = rest_specs(dims, consts)
    n_const = len(consts)
    widest = max(w.shape[0] for w in weights) // dims.steps

    def body(meta_ref, normed_ref, wq, wql, wkl, wvl, down_ref, *refs):
        consts_in, outs = refs[:n_const], refs[n_const : n_const + 6]
        w_out, acc, wide, up_wide = refs[n_const + 6 :]
        step = pl.program_id(0)

        @pl.when(step == 0)
        def _():
            acc[...] = jnp.zeros_like(acc)

        unpack_weight(wq, wide, hd, dims.ca // 128, w_out, 0)
        unpack_weight(wql, wide, hd, dims.ck // 128, w_out, hd * dims.ca)
        unpack_weight(wkl, wide, hd, dims.ck // 128, w_out, hd * (dims.ca + dims.ck))
        unpack_weight(wvl, wide, hd, dims.cv // 128, w_out, hd * (dims.ca + 2 * dims.ck))
        at = pl.multiple_of(step * dims.chunk, dims.chunk)
        acc[...] += dot(normed_ref[:, pl.ds(at, dims.chunk)], w_out[...])

        @pl.when(step == dims.steps - 1)
        def _():
            low = dot(normed_ref[...], down_ref[...], ((1,), (1,))).astype(BF16)
            slot_state, up, bias, retain, query_gain = consts_in
            local_part(dims, acc, low, meta_ref, slot_state, up, up_wide, bias, retain, query_gain, outs)

    return pl.pallas_call(
        body,
        grid=(dims.steps,),
        in_specs=[SMEM, whole(normed.shape)]
        + [pl.BlockSpec((w.shape[0] // dims.steps, 128), lambda i: (i, 0)) for w in weights]
        + [whole(down.shape)]
        + const_specs,
        out_specs=out_specs + [pl.BlockSpec((dims.chunk, dims.rest), lambda i: (i, 0))],
        out_shape=rest_outputs(dims) + [jax.ShapeDtypeStruct((dims.model, dims.rest), BF16)],
        scratch_shapes=[
            pltpu.VMEM((dims.rows, dims.rest), F32),
            pltpu.VMEM((widest, 128), F32),
            pltpu.VMEM(consts[1].shape, F32),
        ],
        name="rest_first",
    )(meta, normed, *weights, down, *consts)


def rest_other(dims, normed, weights, down, consts, meta):
    const_specs, out_specs = rest_specs(dims, consts)
    n_const = len(consts)

    def body(meta_ref, normed_ref, w_ref, down_ref, *refs):
        consts_in, outs = refs[:n_const], refs[n_const : n_const + 6]
        acc, up_wide = refs[n_const + 6 :]
        acc[...] = dot(normed_ref[...], w_ref[...])
        low = dot(normed_ref[...], down_ref[...], ((1,), (1,))).astype(BF16)
        slot_state, up, bias, retain, query_gain = consts_in
        local_part(dims, acc, low, meta_ref, slot_state, up, up_wide, bias, retain, query_gain, outs)

    return pl.pallas_call(
        body,
        in_specs=[SMEM, whole(normed.shape), whole(weights.shape), whole(down.shape)] + const_specs,
        out_specs=out_specs,
        out_shape=rest_outputs(dims),
        scratch_shapes=[pltpu.VMEM((dims.rows, dims.rest), F32), pltpu.VMEM(consts[1].shape, F32)],
        name="rest_other",
    )(meta, normed, weights, down, *consts)


def columns_of(row, width):
    return dot(row, jnp.ones((1, width), row.dtype), ((0,), (0,)), precision=HIGH if row.dtype == F32 else None)


def combine(dims, bit, state, decay, prefix, prefix_decay, received, meta):
    hd, ck, cv = dims.heads, dims.ck, dims.cv

    def body(meta_ref, st, dec, pre, pre_dec, rec, send_out, st_out, dec_out, pre_out, pre_dec_out):
        upper = (meta_ref[0] // bit) % 2 == 1
        send_out[hd * ck :, :] = jnp.zeros((16, cv), BF16)
        dec_out[...] = jnp.ones_like(dec_out)
        pre_dec_out[...] = jnp.ones_like(pre_dec_out)
        for h in range(hd):
            at = slice(h * ck, (h + 1) * ck)
            other = rec[at, :].astype(F32)
            other_dec = rec[hd * ck + h : hd * ck + h + 1, :ck].astype(F32)
            mine, mine_dec = st[at, :], dec[h : h + 1, :]
            earlier = jnp.where(upper, other, mine)
            late = jnp.where(upper, mine, other)
            total = earlier * columns_of(jnp.where(upper, mine_dec, other_dec), cv) + late
            st_out[at, :] = total
            send_out[at, :] = total.astype(BF16)
            both = mine_dec * other_dec
            dec_out[h : h + 1, :] = both
            send_out[hd * ck + h : hd * ck + h + 1, :ck] = both.astype(BF16)
            pre_row = pre_dec[h : h + 1, :]
            pre_out[at, :] = pre[at, :] + jnp.where(upper, columns_of(pre_row, cv) * other, 0.0)
            pre_dec_out[h : h + 1, :] = jnp.where(upper, pre_row * other_dec, pre_row)

    shapes = [
        jax.ShapeDtypeStruct((hd * ck + 16, cv), BF16),
        jax.ShapeDtypeStruct((hd * ck, cv), F32),
        jax.ShapeDtypeStruct((16, ck), F32),
        jax.ShapeDtypeStruct((hd * ck, cv), F32),
        jax.ShapeDtypeStruct((16, ck), F32),
    ]
    args = (state, decay, prefix, prefix_decay, received)
    return pl.pallas_call(
        body,
        in_specs=[SMEM] + [whole(a.shape) for a in args],
        out_specs=[whole(s.shape) for s in shapes],
        out_shape=shapes,
        name="combine",
    )(meta, *args)


def finish(dims, bit, slot_index, kv_blocks, q_unit, reach, inside, prefix, prefix_decay, received, gains, lam, meta):
    hd, rows, ca, va, ck, cv = dims.heads, dims.rows, dims.ca, dims.va, dims.ck, dims.cv
    count = len(kv_blocks)
    mix_gain, state_gain = gains
    scale = (ca // 2) ** (-0.5)

    def body(meta_ref, lam_ref, *refs):
        kvs = refs[:count]
        q_ref, reach_ref, inside_ref, pre, pre_dec, rec, mix_ref, sg_ref, out = refs[count:]
        place = meta_ref[0]
        lane = lax.broadcasted_iota(jnp.int32, (rows, ca), 1)
        row_id = lax.broadcasted_iota(jnp.int32, (2 * rows, rows), 0) % rows
        col_id = lax.broadcasted_iota(jnp.int32, (2 * rows, rows), 1)
        allowed = row_id // BLK >= col_id // BLK
        upper = (place // bit) % 2 == 1
        for h in range(hd):
            q = q_ref[:, h * ca : (h + 1) * ca]
            zero = jnp.zeros_like(q)
            pair = jnp.concatenate([jnp.where(lane < ca // 2, q, zero), jnp.where(lane < ca // 2, zero, q)], axis=0)
            scores = []
            for m in range(count):
                s = dot(pair, kvs[m][:, h * ca : (h + 1) * ca], ((1,), (1,))) * scale
                if m == 0:
                    s = jnp.where(allowed, s, -jnp.inf)
                else:
                    s = jnp.where(jnp.bitwise_xor(place, m) < place, s, -jnp.inf)
                scores.append(s)
            top = functools.reduce(jnp.maximum, [jnp.max(s, axis=1, keepdims=True) for s in scores])
            total = jnp.zeros((2 * rows, 1), F32)
            sums = jnp.zeros((2 * rows, va), F32)
            for m in range(count):
                raised = jnp.exp(scores[m] - top)
                total = total + jnp.sum(raised, axis=1, keepdims=True)
                at = hd * ca + h * va
                sums = sums + dot(raised.astype(BF16), kvs[m][:, at : at + va])
            ratio = sums / total
            diff = ratio[:rows] - lam_ref[meta_ref[1] + h] * ratio[rows:]
            out[:, h * va : (h + 1) * va] = rms(diff, mix_ref[...]).astype(BF16)
            at = slice(h * ck, (h + 1) * ck)
            enter = pre[at, :]
            if rec is not None:
                more = columns_of(pre_dec[h : h + 1, :], cv) * rec[at, :].astype(F32)
                enter = enter + jnp.where(upper, more, 0.0)
            raw = inside_ref[:, h * cv : (h + 1) * cv] + dot(reach_ref[:, h * ck : (h + 1) * ck], enter.astype(BF16))
            at = hd * va + h * cv
            out[:, at : at + cv] = rms(raw, sg_ref[...]).astype(BF16)

    args = (*kv_blocks, q_unit, reach, inside, prefix, prefix_decay, received, mix_gain, state_gain)
    return pl.pallas_call(
        body,
        in_specs=[SMEM, SMEM] + [whole(a.shape) for a in args],
        out_specs=whole((rows, hd * (va + cv))),
        out_shape=jax.ShapeDtypeStruct((rows, hd * (va + cv)), BF16),
        name="finish",
    )(meta, lam, *args)


def project_out(dims, pieces, owners, weights, start):
    wa, wl = weights
    rows, cols = dims.rows, wa.shape[1]
    step_a, step_l = dims.heads * dims.va, dims.heads * dims.cv
    count = len(pieces)
    last = start is not None

    def body(own_ref, *refs):
        parts, (wa_ref, wl_ref) = refs[:count], refs[count : count + 2]
        out = refs[-1]
        total = refs[count + 2][...] if last else jnp.zeros((rows, cols), F32)
        for i in range(count):
            at = pl.multiple_of(own_ref[i] * step_a, step_a)
            total = total + dot(parts[i][:, :step_a], wa_ref[pl.ds(at, step_a), :])
            at = pl.multiple_of(own_ref[i] * step_l, step_l)
            total = total + dot(parts[i][:, step_a:], wl_ref[pl.ds(at, step_l), :])
        out[...] = total.astype(out.dtype)

    args = [*pieces, wa, wl] + ([start] if last else [])
    return pl.pallas_call(
        body,
        in_specs=[SMEM] + [whole(a.shape) for a in args],
        out_specs=whole((rows, cols)),
        out_shape=jax.ShapeDtypeStruct((rows, cols), BF16 if last else F32),
        name="project_last" if last else "project_own",
    )(owners, *args)


def swap(x, axis, bit, size):
    return lax.ppermute(x, axis, [(i, i ^ bit) for i in range(size)])


def shift(x, axis, by, size):
    return lax.ppermute(x, axis, [(i, (i + by) % size) for i in range(size)])


def low_bit(m):
    return m & -m


def body(
    tokens,
    norm_gain,
    query_attend,
    key_attend,
    value_attend,
    query_linear,
    key_linear,
    value_linear,
    decay_down,
    decay_up,
    decay_bias,
    log_retain,
    query_gain,
    key_gain,
    diff_lambda,
    mix_gain,
    state_gain,
    init_state,
    output_attend,
    output_linear,
):
    fs_size, tp_size, sp_size = (lax.axis_size(a) for a in ("fs", "tp", "sp"))
    fs, tp, sp = (lax.axis_index(a).astype(jnp.int32) for a in ("fs", "tp", "sp"))
    dims = Dims(tokens, query_attend, value_attend, key_linear, value_linear, decay_up)
    hd, rows, model = dims.heads, dims.rows, dims.model
    device = fs * tp_size + tp
    meta = jnp.stack([sp, device * hd, tp, fs])

    def flat(w):
        d, h, c = w.shape
        parts = c // 128
        return w.reshape(d, h, parts, 128).transpose(0, 2, 1, 3).reshape(d * parts * h, 128)

    own = tokens[0]
    retain_own = log_retain[0].T
    piece = rows // tp_size
    mine = lax.dynamic_slice_in_dim(own, tp * piece, piece, 0)
    token_parts, retains = [None], [retain_own]
    for j in range(1, fs_size):
        part = shift(mine, "fs", j, fs_size)
        retains.append(shift(retain_own, "fs", j, fs_size))
        token_parts.append([part] + [shift(part, "tp", -i, tp_size) for i in range(1, tp_size)])

    gain = norm_gain.reshape(1, -1)
    kg = key_gain.reshape(-1, key_gain.shape[-1])
    qg = query_gain.reshape(1, -1)
    up = decay_up.reshape(-1, decay_up.shape[-1])
    down = decay_down.T

    def consts(j):
        seq = (fs - j) % fs_size
        state = lax.dynamic_index_in_dim(init_state, seq, 0, False) if fs_size > 1 else init_state[0]
        return state.reshape(hd * dims.ck, dims.cv), up, decay_bias, retains[j], qg

    kv_blocks, results, states = [], [], []

    def spread(kv):
        blocks = [kv]
        for m in range(1, sp_size):
            blocks.append(swap(blocks[m - low_bit(m)] if m != low_bit(m) else kv, "sp", low_bit(m), sp_size))
        return blocks

    def prefix_of(j, outs, begin):
        _, _, _, send, state, decay = outs
        prefix = jnp.where(sp == 0, begin, 0.0)
        prefix_decay = jnp.ones((16, dims.ck), F32)
        bit = 1
        while True:
            received = swap(send, "sp", bit, sp_size)
            if bit * 2 >= sp_size:
                return bit, prefix, prefix_decay, received
            send, state, decay, prefix, prefix_decay = combine(
                dims, bit, state, decay, prefix, prefix_decay, received, meta
            )
            bit *= 2

    kv_w = rest_w = None
    for j in range(fs_size):
        if j == 0:
            kv, normed, kv_w = kv_first(dims, own, gain, flat(key_attend), flat(value_attend), kg, meta)
        else:
            kv, normed = kv_other(dims, token_parts[j], gain, kv_w, kg, meta)
        kv_blocks.append(spread(kv))
        c = consts(j)
        if j == 0:
            *outs, rest_w = rest_first(
                dims, normed, [flat(w) for w in (query_attend, query_linear, key_linear, value_linear)], down, c, meta
            )
        else:
            outs = rest_other(dims, normed, rest_w, down, c, meta)
        results.append(outs)
        states.append(prefix_of(j, outs, c[0]))

    gains = (mix_gain.reshape(1, -1), state_gain.reshape(1, -1))
    weights = (output_attend, output_linear)
    total = None
    late_pieces, late_owners = [], []
    for j in range(fs_size):
        bit, prefix, prefix_decay, received = states[j]
        q_unit, reach, inside = results[j][:3]
        mixed = finish(
            dims, bit, j, kv_blocks[j], q_unit, reach, inside, prefix, prefix_decay, received, gains, diff_lambda, meta
        )
        if j:
            mixed = shift(mixed, "fs", -j, fs_size)
        source = (fs + j) % fs_size
        pieces = [mixed] + [shift(mixed, "tp", -i, tp_size) for i in range(1, tp_size)]
        owners = [source * tp_size + (tp + i) % tp_size for i in range(tp_size)]
        if j == 0 and fs_size > 1:
            total = project_out(dims, pieces, jnp.stack(owners), weights, None)
        else:
            late_pieces += pieces
            late_owners += owners
    result = project_out(dims, late_pieces, jnp.stack(late_owners), weights, total)
    return result.reshape(1, rows, -1)


def solution(mesh):
    heads = P(None, ("fs", "tp"), None)
    positions = P(("grp", "fs"), "sp", None)
    in_specs = (
        positions,
        P(),
        heads,
        heads,
        heads,
        heads,
        heads,
        heads,
        P(),
        P(),
        P(),
        positions,
        P(),
        P(),
        P(),
        P(),
        P(),
        P("grp", ("fs", "tp"), None, None),
        P(None, "tp"),
        P(None, "tp"),
    )
    out_specs = P(("grp", "fs"), "sp", "tp")
    return jax.shard_map(body, mesh=mesh, in_specs=in_specs, out_specs=out_specs, check_vma=False)
```

time: 176 us -> 100 us (0.57)
  the two profiles are of different devices: /device:TPU:31 before, /device:TPU:0 now
where the time goes in v1:
time: 100 us; the launch traced here: 99.6 us
  Pallas kernels  44.1 us (44%)
  waiting for transfers between devices  23.6 us (24%)
  starting transfers between devices  20.8 us (21%)
  local copies, waits for them, and re-layouts  8.28 us (8%)
  other arithmetic  2.66 us (3%)
    ppermute x10, waiting for transfers between devices, swap(): return lax.ppermute(x, axis, [(i, i ^ bit) for i in range(size)])  16.8 us
    ppermute x10, starting transfers between devices, swap(): return lax.ppermute(x, axis, [(i, i ^ bit) for i in range(size)])  14.9 us
    pallas_call x1, Pallas kernels, rest_first(): pl.pallas_call(body, grid=(dims.steps,), in_specs=[SMEM, whole(normed.sha...  9.19 us
    pallas_call x2, Pallas kernels, project_out(): pl.pallas_call(body, in_specs=[SMEM] + [whole(a.shape) for a in args], ou...  8.82 us
    ppermute x6, waiting for transfers between devices, shift(): return lax.ppermute(x, axis, [(i, (i + by) % size) for i in range(size)])  6.78 us
    pallas_call x2, Pallas kernels, finish(): pl.pallas_call(body, in_specs=[SMEM, SMEM] + [whole(a.shape) for a in arg...  6.59 us
    pallas_call x1, Pallas kernels, rest_other(): pl.pallas_call(body, in_specs=[SMEM, whole(normed.shape), whole(weights.s...  5.94 us
    ppermute x6, starting transfers between devices, shift(): return lax.ppermute(x, axis, [(i, (i + by) % size) for i in range(size)])  5.82 us
  transfers between devices with their start and end apart: 16, of which 7 were waited for; matrix products, arithmetic and copies ran while one was open for 5% of the time, Pallas kernels for 40%

profile of v1, /device:TPU:0, one launch (start us, length us, event | category | flops | bytes accessed | tf_op | source)
XLA Modules:
  0.0 99.6 jit_solution(6555065257323157112)
XLA Ops:
  1.0 3.0 %collective-permute-start = (bf16[64,2048]{1,0:T(8,128)(2,1)S(1)}, bf16[64,2048]{1,0:T(8,128)(2,1)S(1)}, u32[]{:S(2)}, u32[]{:S(2)}) collective-permute-start(bf16[64,2048]{1,0:T(8,128)(2,1)S(1)} %dynamic-slice_bitcast_fusion), channel_id=1, source_target_pairs={{0,2},{2,0},{1,3},{3,1},{4,6},{6,4},{5,7},{7,5},{8,10},{10,8},{9,1... | collective-permute-start | bytes 786440 | tf_op jit(solution)/shard_map/ppermute | solution.py:453
  4.0 6.3 %collective-permute-done.refs_0_ = bf16[64,2048]{1,0:T(8,128)(2,1)S(1)} collective-permute-done((bf16[64,2048]{1,0:T(8,128)(2,1)S(1)}, bf16[64,2048]{1,0:T(8,128)(2,1)S(1)}, u32[]{:S(2)}, u32[]{:S(2)}) %collective-permute-start) | collective-permute-done | bytes 262176 | tf_op jit(solution)/shard_map/ppermute | solution.py:453
  10.3 1.7 %collective-permute-start.5 = (f32[8,128]{1,0:T(8,128)}, f32[8,128]{1,0:T(8,128)S(1)}, u32[]{:S(2)}, u32[]{:S(2)}) collective-permute-start(f32[8,128]{1,0:T(8,128)} %bitcast.53), channel_id=1, source_target_pairs={{0,2},{2,0},{1,3},{3,1},{4,6},{6,4},{5,7},{7,5},{8,10},{10,8},{9,1... | collective-permute-start | bytes 12296 | tf_op jit(solution)/shard_map/ppermute | solution.py:453
  12.1 1.9 %constant_dynamic-slice_fusion = (f32[1,2,128,256]{3,2,1,0:T(8,128)}, f32[1,2,128,256]{3,2,1,0:T(8,128)}) fusion(f32[2,2,128,256]{3,2,1,0:T(8,128)} %param.37, s32[]{:T(128)S(6)} %select_n.58, s32[]{:T(128)S(6)} %select_n.56), kind=kLoop, calls=%fused_computation.3 | loop fusion | bytes 1048584 | tf_op jit(solution)/shard_map/jit(dynamic_index_in_dim)/dynamic_slice | solution.py:512
  14.5 5.3 %kv_first.1 = (bf16[128,512]{1,0:T(8,128)(2,1)}, bf16[128,2048]{1,0:T(8,128)(2,1)}, bf16[2048,512]{1,0:T(8,128)(2,1)}) custom-call(s32[4]{0:T(128)} %pad_add_fusion.1.meta_ref, bf16[128,2048]{1,0:T(8,128)(2,1)} %bitcast.39, f32[1,2048]{1,0:T(1,128)} %bitcast.49, bf16[4096,128]{1,0:T(8,128)(2,1)} %bitcast.43, bf16[4096,128]{1,0:T(8,128)(2,1)} %bitcast.44, ...), custom_call_target="tpu_custom_call" | custom-call | tf_op jit(solution)/shard_map/kv_first/pallas_call | solution.py:109
  19.8 9.2 %rest_first.1 = (bf16[128,256]{1,0:T(8,128)(2,1)}, bf16[128,256]{1,0:T(8,128)(2,1)}, f32[128,512]{1,0:T(8,128)}, bf16[272,256]{1,0:T(8,128)(2,1)}, f32[256,256]{...) custom-call(s32[4]{0:T(128)} %pad_add_fusion.1.meta_ref, bf16[128,2048]{1,0:T(8,128)(2,1)} %get-tuple-element.32.normed_ref, ...), custom_call_target="tpu_custom_call" | custom-call | tf_op jit(solution)/shard_map/rest_first/pallas_call | solution.py:277
  29.7 3.1 %kv_other.1 = (bf16[128,512]{1,0:T(8,128)(2,1)}, bf16[128,2048]{1,0:T(8,128)(2,1)}) custom-call(s32[4]{0:T(128)} %pad_add_fusion.1.meta_ref, bf16[64,2048]{1,0:T(8,128)(2,1)} %copy-done.2, bf16[64,2048]{1,0:T(8,128)(2,1)} %copy-done.3, f32[1,2048]{1,0:T(1,128)} %bitcast.50, bf16[2048,512]{1,0:T(8,128)(2,1)} %get-tuple-element.29.refs_3_, f32[16,64]{1,0:T(8,128)} %bitcast.52), custom_call_target="tpu_custom_call" | custom-call | tf_op jit(solution)/shard_map/kv_other/pallas_call | solution.py:147
  32.8 2.6 %collective-permute-start.3 = (bf16[128,512]{1,0:T(8,128)(2,1)}, bf16[128,512]{1,0:T(8,128)(2,1)S(1)}, u32[]{:S(2)}, u32[]{:S(2)}) collective-permute-start(bf16[128,512]{1,0:T(8,128)(2,1)} %get-tuple-element.30.refs_0_), channel_id=1, source_target_pairs={{0,8},{4,12},{8,0},{12,4},{1,9},{5,13},{9,1},{13,5},{2,10},{6,14},... | collective-permute-start | bytes 393224 | tf_op jit(solution)/shard_map/ppermute | solution.py:449
  36.0 5.9 %rest_other.1 = (bf16[128,256]{1,0:T(8,128)(2,1)}, bf16[128,256]{1,0:T(8,128)(2,1)}, f32[128,512]{1,0:T(8,128)}, bf16[272,256]{1,0:T(8,128)(2,1)}, f32[256,256]{1,0:T(8,128)}, /*index=5*/f32[16,128]{1,0:T(8,128)}) custom-call(s32[4]{0:T(128)} %pad_add_fusion.1.meta_ref, bf16[128,2048]{1,0:T(8,128)(2,1)} %get-tuple-element.31.normed_ref, ...), custom_call_target="tpu_custom_call" | custom-call | tf_op jit(solution)/shard_map/rest_other/pallas_call | solution.py:307
  42.0 1.6 %collective-permute-start.6 = (bf16[272,256]{1,0:T(8,128)(2,1)}, bf16[272,256]{1,0:T(8,128)(2,1)S(1)}, u32[]{:S(2)}, u32[]{:S(2)}) collective-permute-start(bf16[272,256]{1,0:T(8,128)(2,1)} %get-tuple-element.39), channel_id=1, source_target_pairs={{0,4},{4,0},{8,12},{12,8},{1,5},{5,1},{9,13},{13,9},{2,6},{6,2},{1... | collective-permute-start | bytes 417800 | tf_op jit(solution)/shard_map/ppermute | solution.py:449
  44.3 3.4 %collective-permute-done.6.rec = bf16[272,256]{1,0:T(8,128)(2,1)S(1)} collective-permute-done((bf16[272,256]{1,0:T(8,128)(2,1)}, bf16[272,256]{1,0:T(8,128)(2,1)S(1)}, u32[]{:S(2)}, u32[]{:S(2)}) %collective-permute-start.6) | collective-permute-done | bytes 139296 | tf_op jit(solution)/shard_map/ppermute | solution.py:449
  48.4 2.6 %combine.2 = (bf16[272,256]{1,0:T(8,128)(2,1)}, f32[256,256]{1,0:T(8,128)}, f32[16,128]{1,0:T(8,128)}, f32[256,256]{1,0:T(8,128)}, f32[16,128]{1,0:T(8,128)}) custom-call(s32[4]{0:T(128)} %pad_add_fusion.1.meta_ref, f32[256,256]{1,0:T(8,128)} %get-tuple-element.37.st, f32[16,128]{1,0:T(8,128)} %get-tuple-element.38.dec, ...), custom_call_target="tpu_custom_call" | custom-call | tf_op jit(solution)/shard_map/combine/pallas_call | solution.py:354
  51.4 1.6 %collective-permute-start.2 = (bf16[128,512]{1,0:T(8,128)(2,1)S(1)}, bf16[128,512]{1,0:T(8,128)(2,1)S(1)}, u32[]{:S(2)}, u32[]{:S(2)}) collective-permute-start(bf16[128,512]{1,0:T(8,128)(2,1)S(1)} %copy-done.13), channel_id=1, source_target_pairs={{0,4},{4,0},{8,12},{12,8},{1,5},{5,1},{9,13},{13,9},{2,6},{6,2},{1... | collective-permute-start | bytes 393224 | tf_op jit(solution)/shard_map/ppermute | solution.py:449
  53.4 2.6 %collective-permute-start.11 = (bf16[128,512]{1,0:T(8,128)(2,1)S(1)}, bf16[128,512]{1,0:T(8,128)(2,1)S(1)}, u32[]{:S(2)}, u32[]{:S(2)}) collective-permute-start(bf16[128,512]{1,0:T(8,128)(2,1)S(1)} %copy-done.11), channel_id=1, source_target_pairs={{0,8},{4,12},{8,0},{12,4},{1,9},{5,13},{9,1},{13,5},{2,10},{6,14},... | collective-permute-start | bytes 393224 | tf_op jit(solution)/shard_map/ppermute | solution.py:449
  57.6 1.9 %collective-permute-done.2.refs_1_ = bf16[128,512]{1,0:T(8,128)(2,1)S(1)} collective-permute-done((bf16[128,512]{1,0:T(8,128)(2,1)S(1)}, bf16[128,512]{1,0:T(8,128)(2,1)S(1)}, u32[]{:S(2)}, u32[]{:S(2)}) %collective-permute-start.2) | collective-permute-done | bytes 131104 | tf_op jit(solution)/shard_map/ppermute | solution.py:449
  59.4 5.9 %collective-permute-done.4.refs_3_ = bf16[128,512]{1,0:T(8,128)(2,1)S(1)} collective-permute-done((bf16[128,512]{1,0:T(8,128)(2,1)S(1)}, bf16[128,512]{1,0:T(8,128)(2,1)S(1)}, u32[]{:S(2)}, u32[]{:S(2)}) %collective-permute-start.4) | collective-permute-done | bytes 131104 | tf_op jit(solution)/shard_map/ppermute | solution.py:449
  66.0 3.3 %finish.2 = bf16[128,768]{1,0:T(8,128)(2,1)} custom-call(s32[4]{0:T(128)} %pad_add_fusion.1.meta_ref, f32[8]{0:T(128)} %lam_ref.3, bf16[128,512]{1,0:T(8,128)(2,1)} %get-tuple-element.30.refs_0_, bf16[128,512]{1,0:T(8,128)(2,1)} %copy-done.15, bf16[128,512]{1,0:T(8,128)(2,1)} %copy-done.14, bf16[128,512]{1,0:T(8,128)(2,1)} %copy-done.16, ...), custom_call_target="tpu_custom_call" | custom-call | tf_op jit(solution)/shard_map/finish/pallas_call | solution.py:411
  71.3 2.6 %combine.3 = (bf16[272,256]{1,0:T(8,128)(2,1)}, f32[256,256]{1,0:T(8,128)}, f32[16,128]{1,0:T(8,128)}, f32[256,256]{1,0:T(8,128)}, f32[16,128]{1,0:T(8,128)}) custom-call(s32[4]{0:T(128)} %pad_add_fusion.1.meta_ref, f32[256,256]{1,0:T(8,128)} %get-tuple-element.47.st, f32[16,128]{1,0:T(8,128)} %get-tuple-element.48.dec, ...), custom_call_target="tpu_custom_call" | custom-call | tf_op jit(solution)/shard_map/combine/pallas_call | solution.py:354
  73.9 1.6 %collective-permute-start.14 = (bf16[272,256]{1,0:T(8,128)(2,1)}, bf16[272,256]{1,0:T(8,128)(2,1)S(1)}, u32[]{:S(2)}, u32[]{:S(2)}) collective-permute-start(bf16[272,256]{1,0:T(8,128)(2,1)} %get-tuple-element.52), channel_id=1, source_target_pairs={{0,8},{4,12},{8,0},{12,4},{1,9},{5,13},{9,1},{13,5},{2,10},{6,14},... | collective-permute-start | bytes 417800 | tf_op jit(solution)/shard_map/ppermute | solution.py:449
  75.5 2.5 %collective-permute-start.10 = (bf16[128,512]{1,0:T(8,128)(2,1)S(1)}, bf16[128,512]{1,0:T(8,128)(2,1)S(1)}, u32[]{:S(2)}, u32[]{:S(2)}) collective-permute-start(bf16[128,512]{1,0:T(8,128)(2,1)S(1)} %copy-done.11), channel_id=1, source_target_pairs={{0,4},{4,0},{8,12},{12,8},{1,5},{5,1},{9,13},{13,9},{2,6},{6,2},{1... | collective-permute-start | bytes 393224 | tf_op jit(solution)/shard_map/ppermute | solution.py:449
  78.1 4.2 %collective-permute-done.10.refs_1_ = bf16[128,512]{1,0:T(8,128)(2,1)S(1)} collective-permute-done((bf16[128,512]{1,0:T(8,128)(2,1)S(1)}, bf16[128,512]{1,0:T(8,128)(2,1)S(1)}, u32[]{:S(2)}, u32[]{:S(2)}) %collective-permute-start.10) | collective-permute-done | bytes 131104 | tf_op jit(solution)/shard_map/ppermute | solution.py:449
  84.4 3.3 %finish.3.refs_0_ = bf16[128,768]{1,0:T(8,128)(2,1)} custom-call(s32[4]{0:T(128)} %pad_add_fusion.1.meta_ref, f32[8]{0:T(128)} %lam_ref.3, bf16[128,512]{1,0:T(8,128)(2,1)} %get-tuple-element.43.refs_0_, bf16[128,512]{1,0:T(8,128)(2,1)} %copy-done.17, bf16[128,512]{1,0:T(8,128)(2,1)} %copy-done.12, bf16[128,512]{1,0:T(8,128)(2,1)} %copy-done.18, ...), custom_call_target="tpu_custom_call" | custom-call | tf_op jit(solution)/shard_map/finish/pallas_call | solution.py:411
  90.0 4.4 %project_own.1.refs_4_ = f32[128,1024]{1,0:T(8,128)} custom-call(s32[2]{0:T(128)} %get-tuple-element.56.own_ref, bf16[128,768]{1,0:T(8,128)(2,1)} %finish.3.refs_0_, bf16[128,768]{1,0:T(8,128)(2,1)} %copy-done.4, bf16[1024,1024]{1,0:T(8,128)(2,1)} %refs_2_.7, bf16[2048,1024]{1,0:T(8,128)(2,1)} %refs_3_.3), custom_call_target="tpu_custom_call" | custom-call | tf_op jit(solution)/shard_map/project_own/pallas_call | solution.py:439
  95.2 4.4 %project_last.1 = bf16[128,1024]{1,0:T(8,128)(2,1)} custom-call(s32[2]{0:T(128)} %get-tuple-element.55.own_ref, bf16[128,768]{1,0:T(8,128)(2,1)} %copy-done.5, bf16[128,768]{1,0:T(8,128)(2,1)} %copy-done.6, bf16[1024,1024]{1,0:T(8,128)(2,1)} %refs_2_.7, bf16[2048,1024]{1,0:T(8,128)(2,1)} %refs_3_.3, f32[128,1024]{1,0:T(8,128)} %project_own.1.refs_4_), custom_call_target="tpu_custom_call" | custom-call | tf_op jit(solution)/shard_map/project_last/pallas_call | solution.py:439
  (67 shorter events, 14.4 us)
Async XLA Ops:
  1.0 9.3 %collective-permute-start = (bf16[64,2048]{1,0:T(8,128)(2,1)S(1)}, bf16[64,2048]{1,0:T(8,128)(2,1)S(1)}, u32[]{:S(2)}, u32[]{:S(2)}) collective-permute-start(bf16[64,2048]{1,0:T(8,128)(2,1)S(1)} %dynamic-slice_bitcast_fusion), channel_id=1, source_target_pairs={{0,2},{2,0},{1,3},{3,1},{4,6},{6,4},{5,7},{7,5},{8,10},{10,8},{9,1... | collective-permute-start | bytes 786440 | tf_op jit(solution)/shard_map/ppermute | solution.py:453
  10.3 18.7 %copy-start.2 = (bf16[64,2048]{1,0:T(8,128)(2,1)}, bf16[64,2048]{1,0:T(8,128)(2,1)S(1)}, u32[]{:S(2)}) copy-start(bf16[64,2048]{1,0:T(8,128)(2,1)S(1)} %collective-permute-done.refs_0_) | copy-start | bytes 786436
  10.3 18.7 %collective-permute-start.1 = (bf16[64,2048]{1,0:T(8,128)(2,1)S(1)}, bf16[64,2048]{1,0:T(8,128)(2,1)S(1)}, u32[]{:S(2)}, u32[]{:S(2)}) collective-permute-start(bf16[64,2048]{1,0:T(8,128)(2,1)S(1)} %collective-permute-done.refs_0_), channel_id=1, source_target_pairs={{0,1},{1,0},{2,3},{3,2},{4,5},{5,4},{6,7},{7,6},{8,9},{9,8},{10,11... | collective-permute-start | bytes 786440 | tf_op jit(solution)/shard_map/ppermute | solution.py:453
  10.3 25.1 %collective-permute-start.5 = (f32[8,128]{1,0:T(8,128)}, f32[8,128]{1,0:T(8,128)S(1)}, u32[]{:S(2)}, u32[]{:S(2)}) collective-permute-start(f32[8,128]{1,0:T(8,128)} %bitcast.53), channel_id=1, source_target_pairs={{0,2},{2,0},{1,3},{3,1},{4,6},{6,4},{5,7},{7,5},{8,10},{10,8},{9,1... | collective-permute-start | bytes 12296 | tf_op jit(solution)/shard_map/ppermute | solution.py:453
  32.8 20.1 %collective-permute-start.3 = (bf16[128,512]{1,0:T(8,128)(2,1)}, bf16[128,512]{1,0:T(8,128)(2,1)S(1)}, u32[]{:S(2)}, u32[]{:S(2)}) collective-permute-start(bf16[128,512]{1,0:T(8,128)(2,1)} %get-tuple-element.30.refs_0_), channel_id=1, source_target_pairs={{0,8},{4,12},{8,0},{12,4},{1,9},{5,13},{9,1},{13,5},{2,10},{6,14},... | collective-permute-start | bytes 393224 | tf_op jit(solution)/shard_map/ppermute | solution.py:449
  36.0 7.6 %copy-start.1 = (f32[1,2,128,256]{3,2,1,0:T(8,128)S(1)}, f32[1,2,128,256]{3,2,1,0:T(8,128)}, u32[]{:S(2)}) copy-start(f32[1,2,128,256]{3,2,1,0:T(8,128)} %get-tuple-element.53) | copy-start | bytes 786436
  36.0 15.3 %copy-start.13 = (bf16[128,512]{1,0:T(8,128)(2,1)S(1)}, bf16[128,512]{1,0:T(8,128)(2,1)}, u32[]{:S(2)}) copy-start(bf16[128,512]{1,0:T(8,128)(2,1)} %get-tuple-element.30.refs_0_) | copy-start | bytes 393220
  36.0 17.4 %copy-start.11 = (bf16[128,512]{1,0:T(8,128)(2,1)S(1)}, bf16[128,512]{1,0:T(8,128)(2,1)}, u32[]{:S(2)}) copy-start(bf16[128,512]{1,0:T(8,128)(2,1)} %get-tuple-element.43.refs_0_) | copy-start | bytes 393220
  36.0 20.0 %copy-start.20 = (bf16[272,256]{1,0:T(8,128)(2,1)S(1)}, bf16[272,256]{1,0:T(8,128)(2,1)}, u32[]{:S(2)}) copy-start(bf16[272,256]{1,0:T(8,128)(2,1)} %get-tuple-element.49) | copy-start | bytes 417796
  42.0 27.9 %copy-start = (f32[1,2,128,256]{3,2,1,0:T(8,128)S(1)}, f32[1,2,128,256]{3,2,1,0:T(8,128)}, u32[]{:S(2)}) copy-start(f32[1,2,128,256]{3,2,1,0:T(8,128)} %get-tuple-element.54) | copy-start | bytes 786436
  42.0 5.8 %collective-permute-start.6 = (bf16[272,256]{1,0:T(8,128)(2,1)}, bf16[272,256]{1,0:T(8,128)(2,1)S(1)}, u32[]{:S(2)}, u32[]{:S(2)}) collective-permute-start(bf16[272,256]{1,0:T(8,128)(2,1)} %get-tuple-element.39), channel_id=1, source_target_pairs={{0,4},{4,0},{8,12},{12,8},{1,5},{5,1},{9,13},{13,9},{2,6},{6,2},{1... | collective-permute-start | bytes 417800 | tf_op jit(solution)/shard_map/ppermute | solution.py:449
  51.0 14.3 %collective-permute-start.7 = (bf16[272,256]{1,0:T(8,128)(2,1)}, bf16[272,256]{1,0:T(8,128)(2,1)S(1)}, u32[]{:S(2)}, u32[]{:S(2)}) collective-permute-start(bf16[272,256]{1,0:T(8,128)(2,1)} %get-tuple-element.42), channel_id=1, source_target_pairs={{0,8},{4,12},{8,0},{12,4},{1,9},{5,13},{9,1},{13,5},{2,10},{6,14},... | collective-permute-start | bytes 417800 | tf_op jit(solution)/shard_map/ppermute | solution.py:449
  51.4 8.1 %collective-permute-start.2 = (bf16[128,512]{1,0:T(8,128)(2,1)S(1)}, bf16[128,512]{1,0:T(8,128)(2,1)S(1)}, u32[]{:S(2)}, u32[]{:S(2)}) collective-permute-start(bf16[128,512]{1,0:T(8,128)(2,1)S(1)} %copy-done.13), channel_id=1, source_target_pairs={{0,4},{4,0},{8,12},{12,8},{1,5},{5,1},{9,13},{13,9},{2,6},{6,2},{1... | collective-permute-start | bytes 393224 | tf_op jit(solution)/shard_map/ppermute | solution.py:449
  52.9 12.4 %copy-start.14 = (bf16[128,512]{1,0:T(8,128)(2,1)}, bf16[128,512]{1,0:T(8,128)(2,1)S(1)}, u32[]{:S(2)}) copy-start(bf16[128,512]{1,0:T(8,128)(2,1)S(1)} %collective-permute-done.3.refs_2_) | copy-start | bytes 393220
  52.9 12.4 %collective-permute-start.4 = (bf16[128,512]{1,0:T(8,128)(2,1)S(1)}, bf16[128,512]{1,0:T(8,128)(2,1)S(1)}, u32[]{:S(2)}, u32[]{:S(2)}) collective-permute-start(bf16[128,512]{1,0:T(8,128)(2,1)S(1)} %collective-permute-done.3.refs_2_), channel_id=1, source_target_pairs={{0,4},{4,0},{8,12},{12,8},{1,5},{5,1},{9,13},{13,9},{2,6},{6,2},{1... | collective-permute-start | bytes 393224 | tf_op jit(solution)/shard_map/ppermute | solution.py:449
  53.4 24.6 %collective-permute-start.11 = (bf16[128,512]{1,0:T(8,128)(2,1)S(1)}, bf16[128,512]{1,0:T(8,128)(2,1)S(1)}, u32[]{:S(2)}, u32[]{:S(2)}) collective-permute-start(bf16[128,512]{1,0:T(8,128)(2,1)S(1)} %copy-done.11), channel_id=1, source_target_pairs={{0,8},{4,12},{8,0},{12,4},{1,9},{5,13},{9,1},{13,5},{2,10},{6,14},... | collective-permute-start | bytes 393224 | tf_op jit(solution)/shard_map/ppermute | solution.py:449
  56.0 14.6 %collective-permute-start.13 = (bf16[272,256]{1,0:T(8,128)(2,1)S(1)}, bf16[272,256]{1,0:T(8,128)(2,1)S(1)}, u32[]{:S(2)}, u32[]{:S(2)}) collective-permute-start(bf16[272,256]{1,0:T(8,128)(2,1)S(1)} %copy-done.20), channel_id=1, source_target_pairs={{0,4},{4,0},{8,12},{12,8},{1,5},{5,1},{9,13},{13,9},{2,6},{6,2},{1... | collective-permute-start | bytes 417800 | tf_op jit(solution)/shard_map/ppermute | solution.py:449
  69.3 18.4 %collective-permute-start.8 = (bf16[128,768]{1,0:T(8,128)(2,1)}, bf16[128,768]{1,0:T(8,128)(2,1)S(1)}, u32[]{:S(2)}, u32[]{:S(2)}) collective-permute-start(bf16[128,768]{1,0:T(8,128)(2,1)} %finish.2), channel_id=1, source_target_pairs={{0,2},{2,0},{1,3},{3,1},{4,6},{6,4},{5,7},{7,5},{8,10},{10,8},{9,1... | collective-permute-start | bytes 589832 | tf_op jit(solution)/shard_map/ppermute | solution.py:453
  73.9 9.8 %collective-permute-start.14 = (bf16[272,256]{1,0:T(8,128)(2,1)}, bf16[272,256]{1,0:T(8,128)(2,1)S(1)}, u32[]{:S(2)}, u32[]{:S(2)}) collective-permute-start(bf16[272,256]{1,0:T(8,128)(2,1)} %get-tuple-element.52), channel_id=1, source_target_pairs={{0,8},{4,12},{8,0},{12,4},{1,9},{5,13},{9,1},{13,5},{2,10},{6,14},... | collective-permute-start | bytes 417800 | tf_op jit(solution)/shard_map/ppermute | solution.py:449
  75.5 6.8 %collective-permute-start.10 = (bf16[128,512]{1,0:T(8,128)(2,1)S(1)}, bf16[128,512]{1,0:T(8,128)(2,1)S(1)}, u32[]{:S(2)}, u32[]{:S(2)}) collective-permute-start(bf16[128,512]{1,0:T(8,128)(2,1)S(1)} %copy-done.11), channel_id=1, source_target_pairs={{0,4},{4,0},{8,12},{12,8},{1,5},{5,1},{9,13},{13,9},{2,6},{6,2},{1... | collective-permute-start | bytes 393224 | tf_op jit(solution)/shard_map/ppermute | solution.py:449
  78.0 5.7 %collective-permute-start.12 = (bf16[128,512]{1,0:T(8,128)(2,1)S(1)}, bf16[128,512]{1,0:T(8,128)(2,1)S(1)}, u32[]{:S(2)}, u32[]{:S(2)}) collective-permute-start(bf16[128,512]{1,0:T(8,128)(2,1)S(1)} %collective-permute-done.11.refs_2_), channel_id=1, source_target_pairs={{0,4},{4,0},{8,12},{12,8},{1,5},{5,1},{9,13},{13,9},{2,6},{6,2},{1... | collective-permute-start | bytes 393224 | tf_op jit(solution)/shard_map/ppermute | solution.py:449
  87.7 1.7 %collective-permute-start.15 = (bf16[128,768]{1,0:T(8,128)(2,1)}, bf16[128,768]{1,0:T(8,128)(2,1)S(1)}, u32[]{:S(2)}, u32[]{:S(2)}) collective-permute-start(bf16[128,768]{1,0:T(8,128)(2,1)} %finish.3.refs_0_), channel_id=1, source_target_pairs={{0,1},{1,0},{2,3},{3,2},{4,5},{5,4},{6,7},{7,6},{8,9},{9,8},{10,11... | collective-permute-start | bytes 589832 | tf_op jit(solution)/shard_map/ppermute | solution.py:453
  87.7 6.8 %copy-start.5 = (bf16[128,768]{1,0:T(8,128)(2,1)}, bf16[128,768]{1,0:T(8,128)(2,1)S(1)}, u32[]{:S(2)}) copy-start(bf16[128,768]{1,0:T(8,128)(2,1)S(1)} %collective-permute-done.8.refs_0_) | copy-start | bytes 589828
  87.7 6.8 %collective-permute-start.9 = (bf16[128,768]{1,0:T(8,128)(2,1)S(1)}, bf16[128,768]{1,0:T(8,128)(2,1)S(1)}, u32[]{:S(2)}, u32[]{:S(2)}) collective-permute-start(bf16[128,768]{1,0:T(8,128)(2,1)S(1)} %collective-permute-done.8.refs_0_), channel_id=1, source_target_pairs={{0,1},{1,0},{2,3},{3,2},{4,5},{5,4},{6,7},{7,6},{8,9},{9,8},{10,11... | collective-permute-start | bytes 589832 | tf_op jit(solution)/shard_map/ppermute | solution.py:453
  (13 other events, 19.7 us)

commit v2 on v1

v2 whole, which is shorter than its diff:
```python
import functools

import jax
import jax.numpy as jnp
from jax import lax
from jax.experimental import pallas as pl
from jax.experimental.pallas import tpu as pltpu
from jax.sharding import PartitionSpec as P

EPS = 1e-06
TAU = 16.0
BLK = 64
F32 = jnp.float32
BF16 = jnp.bfloat16
HIGH = lax.Precision.HIGHEST


def dot(a, b, dims=((1,), (0,)), precision=None):
    return lax.dot_general(a, b, (dims, ((), ())), precision=precision, preferred_element_type=F32)


def rms(x, gain):
    return x * lax.rsqrt(jnp.mean(x * x, axis=-1, keepdims=True) + EPS) * gain


def rms_halves(x, gain):
    _, width = x.shape
    half = width // 2
    first = lax.broadcasted_iota(jnp.int32, x.shape, 1) < half
    sq = x * x
    low = jnp.sum(jnp.where(first, sq, 0.0), axis=-1, keepdims=True) / half
    high = jnp.sum(jnp.where(first, 0.0, sq), axis=-1, keepdims=True) / half
    return x * jnp.where(first, lax.rsqrt(low + EPS), lax.rsqrt(high + EPS)) * gain


def whole(shape, memory_space=pltpu.VMEM):
    return pl.BlockSpec(shape, lambda *_: (0,) * len(shape), memory_space=memory_space)


def params(mib):
    return pltpu.CompilerParams(vmem_limit_bytes=int(mib * 2**20))


def cost(us):
    return pl.CostEstimate(flops=int(us * COST_SCALE), transcendentals=0, bytes_accessed=0)


COST_SCALE = 2e8
FIRST_US = 8
FIRST_MIB = 56


def unpack_weight(w_ref, wide_ref, heads, parts, out_ref, column):
    rows = w_ref.shape[0] // (heads * parts)
    if heads * parts == 1:
        out_ref[:, column : column + 128] = w_ref[...]
        return
    wide_ref[: w_ref.shape[0], :] = w_ref[...].astype(F32)
    for head in range(heads):
        for part in range(parts):
            piece = wide_ref[pl.ds(part * heads + head, rows, stride=heads * parts), :]
            at = column + (head * parts + part) * 128
            out_ref[:, at : at + 128] = piece.astype(BF16)


class Dims:
    def __init__(self, tokens, query_attend, value_attend, key_linear, value_linear, decay_up):
        self.rows = tokens.shape[1]
        self.model = tokens.shape[2]
        self.heads = query_attend.shape[1]
        self.ca = query_attend.shape[2]
        self.va = value_attend.shape[2]
        self.ck = key_linear.shape[2]
        self.cv = value_linear.shape[2]
        self.all_heads = decay_up.shape[1]
        self.rank = decay_up.shape[0]
        self.kv = self.heads * (self.ca + self.va)
        self.rest = self.heads * (self.ca + 2 * self.ck + self.cv)
        self.steps = 4
        self.chunk = self.model // self.steps
        self.fs_size = lax.axis_size("fs")
        self.tp_size = lax.axis_size("tp")
        self.sp_size = lax.axis_size("sp")
        self.joined = self.heads * self.ca == self.cv
        self.state_at = 2 * self.rows if self.joined else 0

    def first_head(self):
        return (lax.axis_index("fs") * self.tp_size + lax.axis_index("tp")) * self.heads


class Fetch:
    def __init__(self, pairs, sems):
        self.copies = [pltpu.make_async_copy(src, dst, sems.at[i]) for i, (src, dst) in enumerate(pairs)]
        for copy in self.copies:
            copy.start()

    def wait(self, *which):
        for i in which:
            self.copies[i].wait()


HBM = pl.BlockSpec(memory_space=pltpu.HBM)


def like(x):
    return pltpu.VMEM(x.shape, x.dtype)


def call(body, us, mib, args, in_specs, outs, scratch, last_in_hbm=False):
    many = isinstance(outs, list)
    specs = [whole(o.shape) for o in outs] if many else whole(outs.shape)
    if last_in_hbm:
        specs[-1] = HBM
    return pl.pallas_call(
        body,
        in_specs=in_specs,
        out_specs=specs,
        out_shape=outs,
        scratch_shapes=scratch,
        compiler_params=params(mib),
        cost_estimate=cost(us),
    )(*args)


def write_kv(acc, key_gain, dims, outs):
    first = dims.first_head()
    rows, width = dims.rows, dims.heads * dims.ca
    for h in range(dims.heads):
        k = acc[:, h * dims.ca : (h + 1) * dims.ca].astype(BF16).astype(F32)
        row = 2 * (first + h)
        gain = jnp.concatenate([key_gain[pl.ds(row, 1), :], key_gain[pl.ds(row + 1, 1), :]], axis=1)
        k = rms_halves(k, gain).astype(BF16)
        for out in outs:
            out[:rows, h * dims.ca : (h + 1) * dims.ca] = k
    v = acc[:, width : width + dims.heads * dims.va].astype(BF16)
    for out in outs:
        out[rows : 2 * rows, :] = v


def chunks_of(raw_refs, dst_refs, steps):
    pairs = []
    for c in range(steps):
        for src, dst in zip(raw_refs, dst_refs):
            n = src.shape[0] // steps
            pairs.append((src.at[pl.ds(c * n, n), :], dst.at[pl.ds(c * n, n), :]))
    return pairs


def projected(normed_ref, raws, layout, dims, w_out, wide, fetch, first_copy, keep=None):
    acc = None
    for c in range(dims.steps):
        here = slice(c * dims.chunk, (c + 1) * dims.chunk)
        column = 0
        for i, (raw, parts) in enumerate(zip(raws, layout)):
            fetch.wait(first_copy + c * len(raws) + i)
            n = raw.shape[0] // dims.steps
            unpack_weight(
                raw.at[c * n : (c + 1) * n, :], wide.at[i % 2], dims.heads, parts, w_out.at[here, :], column
            )
            column += dims.heads * parts * 128
        if keep is not None:
            keep(here)
        part = dot(normed_ref[:, here], w_out[here, :])
        acc = part if acc is None else acc + part
    return acc


def slot_outputs(dims):
    hd, rows = dims.heads, dims.rows
    return [
        jax.ShapeDtypeStruct((rows, hd * dims.ca), BF16),
        jax.ShapeDtypeStruct((rows, hd * dims.ck), BF16),
        jax.ShapeDtypeStruct((rows, hd * dims.cv), F32),
        jax.ShapeDtypeStruct((2 * rows, hd * dims.ca), BF16),
        jax.ShapeDtypeStruct((dims.state_at + hd * dims.ck + 16, dims.cv), BF16),
        jax.ShapeDtypeStruct((hd * dims.ck, dims.cv), F32),
        jax.ShapeDtypeStruct((hd * dims.ck, dims.cv), F32),
        jax.ShapeDtypeStruct((hd * dims.ck, dims.cv), F32),
    ]


def slot_sequence(dims, slot):
    return lax.rem(lax.axis_index("fs") + dims.fs_size - slot, dims.fs_size)


def columns_of(row, width):
    return dot(row, jnp.ones((1, width), row.dtype), ((0,), (0,)), precision=HIGH if row.dtype == F32 else None)


def local_part(dims, slot, acc, base, low_rank, init, up, up_wide, bias, retain, query_gain, outs):
    q_out, reach_out, inside_out, _, send_out, state_out, decay_out, begin_out = outs
    state_at = dims.state_at
    hd, rows, ck, cv = dims.heads, dims.rows, dims.ck, dims.cv
    gain = jnp.concatenate([query_gain[...], query_gain[...]], axis=1)
    up_wide[...] = up[...].astype(F32)
    retain_columns = jnp.transpose(retain[...])
    head_lane = lax.broadcasted_iota(jnp.int32, retain_columns.shape, 1)
    row_id = lax.broadcasted_iota(jnp.int32, (rows, rows), 0)
    col_id = lax.broadcasted_iota(jnp.int32, (rows, rows), 1)
    same_block = row_id // BLK == col_id // BLK
    lower = row_id >= col_id
    summing = jnp.where(same_block & lower, 1.0, 0.0).astype(BF16)
    blocks = rows // BLK
    first = lax.axis_index("sp") == 0
    head0 = dims.first_head()
    sequence = slot_sequence(dims, slot)
    send_out[state_at + hd * ck :, :] = jnp.zeros((16, cv), BF16)
    for h in range(hd):
        q = acc[:, base + h * dims.ca : base + (h + 1) * dims.ca].astype(BF16).astype(F32)
        q_out[:, h * dims.ca : (h + 1) * dims.ca] = rms_halves(q, gain).astype(BF16)
    logs = []
    for h in range(hd):
        head = head0 + h
        up_head = up_wide[pl.ds(head, dims.rank, stride=dims.all_heads), :].astype(BF16)
        pre = dot(low_rank, up_head) + bias[pl.ds(head, 1), :]
        gate = jnp.minimum(pre, 0.0) - jnp.log1p(jnp.exp(-jnp.abs(pre)))
        kept = jnp.sum(jnp.where(head_lane == head, retain_columns, 0.0), axis=1, keepdims=True)
        logs.append(gate / TAU + kept)
    log_decay = jnp.concatenate(logs, axis=1)
    running = jnp.zeros_like(log_decay)
    left = log_decay
    for _ in range(3):
        term = left.astype(BF16)
        running = running + dot(summing, term)
        left = left - term.astype(F32)
    finals = [running[(b + 1) * BLK - 1 : (b + 1) * BLK, :] for b in range(blocks)]
    pivots = [running[b * BLK + BLK // 2 : b * BLK + BLK // 2 + 1, :] for b in range(blocks)]
    at = base + hd * dims.ca
    queries = acc[:, at : at + hd * ck].astype(BF16).astype(F32) * ck ** (-0.5)
    keys = acc[:, at + hd * ck : at + 2 * hd * ck].astype(BF16).astype(F32)
    q_edge, q_piv, k_piv, k_end, reach, faded = [], [], [], [], [], [None] * blocks
    before = jnp.zeros_like(finals[0])
    for b in range(blocks):
        here = slice(b * BLK, (b + 1) * BLK)
        run, q, k = running[here], queries[here], keys[here]
        q_edge.append(q * jnp.exp(run))
        q_piv.append((q * jnp.exp(run - pivots[b])).astype(BF16))
        k_piv.append((k * jnp.exp(pivots[b] - run)).astype(BF16))
        k_end.append(k * jnp.exp(finals[b] - run))
        reach.append((q_edge[b] * jnp.exp(before)).astype(BF16))
        reach_out[here, :] = reach[b]
        before = before + finals[b]
    later = jnp.zeros_like(finals[0])
    for b in range(blocks - 1, -1, -1):
        faded[b] = (k_end[b] * jnp.exp(later)).astype(BF16)
        later = later + finals[b]
    faded_rows = jnp.concatenate(faded, axis=0)
    decay = jnp.exp(before)
    for h in range(hd):
        of = slice(h * ck, (h + 1) * ck)
        at = base + hd * (dims.ca + 2 * ck) + h * cv
        vl = acc[:, at : at + cv].astype(BF16)
        for b in range(blocks):
            here = slice(b * BLK, (b + 1) * BLK)
            own = dot(q_piv[b][:, of], k_piv[b][:, of], ((1,), (1,)))
            own = jnp.where(lower[:BLK, :BLK], own, 0.0).astype(BF16)
            result = dot(own, vl[here])
            gap = jnp.zeros_like(finals[0][:, of])
            for c in range(b - 1, -1, -1):
                edge = (k_end[c][:, of] * jnp.exp(gap)).astype(BF16)
                across = dot(q_edge[b][:, of].astype(BF16), edge, ((1,), (1,)))
                result = result + dot(across.astype(BF16), vl[c * BLK : (c + 1) * BLK])
                gap = gap + finals[c][:, of]
            inside_out[here, h * cv : (h + 1) * cv] = result
        state = dot(faded_rows[:, of], vl, ((0,), (0,)))
        columns = columns_of(decay[:, of], cv)
        begin = init[pl.ds((sequence * hd + h) * ck, ck), :]
        begin = jnp.where(first, begin, 0.0)
        begin_out[of, :] = begin
        state = state + columns * begin
        state_out[of, :] = state
        decay_out[of, :] = columns
        send_out[state_at + h * ck : state_at + (h + 1) * ck, :] = state.astype(BF16)
        at = state_at + hd * ck + h
        send_out[at : at + 1, :ck] = decay[:, of].astype(BF16)


def slot_first(dims, tokens, gain, key_gain, weights, consts):
    parts = [dims.ca, dims.va, dims.ca, dims.ck, dims.ck, dims.cv]
    layout = [p // 128 for p in parts]
    n_const, n_out, n_w = len(consts), len(slot_outputs(dims)), len(weights)
    widest = max(w.shape[0] for w in weights) // dims.steps
    base = dims.kv

    def body(*refs):
        inputs, refs = refs[: 3 + n_w + n_const], refs[3 + n_w + n_const :]
        outs, packed, refs = refs[:n_out], refs[n_out], refs[n_out + 1 :]
        local, (normed, acc, w_out, wide, up_wide, sems, out_sems) = refs[: len(inputs)], refs[len(inputs) :]
        tok, gain_v, kg = local[:3]
        raws_v, consts_v = local[3 : 3 + n_w], local[3 + n_w :]
        pairs = list(zip(inputs[:2], local[:2])) + chunks_of(inputs[3 : 3 + n_w], raws_v, dims.steps)
        small = list(zip(inputs[2:3], local[2:3])) + list(zip(inputs[3 + n_w :], consts_v))
        fetch = Fetch(pairs + small, sems)
        fetch.wait(0, 1)
        normed[...] = rms(tok[...].astype(F32), gain_v[...]).astype(BF16)
        kept = []

        def keep(here):
            kept.append(pltpu.make_async_copy(w_out.at[here, :], packed.at[here, :], out_sems.at[len(kept)]))
            kept[-1].start()

        acc[...] = projected(normed, raws_v, layout, dims, w_out, wide, fetch, 2, keep)
        fetch.wait(*range(len(pairs), len(pairs) + len(small)))
        write_kv(acc, kg, dims, (outs[3], outs[4]) if dims.joined else (outs[3],))
        down, init, up, bias, retain, query_gain = consts_v
        low = dot(normed[...], down[...], ((1,), (1,))).astype(BF16)
        local_part(dims, 0, acc, base, low, init, up, up_wide, bias, retain, query_gain, outs)
        for copy in kept:
            copy.wait()

    args = (tokens, gain, key_gain, *weights, *consts)
    return call(
        body,
        FIRST_US,
        FIRST_MIB,
        args,
        [HBM] * len(args),
        slot_outputs(dims) + [jax.ShapeDtypeStruct((dims.model, dims.kv + dims.rest), BF16)],
        [like(a) for a in args]
        + [
            pltpu.VMEM(tokens.shape, BF16),
            pltpu.VMEM((dims.rows, dims.kv + dims.rest), F32),
            pltpu.VMEM((dims.model, dims.kv + dims.rest), BF16),
            pltpu.VMEM((2, widest, 128), F32),
            pltpu.VMEM(consts[2].shape, F32),
            pltpu.SemaphoreType.DMA((3 + n_w * dims.steps + n_const,)),
            pltpu.SemaphoreType.DMA((dims.steps,)),
        ],
        last_in_hbm=True,
    )


def slot_other(dims, slot, tokens, gain, key_gain, weights, consts):
    n_const, n_out = len(consts), len(slot_outputs(dims))
    base = dims.kv

    def body(tok, w_ref, *refs):
        small, refs = refs[: 2 + n_const], refs[2 + n_const :]
        outs, refs = refs[:n_out], refs[n_out:]
        local, (normed, acc, up_wide, sems) = refs[: 2 + n_const], refs[2 + n_const :]
        fetch = Fetch(list(zip(small, local)), sems)
        gain_v, kg = local[:2]
        fetch.wait(0)
        normed[...] = rms(tok[...].astype(F32), gain_v[...]).astype(BF16)
        acc[...] = dot(normed[...], w_ref[...])
        fetch.wait(*range(1, 2 + n_const))
        write_kv(acc, kg, dims, (outs[3], outs[4]) if dims.joined else (outs[3],))
        down, init, up, bias, retain, query_gain = local[2:]
        low = dot(normed[...], down[...], ((1,), (1,))).astype(BF16)
        local_part(dims, slot, acc, base, low, init, up, up_wide, bias, retain, query_gain, outs)

    args = (tokens, weights, gain, key_gain, *consts)
    return call(
        body,
        4,
        16,
        args,
        [whole(tokens.shape), whole(weights.shape)] + [HBM] * (2 + n_const),
        slot_outputs(dims),
        [like(a) for a in args[2:]]
        + [
            pltpu.VMEM(tokens.shape, BF16),
            pltpu.VMEM((dims.rows, dims.kv + dims.rest), F32),
            pltpu.VMEM(consts[2].shape, F32),
            pltpu.SemaphoreType.DMA((2 + n_const,)),
        ],
    )


def combine(dims, bit, state, decay, prefix, prefix_decay, received, base):
    hd, ck, cv = dims.heads, dims.ck, dims.cv
    begun = prefix_decay is not None

    def body(*refs):
        if begun:
            st, dec, pre, pre_dec, rec, send_out, st_out, dec_out, pre_out, pre_dec_out = refs
        else:
            st, dec, pre, rec, send_out, st_out, dec_out, pre_out, pre_dec_out = refs
        upper = lax.rem(lax.axis_index("sp") // bit, 2) == 1
        send_out[hd * ck :, :] = jnp.zeros((16, cv), BF16)
        for h in range(hd):
            at = slice(h * ck, (h + 1) * ck)
            other = rec[base + h * ck : base + (h + 1) * ck, :].astype(F32)
            other_row = rec[base + hd * ck + h : base + hd * ck + h + 1, :ck]
            other_dec = columns_of(other_row, cv)
            mine, mine_dec = st[at, :], dec[at, :]
            earlier = jnp.where(upper, other, mine)
            late = jnp.where(upper, mine, other)
            total = earlier * jnp.where(upper, mine_dec, other_dec) + late
            st_out[at, :] = total
            send_out[at, :] = total.astype(BF16)
            both = mine_dec * other_dec
            dec_out[at, :] = both
            if bit * 4 < dims.sp_size:
                send_out[hd * ck + h : hd * ck + h + 1, :ck] = jnp.transpose(both[:, :128])[:1, :].astype(BF16)
            if begun:
                pre_out[at, :] = pre[at, :] + jnp.where(upper, pre_dec[at, :] * other, 0.0)
                pre_dec_out[at, :] = jnp.where(upper, pre_dec[at, :] * other_dec, pre_dec[at, :])
            else:
                pre_out[at, :] = jnp.where(upper, other, pre[at, :])
                pre_dec_out[at, :] = jnp.where(upper, other_dec, 1.0)

    full = jax.ShapeDtypeStruct((hd * ck, cv), F32)
    args = (state, decay, prefix) + ((prefix_decay,) if begun else ()) + (received,)
    return call(
        body,
        2,
        6,
        args,
        [whole(a.shape) for a in args],
        [jax.ShapeDtypeStruct((hd * ck + 16, cv), BF16), full, full, full, full],
        [],
    )


def finish(dims, bit, kv_blocks, q_unit, reach, inside, prefix, prefix_decay, received, gains):
    hd, rows, ca, va, ck, cv = dims.heads, dims.rows, dims.ca, dims.va, dims.ck, dims.cv
    count = len(kv_blocks)
    scale = (ca // 2) ** (-0.5)

    def body(*refs):
        kvs = refs[:count]
        q_ref, reach_ref, inside_ref, pre, pre_dec, rec = refs[count : count + 6]
        gains_h, out, gains_v, sems = refs[count + 6 : count + 9], refs[count + 9], refs[count + 10 : -1], refs[-1]
        fetch = Fetch(list(zip(gains_h, gains_v)), sems)
        mix_ref, sg_ref, lam_ref = gains_v
        place = lax.axis_index("sp")
        head0 = dims.first_head()
        lane = lax.broadcasted_iota(jnp.int32, (rows, ca), 1)
        row_id = lax.rem(lax.broadcasted_iota(jnp.int32, (2 * rows, rows), 0), rows)
        col_id = lax.broadcasted_iota(jnp.int32, (2 * rows, rows), 1)
        allowed = row_id // BLK >= col_id // BLK
        upper = lax.rem(place // bit, 2) == 1
        raws, ratios = [], []
        for h in range(hd):
            at = slice(h * ck, (h + 1) * ck)
            enter = pre[at, :] + jnp.where(upper, pre_dec[at, :] * rec[at, :].astype(F32), 0.0)
            raws.append(inside_ref[:, h * cv : (h + 1) * cv] + dot(reach_ref[:, at], enter.astype(BF16)))
        for h in range(hd):
            q = q_ref[:, h * ca : (h + 1) * ca]
            zero = jnp.zeros_like(q)
            pair = jnp.concatenate([jnp.where(lane < ca // 2, q, zero), jnp.where(lane < ca // 2, zero, q)], axis=0)
            scores = []
            for m in range(count):
                s = dot(pair, kvs[m][:rows, h * ca : (h + 1) * ca], ((1,), (1,))) * scale
                if m == 0:
                    s = jnp.where(allowed, s, -jnp.inf)
                else:
                    s = jnp.where(jnp.bitwise_xor(place, m) < place, s, -jnp.inf)
                scores.append(s)
            top = jnp.max(functools.reduce(jnp.maximum, scores), axis=1, keepdims=True)
            total = jnp.zeros((2 * rows, rows), F32)
            sums = jnp.zeros((2 * rows, va), F32)
            for m in range(count):
                raised = jnp.exp(scores[m] - top)
                total = total + raised
                sums = sums + dot(raised.astype(BF16), kvs[m][rows : 2 * rows, h * va : (h + 1) * va])
            ratios.append(sums / jnp.sum(total, axis=1, keepdims=True))
        fetch.wait(0, 1, 2)
        lam_lane = lax.broadcasted_iota(jnp.int32, lam_ref.shape, 1)
        for h in range(hd):
            lam = jnp.sum(jnp.where(lam_lane == head0 + h, lam_ref[...], 0.0), axis=1, keepdims=True)
            diff = ratios[h][:rows] - lam * ratios[h][rows:]
            out[:, h * va : (h + 1) * va] = rms(diff, mix_ref[...]).astype(BF16)
            at = hd * va + h * cv
            out[:, at : at + cv] = rms(raws[h], sg_ref[...]).astype(BF16)

    args = (*kv_blocks, q_unit, reach, inside, prefix, prefix_decay, received)
    return call(
        body,
        3,
        10,
        args + gains,
        [whole(a.shape) for a in args] + [HBM] * 3,
        jax.ShapeDtypeStruct((rows, hd * (va + cv)), BF16),
        [like(g) for g in gains] + [pltpu.SemaphoreType.DMA((3,))],
    )


def project_out(dims, pieces, places, weights, start):
    wa, wl = weights
    rows, cols = dims.rows, wa.shape[1]
    step_a, step_l = dims.heads * dims.va, dims.heads * dims.cv
    count = len(pieces)
    last = start is not None

    def body(*refs):
        parts, (wa_h, wl_h), refs = refs[:count], refs[count : count + 2], refs[count + 2 :]
        begin = refs[0] if last else None
        out, a_v, l_v, sems = refs[1:] if last else refs
        pairs, fs, tp = [], lax.axis_index("fs"), lax.axis_index("tp")
        for i, (j, step) in enumerate(places):
            owner = lax.rem(fs + j, dims.fs_size) * dims.tp_size + lax.rem(tp + step, dims.tp_size)
            pairs.append((wa_h.at[pl.ds(pl.multiple_of(owner * step_a, step_a), step_a), :], a_v.at[i]))
            pairs.append((wl_h.at[pl.ds(pl.multiple_of(owner * step_l, step_l), step_l), :], l_v.at[i]))
        fetch = Fetch(pairs, sems)
        total = begin[...] if last else jnp.zeros((rows, cols), F32)
        for i in range(count):
            fetch.wait(2 * i)
            total = total + dot(parts[i][:, :step_a], a_v[i])
            fetch.wait(2 * i + 1)
            total = total + dot(parts[i][:, step_a:], l_v[i])
        out[...] = total.astype(out.dtype)

    starts = [start] if last else []
    return call(
        body,
        3,
        20,
        (*pieces, wa, wl, *starts),
        [whole(p.shape) for p in pieces] + [HBM] * 2 + [whole(s.shape) for s in starts],
        jax.ShapeDtypeStruct((rows, cols), BF16 if last else F32),
        [
            pltpu.VMEM((count, step_a, cols), BF16),
            pltpu.VMEM((count, step_l, cols), BF16),
            pltpu.SemaphoreType.DMA((2 * count,)),
        ],
    )


def swap(x, axis, bit, size):
    return lax.ppermute(x, axis, [(i, i ^ bit) for i in range(size)])


def shift(x, axis, by, size):
    return lax.ppermute(x, axis, [(i, (i + by) % size) for i in range(size)])


def low_bit(m):
    return m & -m


def body(
    tokens,
    norm_gain,
    query_attend,
    key_attend,
    value_attend,
    query_linear,
    key_linear,
    value_linear,
    decay_down,
    decay_up,
    decay_bias,
    log_retain,
    query_gain,
    key_gain,
    diff_lambda,
    mix_gain,
    state_gain,
    init_state,
    output_attend,
    output_linear,
):
    fs_size, tp_size, sp_size = (lax.axis_size(a) for a in ("fs", "tp", "sp"))
    dims = Dims(tokens, query_attend, value_attend, key_linear, value_linear, decay_up)
    rows = dims.rows

    def flat(w):
        d, h, c = w.shape
        parts = c // 128
        return w.reshape(d, h, parts, 128).transpose(0, 2, 1, 3).reshape(d * parts * h, 128)

    own = tokens[0]
    retain_own = log_retain[0].T
    gain = norm_gain.reshape(1, -1)
    kg = key_gain.reshape(-1, key_gain.shape[-1])
    up = decay_up.reshape(-1, decay_up.shape[-1])
    init = init_state.reshape(-1, dims.cv)
    token_slots = [own] + [shift(own, "fs", j, fs_size) for j in range(1, fs_size)]
    retains = [retain_own] + [shift(retain_own, "fs", j, fs_size) for j in range(1, fs_size)]

    def exchange(kv, send, state, decay, prefix):
        near = swap(send, "sp", 1, sp_size)
        blocks = [kv, near if dims.joined else swap(kv, "sp", 1, sp_size)]
        for m in range(2, sp_size):
            source = blocks[m - low_bit(m)]
            blocks.append(swap(source, "sp", low_bit(m), sp_size))
        prefix_decay = None
        received, base, bit = near, dims.state_at, 1
        while bit * 2 < sp_size:
            send, state, decay, prefix, prefix_decay = combine(
                dims, bit, state, decay, prefix, prefix_decay, received, base
            )
            bit, base = bit * 2, 0
            received = swap(send, "sp", bit, sp_size)
        return blocks, (bit, prefix, prefix_decay, received)

    all_weights = (key_attend, value_attend, query_attend, query_linear, key_linear, value_linear)
    results = []
    packed = None
    for j in range(fs_size):
        consts = (decay_down.T, init, up, decay_bias, retains[j], query_gain.reshape(1, -1))
        if j == 0:
            *outs, packed = slot_first(dims, own, gain, kg, [flat(w) for w in all_weights], consts)
        else:
            outs = slot_other(dims, j, token_slots[j], gain, kg, packed, consts)
        results.append((outs, exchange(*outs[3:])))

    gains = (mix_gain.reshape(1, -1), state_gain.reshape(1, -1), diff_lambda.reshape(1, -1))
    weights = (output_attend, output_linear)
    total = None
    pieces, places = [], []
    for j in range(fs_size):
        outs, (blocks, (bit, prefix, prefix_decay, received)) = results[j]
        mixed = finish(dims, bit, blocks, *outs[:3], prefix, prefix_decay, received, gains)
        if j:
            mixed = shift(mixed, "fs", -j, fs_size)
        arrived = [mixed] + [shift(mixed, "tp", -i, tp_size) for i in range(1, tp_size)]
        if j == 0 and fs_size > 1:
            total = project_out(dims, arrived, [(0, i) for i in range(tp_size)], weights, None)
        else:
            pieces += arrived
            places += [(j, i) for i in range(tp_size)]
    result = project_out(dims, pieces, places, weights, total)
    return result.reshape(1, rows, -1)


def solution(mesh):
    heads = P(None, ("fs", "tp"), None)
    positions = P(("grp", "fs"), "sp", None)
    in_specs = (
        positions,
        P(),
        heads,
        heads,
        heads,
        heads,
        heads,
        heads,
        P(),
        P(),
        P(),
        positions,
        P(),
        P(),
        P(),
        P(),
        P(),
        P("grp", ("fs", "tp"), None, None),
        P(None, "tp"),
        P(None, "tp"),
    )
    out_specs = P(("grp", "fs"), "sp", "tp")

    return jax.shard_map(body, mesh=mesh, in_specs=in_specs, out_specs=out_specs, check_vma=False)
```

time: 100 us -> 60.4 us (0.60)
  Pallas kernels: 44.1 us -> 18.6 us
  local copies, waits for them, and re-layouts: 8.28 us -> 3.17 us
  waiting for transfers between devices: 23.6 us -> 20.5 us
  starting transfers between devices: 20.8 us -> 17.8 us
  other arithmetic: 2.66 us -> 0 us
    pallas_call x10 -> x8, Pallas kernels: 44.1 us -> 18.6 us  [call(): pl.pallas_call(body, in_specs=in_specs, out_specs=specs, out_shape=outs,...]
    dynamic_slice x2 -> x0, local copies, waits for them, and re-layouts: 2.88 us -> none  [the longest x1 1.91 us: consts(): lax.dynamic_index_in_dim(init_state, seq, 0, False)]
    ppermute x10 -> x8, starting transfers between devices: 14.9 us -> 12.7 us  [swap(): return lax.ppermute(x, axis, [(i, i ^ bit) for i in range(size)])]
    ppermute x6 -> x5, waiting for transfers between devices: 6.78 us -> 4.92 us  [shift(): return lax.ppermute(x, axis, [(i, (i + by) % size) for i in range(size)])]
    unnamed x42, local copies, waits for them, and re-layouts: 4.77 us -> 3.17 us
    select_n x2 -> x0, other arithmetic: 1.44 us -> none  [prefix_of(): prefix = jnp.where(sp == 0, begin, 0.0)]
    ppermute x10 -> x8, waiting for transfers between devices: 16.8 us -> 15.5 us  [swap(): return lax.ppermute(x, axis, [(i, i ^ bit) for i in range(size)])]
    another operation x2 -> x0, other arithmetic: 1.23 us -> none  [the longest x1 0.67 us: body(): jnp.stack(late_owners)]
  transfers between devices with their start and end apart: 16 -> 13, of which waited for: 7 -> 6; matrix products, arithmetic and copies ran while one was open for 5% -> 0% of each run, Pallas kernels for 40% -> 22%
where the time goes in v2:
time: 60.4 us; the launch traced here: 60.3 us
  waiting for transfers between devices  20.5 us (34%)
  Pallas kernels  18.6 us (31%)
  starting transfers between devices  17.8 us (29%)
  local copies, waits for them, and re-layouts  3.17 us (5%)
    pallas_call x8, Pallas kernels, call(): pl.pallas_call(body, in_specs=in_specs, out_specs=specs, out_shape=outs,...  18.6 us
    ppermute x8, waiting for transfers between devices, swap(): return lax.ppermute(x, axis, [(i, i ^ bit) for i in range(size)])  15.5 us
    ppermute x8, starting transfers between devices, swap(): return lax.ppermute(x, axis, [(i, i ^ bit) for i in range(size)])  12.7 us
    ppermute x5, starting transfers between devices, shift(): return lax.ppermute(x, axis, [(i, (i + by) % size) for i in range(size)])  5.1 us
    ppermute x5, waiting for transfers between devices, shift(): return lax.ppermute(x, axis, [(i, (i + by) % size) for i in range(size)])  4.92 us
    unnamed x42, local copies, waits for them, and re-layouts  3.17 us
  transfers between devices with their start and end apart: 13, of which 6 were waited for; matrix products, arithmetic and copies ran while one was open for 0% of the time, Pallas kernels for 22%

profile of v2, /device:TPU:0, one launch (start us, length us, event | category | flops | bytes accessed | tf_op | source)
XLA Modules:
  0.0 60.3 jit_solution(2977378215890637279)
XLA Ops:
  0.0 3.0 %collective-permute-start = (bf16[128,2048]{1,0:T(8,128)(2,1)}, bf16[128,2048]{1,0:T(8,128)(2,1)S(1)}, u32[]{:S(2)}, u32[]{:S(2)}) collective-permute-start(bf16[128,2048]{1,0:T(8,128)(2,1)} %bitcast.48), channel_id=1, source_target_pairs={{0,2},{2,0},{1,3},{3,1},{4,6},{6,4},{5,7},{7,5},{8,10},{10,8},{9,1... | collective-permute-start | bytes 1572872 | tf_op jit(solution)/shard_map/ppermute | solution.py:526
  3.0 8.2 %shard_map.190 = (bf16[128,256]{1,0:T(8,128)(2,1)}, bf16[128,256]{1,0:T(8,128)(2,1)}, f32[128,512]{1,0:T(8,128)}, bf16[256,256]{1,0:T(8,128)(2,1)}, bf16[528,256...) custom-call(bf16[128,2048]{1,0:T(8,128)(2,1)} %bitcast.49, ...), custom_call_target="tpu_custom_call" | custom-call | flops 1600000000 | tf_op jit(solution)/shard_map/pallas_call | solution.py:114
  11.2 4.0 %collective-permute-done.1.refs_6_ = f32[8,128]{1,0:T(8,128)S(1)} collective-permute-done((f32[8,128]{1,0:T(8,128)}, f32[8,128]{1,0:T(8,128)S(1)}, u32[]{:S(2)}, u32[]{:S(2)}) %collective-permute-start.1) | collective-permute-done | bytes 4128 | tf_op jit(solution)/shard_map/ppermute | solution.py:526
  15.3 3.1 %copy-done.2 = bf16[2048,1792]{1,0:T(8,128)(2,1)S(1)} copy-done((bf16[2048,1792]{1,0:T(8,128)(2,1)S(1)}, bf16[2048,1792]{1,0:T(8,128)(2,1)}, u32[]{:S(2)}) %copy-start.2) | copy-done | bytes 7340056
  18.4 3.4 %shard_map.191 = (bf16[128,256]{1,0:T(8,128)(2,1)S(1)}, bf16[128,256]{1,0:T(8,128)(2,1)S(1)}, f32[128,512]{1,0:T(8,128)S(1)}, bf16[256,256]{1,0:T(8,128)(2,1)S(1...) custom-call(bf16[128,2048]{1,0:T(8,128)(2,1)S(1)} %collective-permut, ...), custom_call_target="tpu_custom_call" | custom-call | flops 800000000 | tf_op jit(solution)/shard_map/pallas_call | solution.py:114
  21.9 1.9 %collective-permute-start.2 = (bf16[528,256]{1,0:T(8,128)(2,1)S(1)}, bf16[528,256]{1,0:T(8,128)(2,1)S(1)}, u32[]{:S(2)}, u32[]{:S(2)}) collective-permute-start(bf16[528,256]{1,0:T(8,128)(2,1)S(1)} %get-tuple-element.30), channel_id=1, source_target_pairs={{0,4},{4,0},{8,12},{12,8},{1,5},{5,1},{9,13},{13,9},{2,6},{6,2},{1... | collective-permute-start | bytes 811016 | tf_op jit(solution)/shard_map/ppermute | solution.py:522
  23.8 0.2 collective-permute-start.8
  24.0 2.8 %collective-permute-start.3 = (bf16[256,256]{1,0:T(8,128)(2,1)S(1)}, bf16[256,256]{1,0:T(8,128)(2,1)S(1)}, u32[]{:S(2)}, u32[]{:S(2)}) collective-permute-start(bf16[256,256]{1,0:T(8,128)(2,1)S(1)} %get-tuple-element.29.refs_0_), channel_id=1, source_target_pairs={{0,8},{4,12},{8,0},{12,4},{1,9},{5,13},{9,1},{13,5},{2,10},{6,14},... | collective-permute-start | bytes 393224 | tf_op jit(solution)/shard_map/ppermute | solution.py:522
  26.9 10.0 %collective-permute-done.2.refs_3_.refs_1_ = bf16[528,256]{1,0:T(8,128)(2,1)S(1)} collective-permute-done((bf16[528,256]{1,0:T(8,128)(2,1)S(1)}, bf16[528,256]{1,0:T(8,128)(2,1)S(1)}, u32[]{:S(2)}, u32[]{:S(2)}) %collective-permute-start.2) | collective-permute-done | bytes 270368 | tf_op jit(solution)/shard_map/ppermute | solution.py:522
  36.9 1.0 %shard_map.192 = (bf16[272,256]{1,0:T(8,128)(2,1)S(1)}, f32[256,256]{1,0:T(8,128)}, f32[256,256]{1,0:T(8,128)}, f32[256,256]{1,0:T(8,128)S(1)}, f32[256,256]{1,0:T(8,128)S(1)}) custom-call(f32[256,256]{1,0:T(8,128)S(1)} %get-tuple-element.34.refs_0_, f32[256,256]{1,0:T(8,128)S(1)} %get-tuple-element.35.refs_1_, f32[256,256]{1,0:T(8,128)S(1)} %get-tuple-element.36.refs_2_, ...), custom_call_target="tpu_custom_call" | custom-call | flops 400000000 | tf_op jit(solution)/shard_map/pallas_call | solution.py:114
  37.9 1.9 %collective-permute-start.5 = (bf16[272,256]{1,0:T(8,128)(2,1)S(1)}, bf16[272,256]{1,0:T(8,128)(2,1)S(1)}, u32[]{:S(2)}, u32[]{:S(2)}) collective-permute-start(bf16[272,256]{1,0:T(8,128)(2,1)S(1)} %get-tuple-element.39), channel_id=1, source_target_pairs={{0,8},{4,12},{8,0},{12,4},{1,9},{5,13},{9,1},{13,5},{2,10},{6,14},... | collective-permute-start | bytes 417800 | tf_op jit(solution)/shard_map/ppermute | solution.py:522
  39.9 3.0 %collective-permute-start.4 = (bf16[256,256]{1,0:T(8,128)(2,1)S(1)}, bf16[256,256]{1,0:T(8,128)(2,1)S(1)}, u32[]{:S(2)}, u32[]{:S(2)}) collective-permute-start(bf16[256,256]{1,0:T(8,128)(2,1)S(1)} %collective-permute-done.3.refs_2_), channel_id=1, source_target_pairs={{0,4},{4,0},{8,12},{12,8},{1,5},{5,1},{9,13},{13,9},{2,6},{6,2},{1... | collective-permute-start | bytes 393224 | tf_op jit(solution)/shard_map/ppermute | solution.py:522
  42.8 2.8 %collective-permute-start.10 = (bf16[256,256]{1,0:T(8,128)(2,1)S(1)}, bf16[256,256]{1,0:T(8,128)(2,1)S(1)}, u32[]{:S(2)}, u32[]{:S(2)}) collective-permute-start(bf16[256,256]{1,0:T(8,128)(2,1)S(1)} %collective-permute-done.9.refs_2_), channel_id=1, source_target_pairs={{0,4},{4,0},{8,12},{12,8},{1,5},{5,1},{9,13},{13,9},{2,6},{6,2},{1... | collective-permute-start | bytes 393224 | tf_op jit(solution)/shard_map/ppermute | solution.py:522
  45.6 1.0 %shard_map.194 = (bf16[272,256]{1,0:T(8,128)(2,1)S(1)}, f32[256,256]{1,0:T(8,128)}, f32[256,256]{1,0:T(8,128)}, f32[256,256]{1,0:T(8,128)S(1)}, f32[256,256]{1,0:T(8,128)S(1)}) custom-call(f32[256,256]{1,0:T(8,128)S(1)} %copy-done.11, f32[256,256]{1,0:T(8,128)S(1)} %copy-done.12, f32[256,256]{1,0:T(8,128)S(1)} %copy-done.13, ...), custom_call_target="tpu_custom_call" | custom-call | flops 400000000 | tf_op jit(solution)/shard_map/pallas_call | solution.py:114
  46.6 1.2 %collective-permute-done.4.refs_3_ = bf16[256,256]{1,0:T(8,128)(2,1)S(1)} collective-permute-done((bf16[256,256]{1,0:T(8,128)(2,1)S(1)}, bf16[256,256]{1,0:T(8,128)(2,1)S(1)}, u32[]{:S(2)}, u32[]{:S(2)}) %collective-permute-start.4) | collective-permute-done | bytes 131104 | tf_op jit(solution)/shard_map/ppermute | solution.py:522
  47.9 1.3 %collective-permute-done.5.refs_9_ = bf16[272,256]{1,0:T(8,128)(2,1)S(1)} collective-permute-done((bf16[272,256]{1,0:T(8,128)(2,1)S(1)}, bf16[272,256]{1,0:T(8,128)(2,1)S(1)}, u32[]{:S(2)}, u32[]{:S(2)}) %collective-permute-start.5) | collective-permute-done | bytes 139296 | tf_op jit(solution)/shard_map/ppermute | solution.py:522
  49.2 1.1 %shard_map.193 = bf16[128,768]{1,0:T(8,128)(2,1)S(1)} custom-call(bf16[256,256]{1,0:T(8,128)(2,1)S(1)} %get-tuple-element.29.refs_0_, bf16[528,256]{1,0:T(8,128)(2,1)S(1)} %collective-permute-done.2.refs_3_.refs_1_, bf16[256,256]{1,0:T(8,128)(2,1)S(1)} %collective-permute-done.3.refs_2_, bf16[256,256]{1,0:T(8,128)(2,1)S(1)} %collective-permute-done.4.refs_3_, ...), custom_call_target="tpu_custom_call" | custom-call | flops 600000000 | tf_op jit(solution)/shard_map/pallas_call | solution.py:114
  50.3 1.5 %collective-permute-start.6 = (bf16[128,768]{1,0:T(8,128)(2,1)S(1)}, bf16[128,768]{1,0:T(8,128)(2,1)S(1)}, u32[]{:S(2)}, u32[]{:S(2)}) collective-permute-start(bf16[128,768]{1,0:T(8,128)(2,1)S(1)} %shard_map.193), channel_id=1, source_target_pairs={{0,2},{2,0},{1,3},{3,1},{4,6},{6,4},{5,7},{7,5},{8,10},{10,8},{9,1... | collective-permute-start | bytes 589832 | tf_op jit(solution)/shard_map/ppermute | solution.py:526
  51.9 3.0 %collective-permute-done.11.refs_9_ = bf16[272,256]{1,0:T(8,128)(2,1)S(1)} collective-permute-done((bf16[272,256]{1,0:T(8,128)(2,1)S(1)}, bf16[272,256]{1,0:T(8,128)(2,1)S(1)}, u32[]{:S(2)}, u32[]{:S(2)}) %collective-permute-start.11) | collective-permute-done | bytes 139296 | tf_op jit(solution)/shard_map/ppermute | solution.py:522
  54.9 1.1 %shard_map.195.refs_0_ = bf16[128,768]{1,0:T(8,128)(2,1)S(1)} custom-call(bf16[256,256]{1,0:T(8,128)(2,1)S(1)} %copy-done.14, bf16[528,256]{1,0:T(8,128)(2,1)S(1)} %collective-permute-done.8.refs_3_.refs_1_, bf16[256,256]{1,0:T(8,128)(2,1)S(1)} %collective-permute-done.9.refs_2_, bf16[256,256]{1,0:T(8,128)(2,1)S(1)} %collective-permute-done.10.refs_3_, ...), custom_call_target="tpu_custom_call" | custom-call | flops 600000000 | tf_op jit(solution)/shard_map/pallas_call | solution.py:114
  56.1 0.5 collective-permute-start.7
  56.6 0.9 %collective-permute-done.12.refs_1_ = bf16[128,768]{1,0:T(8,128)(2,1)S(1)} collective-permute-done((bf16[128,768]{1,0:T(8,128)(2,1)S(1)}, bf16[128,768]{1,0:T(8,128)(2,1)S(1)}, u32[]{:S(2)}, u32[]{:S(2)}) %collective-permute-start.12) | collective-permute-done | bytes 196640 | tf_op jit(solution)/shard_map/ppermute | solution.py:526
  57.5 1.0 %shard_map.196.refs_4_ = f32[128,1024]{1,0:T(8,128)S(1)} custom-call(bf16[128,768]{1,0:T(8,128)(2,1)S(1)} %shard_map.195.refs_0_, bf16[128,768]{1,0:T(8,128)(2,1)S(1)} %collective-permute-done.12.refs_1_, bf16[1024,1024]{1,0:T(8,128)(2,1)S(1)} %copy-done.1, bf16[2048,1024]{1,0:T(8,128)(2,1)S(1)} %copy-done), custom_call_target="tpu_custom_call" | custom-call | flops 600000000 | tf_op jit(solution)/shard_map/pallas_call | solution.py:114
  58.5 1.8 %shard_map.197 = bf16[128,1024]{1,0:T(8,128)(2,1)} custom-call(bf16[128,768]{1,0:T(8,128)(2,1)S(1)} %collective-permute-done.6.refs_0_, bf16[128,768]{1,0:T(8,128)(2,1)S(1)} %collective-permute-done.7.refs_1_, bf16[1024,1024]{1,0:T(8,128)(2,1)S(1)} %copy-done.1, bf16[2048,1024]{1,0:T(8,128)(2,1)S(1)} %copy-done, f32[128,1024]{1,0:T(8,128)S(1)} %shard_map.196.refs_4_), custom_call_target="tpu_custom_call" | custom-call | flops 600000000 | tf_op jit(solution)/shard_map/pallas_call | solution.py:114
  (52 shorter events, 0.3 us)
Async XLA Ops:
  0.0 15.2 %collective-permute-start = (bf16[128,2048]{1,0:T(8,128)(2,1)}, bf16[128,2048]{1,0:T(8,128)(2,1)S(1)}, u32[]{:S(2)}, u32[]{:S(2)}) collective-permute-start(bf16[128,2048]{1,0:T(8,128)(2,1)} %bitcast.48), channel_id=1, source_target_pairs={{0,2},{2,0},{1,3},{3,1},{4,6},{6,4},{5,7},{7,5},{8,10},{10,8},{9,1... | collective-permute-start | bytes 1572872 | tf_op jit(solution)/shard_map/ppermute | solution.py:526
  3.0 12.2 %collective-permute-start.1 = (f32[8,128]{1,0:T(8,128)}, f32[8,128]{1,0:T(8,128)S(1)}, u32[]{:S(2)}, u32[]{:S(2)}) collective-permute-start(f32[8,128]{1,0:T(8,128)} %bitcast.50), channel_id=1, source_target_pairs={{0,2},{2,0},{1,3},{3,1},{4,6},{6,4},{5,7},{7,5},{8,10},{10,8},{9,1... | collective-permute-start | bytes 12296 | tf_op jit(solution)/shard_map/ppermute | solution.py:526
  18.3 27.3 %copy-start.11 = (f32[256,256]{1,0:T(8,128)S(1)}, f32[256,256]{1,0:T(8,128)}, u32[]{:S(2)}) copy-start(f32[256,256]{1,0:T(8,128)} %get-tuple-element.45.refs_0_) | copy-start | bytes 786436
  18.3 27.3 %copy-start.12 = (f32[256,256]{1,0:T(8,128)S(1)}, f32[256,256]{1,0:T(8,128)}, u32[]{:S(2)}) copy-start(f32[256,256]{1,0:T(8,128)} %get-tuple-element.46.refs_1_) | copy-start | bytes 786436
  18.3 27.3 %copy-start.13 = (f32[256,256]{1,0:T(8,128)S(1)}, f32[256,256]{1,0:T(8,128)}, u32[]{:S(2)}) copy-start(f32[256,256]{1,0:T(8,128)} %get-tuple-element.47.refs_2_) | copy-start | bytes 786436
  18.4 30.8 %copy-start.17 = (f32[256]{0:T(256)S(1)}, f32[256]{0:T(256)}, u32[]{:S(2)}) copy-start(f32[256]{0:T(256)} %param.36) | copy-start | bytes 3076
  18.4 30.8 %copy-start.18 = (f32[128]{0:T(128)S(1)}, f32[128]{0:T(128)}, u32[]{:S(2)}) copy-start(f32[128]{0:T(128)} %param.35) | copy-start | bytes 1540
  18.4 30.8 %copy-start.19 = (f32[8]{0:T(128)S(1)}, f32[8]{0:T(128)}, u32[]{:S(2)}) copy-start(f32[8]{0:T(128)} %param.34) | copy-start | bytes 100
  18.4 36.5 %copy-start.10 = (f32[128,512]{1,0:T(8,128)S(1)}, f32[128,512]{1,0:T(8,128)}, u32[]{:S(2)}) copy-start(f32[128,512]{1,0:T(8,128)} %get-tuple-element.44.refs_6_) | copy-start | bytes 786436
  18.4 36.5 %copy-start.15 = (bf16[128,256]{1,0:T(8,128)(2,1)S(1)}, bf16[128,256]{1,0:T(8,128)(2,1)}, u32[]{:S(2)}) copy-start(bf16[128,256]{1,0:T(8,128)(2,1)} %get-tuple-element.42.refs_4_) | copy-start | bytes 196612
  18.4 36.5 %copy-start.16 = (bf16[128,256]{1,0:T(8,128)(2,1)S(1)}, bf16[128,256]{1,0:T(8,128)(2,1)}, u32[]{:S(2)}) copy-start(bf16[128,256]{1,0:T(8,128)(2,1)} %get-tuple-element.43.refs_5_) | copy-start | bytes 196612
  21.8 35.7 %copy-start = (bf16[2048,1024]{1,0:T(8,128)(2,1)S(1)}, bf16[2048,1024]{1,0:T(8,128)(2,1)}, u32[]{:S(2)}) copy-start(bf16[2048,1024]{1,0:T(8,128)(2,1)} %refs_3_.3) | copy-start | bytes 12582916
  21.9 35.6 %copy-start.1 = (bf16[1024,1024]{1,0:T(8,128)(2,1)S(1)}, bf16[1024,1024]{1,0:T(8,128)(2,1)}, u32[]{:S(2)}) copy-start(bf16[1024,1024]{1,0:T(8,128)(2,1)} %refs_2_.3) | copy-start | bytes 6291460
  21.9 15.0 %collective-permute-start.2 = (bf16[528,256]{1,0:T(8,128)(2,1)S(1)}, bf16[528,256]{1,0:T(8,128)(2,1)S(1)}, u32[]{:S(2)}, u32[]{:S(2)}) collective-permute-start(bf16[528,256]{1,0:T(8,128)(2,1)S(1)} %get-tuple-element.30), channel_id=1, source_target_pairs={{0,4},{4,0},{8,12},{12,8},{1,5},{5,1},{9,13},{13,9},{2,6},{6,2},{1... | collective-permute-start | bytes 811016 | tf_op jit(solution)/shard_map/ppermute | solution.py:522
  23.8 21.8 %collective-permute-start.8 = (bf16[528,256]{1,0:T(8,128)(2,1)S(1)}, bf16[528,256]{1,0:T(8,128)(2,1)S(1)}, u32[]{:S(2)}, u32[]{:S(2)}) collective-permute-start(bf16[528,256]{1,0:T(8,128)(2,1)S(1)} %copy-done.20), channel_id=1, source_target_pairs={{0,4},{4,0},{8,12},{12,8},{1,5},{5,1},{9,13},{13,9},{2,6},{6,2},{1... | collective-permute-start | bytes 811016 | tf_op jit(solution)/shard_map/ppermute | solution.py:522
  24.0 15.9 %collective-permute-start.3 = (bf16[256,256]{1,0:T(8,128)(2,1)S(1)}, bf16[256,256]{1,0:T(8,128)(2,1)S(1)}, u32[]{:S(2)}, u32[]{:S(2)}) collective-permute-start(bf16[256,256]{1,0:T(8,128)(2,1)S(1)} %get-tuple-element.29.refs_0_), channel_id=1, source_target_pairs={{0,8},{4,12},{8,0},{12,4},{1,9},{5,13},{9,1},{13,5},{2,10},{6,14},... | collective-permute-start | bytes 393224 | tf_op jit(solution)/shard_map/ppermute | solution.py:522
  26.8 16.0 %collective-permute-start.9 = (bf16[256,256]{1,0:T(8,128)(2,1)S(1)}, bf16[256,256]{1,0:T(8,128)(2,1)S(1)}, u32[]{:S(2)}, u32[]{:S(2)}) collective-permute-start(bf16[256,256]{1,0:T(8,128)(2,1)S(1)} %copy-done.14), channel_id=1, source_target_pairs={{0,8},{4,12},{8,0},{12,4},{1,9},{5,13},{9,1},{13,5},{2,10},{6,14},... | collective-permute-start | bytes 393224 | tf_op jit(solution)/shard_map/ppermute | solution.py:522
  37.9 11.2 %collective-permute-start.5 = (bf16[272,256]{1,0:T(8,128)(2,1)S(1)}, bf16[272,256]{1,0:T(8,128)(2,1)S(1)}, u32[]{:S(2)}, u32[]{:S(2)}) collective-permute-start(bf16[272,256]{1,0:T(8,128)(2,1)S(1)} %get-tuple-element.39), channel_id=1, source_target_pairs={{0,8},{4,12},{8,0},{12,4},{1,9},{5,13},{9,1},{13,5},{2,10},{6,14},... | collective-permute-start | bytes 417800 | tf_op jit(solution)/shard_map/ppermute | solution.py:522
  39.9 8.0 %collective-permute-start.4 = (bf16[256,256]{1,0:T(8,128)(2,1)S(1)}, bf16[256,256]{1,0:T(8,128)(2,1)S(1)}, u32[]{:S(2)}, u32[]{:S(2)}) collective-permute-start(bf16[256,256]{1,0:T(8,128)(2,1)S(1)} %collective-permute-done.3.refs_2_), channel_id=1, source_target_pairs={{0,4},{4,0},{8,12},{12,8},{1,5},{5,1},{9,13},{13,9},{2,6},{6,2},{1... | collective-permute-start | bytes 393224 | tf_op jit(solution)/shard_map/ppermute | solution.py:522
  42.8 9.0 %collective-permute-start.10 = (bf16[256,256]{1,0:T(8,128)(2,1)S(1)}, bf16[256,256]{1,0:T(8,128)(2,1)S(1)}, u32[]{:S(2)}, u32[]{:S(2)}) collective-permute-start(bf16[256,256]{1,0:T(8,128)(2,1)S(1)} %collective-permute-done.9.refs_2_), channel_id=1, source_target_pairs={{0,4},{4,0},{8,12},{12,8},{1,5},{5,1},{9,13},{13,9},{2,6},{6,2},{1... | collective-permute-start | bytes 393224 | tf_op jit(solution)/shard_map/ppermute | solution.py:522
  46.6 8.2 %collective-permute-start.11 = (bf16[272,256]{1,0:T(8,128)(2,1)S(1)}, bf16[272,256]{1,0:T(8,128)(2,1)S(1)}, u32[]{:S(2)}, u32[]{:S(2)}) collective-permute-start(bf16[272,256]{1,0:T(8,128)(2,1)S(1)} %get-tuple-element.50), channel_id=1, source_target_pairs={{0,8},{4,12},{8,0},{12,4},{1,9},{5,13},{9,1},{13,5},{2,10},{6,14},... | collective-permute-start | bytes 417800 | tf_op jit(solution)/shard_map/ppermute | solution.py:522
  50.3 5.8 %collective-permute-start.6 = (bf16[128,768]{1,0:T(8,128)(2,1)S(1)}, bf16[128,768]{1,0:T(8,128)(2,1)S(1)}, u32[]{:S(2)}, u32[]{:S(2)}) collective-permute-start(bf16[128,768]{1,0:T(8,128)(2,1)S(1)} %shard_map.193), channel_id=1, source_target_pairs={{0,2},{2,0},{1,3},{3,1},{4,6},{6,4},{5,7},{7,5},{8,10},{10,8},{9,1... | collective-permute-start | bytes 589832 | tf_op jit(solution)/shard_map/ppermute | solution.py:526
  56.0 1.5 %collective-permute-start.12 = (bf16[128,768]{1,0:T(8,128)(2,1)S(1)}, bf16[128,768]{1,0:T(8,128)(2,1)S(1)}, u32[]{:S(2)}, u32[]{:S(2)}) collective-permute-start(bf16[128,768]{1,0:T(8,128)(2,1)S(1)} %shard_map.195.refs_0_), channel_id=1, source_target_pairs={{0,1},{1,0},{2,3},{3,2},{4,5},{5,4},{6,7},{7,6},{8,9},{9,8},{10,11... | collective-permute-start | bytes 589832 | tf_op jit(solution)/shard_map/ppermute | solution.py:526
  56.1 2.4 %collective-permute-start.7 = (bf16[128,768]{1,0:T(8,128)(2,1)S(1)}, bf16[128,768]{1,0:T(8,128)(2,1)S(1)}, u32[]{:S(2)}, u32[]{:S(2)}) collective-permute-start(bf16[128,768]{1,0:T(8,128)(2,1)S(1)} %collective-permute-done.6.refs_0_), channel_id=1, source_target_pairs={{0,1},{1,0},{2,3},{3,2},{4,5},{5,4},{6,7},{7,6},{8,9},{9,8},{10,11... | collective-permute-start | bytes 589832 | tf_op jit(solution)/shard_map/ppermute | solution.py:526
  (10 other events, 102.4 us)

commit v3 on v2

v3 whole, which is shorter than its diff:
```python
import functools

import jax
import jax.numpy as jnp
from jax import lax
from jax.experimental import pallas as pl
from jax.experimental.pallas import tpu as pltpu
from jax.sharding import PartitionSpec as P

EPS = 1e-06
TAU = 16.0
BLK = 64
F32 = jnp.float32
BF16 = jnp.bfloat16
HIGH = lax.Precision.HIGHEST


def dot(a, b, dims=((1,), (0,)), precision=None):
    return lax.dot_general(a, b, (dims, ((), ())), precision=precision, preferred_element_type=F32)


def rms(x, gain):
    return x * lax.rsqrt(jnp.mean(x * x, axis=-1, keepdims=True) + EPS) * gain


def rms_halves(x, gain):
    _, width = x.shape
    half = width // 2
    first = lax.broadcasted_iota(jnp.int32, x.shape, 1) < half
    sq = x * x
    low = jnp.sum(jnp.where(first, sq, 0.0), axis=-1, keepdims=True) / half
    high = jnp.sum(jnp.where(first, 0.0, sq), axis=-1, keepdims=True) / half
    return x * jnp.where(first, lax.rsqrt(low + EPS), lax.rsqrt(high + EPS)) * gain


def whole(shape, memory_space=pltpu.VMEM):
    return pl.BlockSpec(shape, lambda *_: (0,) * len(shape), memory_space=memory_space)


def params(mib):
    return pltpu.CompilerParams(vmem_limit_bytes=int(mib * 2**20))


def cost(us):
    return pl.CostEstimate(flops=int(us * COST_SCALE), transcendentals=0, bytes_accessed=0)


COST_SCALE = 2e8
LINGER_US = 40


def unpack_weight(w_ref, wide_ref, heads, parts, out_ref, column):
    rows = w_ref.shape[0] // (heads * parts)
    if heads * parts == 1:
        out_ref[:, column : column + 128] = w_ref[...]
        return
    wide_ref[: w_ref.shape[0], :] = w_ref[...].astype(F32)
    for head in range(heads):
        for part in range(parts):
            piece = wide_ref[pl.ds(part * heads + head, rows, stride=heads * parts), :]
            at = column + (head * parts + part) * 128
            out_ref[:, at : at + 128] = piece.astype(BF16)


class Dims:
    def __init__(self, tokens, query_attend, value_attend, key_linear, value_linear, decay_up):
        self.rows = tokens.shape[1]
        self.model = tokens.shape[2]
        self.heads = query_attend.shape[1]
        self.ca = query_attend.shape[2]
        self.va = value_attend.shape[2]
        self.ck = key_linear.shape[2]
        self.cv = value_linear.shape[2]
        self.all_heads = decay_up.shape[1]
        self.rank = decay_up.shape[0]
        self.steps = 4
        self.chunk = self.model // self.steps
        self.fs_size = lax.axis_size("fs")
        self.tp_size = lax.axis_size("tp")
        self.sp_size = lax.axis_size("sp")

    def first_head(self):
        return (lax.axis_index("fs") * self.tp_size + lax.axis_index("tp")) * self.heads


class Fetch:
    def __init__(self, pairs, sems, window=None):
        self.copies = [pltpu.make_async_copy(src, dst, sems.at[i]) for i, (src, dst) in enumerate(pairs)]
        self.started = 0
        self.window = len(pairs) if window is None else window
        self.start_to(self.window)

    def start_to(self, end):
        while self.started < min(end, len(self.copies)):
            self.copies[self.started].start()
            self.started += 1

    def wait(self, *which):
        for i in which:
            self.start_to(i + 1)
            self.copies[i].wait()
            self.start_to(i + 1 + self.window)


HBM = pl.BlockSpec(memory_space=pltpu.HBM)


def call(body, us, mib, args, in_specs, outs, scratch):
    many = isinstance(outs, list)
    specs = [whole(o.shape) for o in outs] if many else whole(outs.shape)
    return pl.pallas_call(
        body,
        in_specs=in_specs,
        out_specs=specs,
        out_shape=outs,
        scratch_shapes=scratch,
        compiler_params=params(mib),
        cost_estimate=cost(us),
    )(*args)


def write_kv(acc, key_gain, dims, out):
    first = dims.first_head()
    rows, width = dims.rows, dims.heads * dims.ca
    for h in range(dims.heads):
        k = acc[:, h * dims.ca : (h + 1) * dims.ca].astype(BF16).astype(F32)
        row = 2 * (first + h)
        gain = jnp.concatenate([key_gain[pl.ds(row, 1), :], key_gain[pl.ds(row + 1, 1), :]], axis=1)
        out[:rows, h * dims.ca : (h + 1) * dims.ca] = rms_halves(k, gain).astype(BF16)
    out[rows : 2 * rows, :] = acc[:, width : width + dims.heads * dims.va].astype(BF16)


def projected(normed_ref, raws, layout, dims, w_out, wide):
    acc = None
    for c in range(dims.steps):
        here = slice(c * dims.chunk, (c + 1) * dims.chunk)
        column = 0
        for i, (raw, parts) in enumerate(zip(raws, layout)):
            n = raw.shape[0] // dims.steps
            unpack_weight(
                raw.at[c * n : (c + 1) * n, :], wide.at[i % 2], dims.heads, parts, w_out.at[here, :], column
            )
            column += dims.heads * parts * 128
        part = dot(normed_ref[:, here], w_out[here, :])
        acc = part if acc is None else acc + part
    return acc


def work_scratch(dims, weights):
    width = sum(w.shape[0] for w in weights) // dims.model * 128
    widest = max(w.shape[0] for w in weights) // dims.steps
    return [
        pltpu.VMEM((dims.rows, width), F32),
        pltpu.VMEM((dims.model, width), BF16),
        pltpu.VMEM((2, widest, 128), F32),
    ]


def keys_work(dims, values, gain, weights, key_gain):
    layout = (dims.ca // 128, dims.va // 128)
    raw = gain is not None
    args = (values, *weights, key_gain) + ((gain,) if raw else ())

    def body(*refs):
        tok, weights_in, kg = refs[0], refs[1:3], refs[3]
        if raw:
            gain_ref, kv_out, normed, acc, w_out, wide = refs[4:]
            normed[...] = rms(tok[...].astype(F32), gain_ref[...]).astype(BF16)
        else:
            kv_out, acc, w_out, wide = refs[4:]
            normed = tok
        acc[...] = projected(normed, weights_in, layout, dims, w_out, wide)
        write_kv(acc, kg, dims, kv_out)

    kv = jax.ShapeDtypeStruct((2 * dims.rows, dims.heads * dims.ca), BF16)
    normed = jax.ShapeDtypeStruct(values.shape, BF16)
    outs = [kv] + ([normed] if raw else [])
    return call(
        body, 2, 12, args, [whole(a.shape) for a in args], outs, work_scratch(dims, weights)
    )


def slot_outputs(dims):
    hd, rows = dims.heads, dims.rows
    return [
        jax.ShapeDtypeStruct((rows, hd * dims.ca), BF16),
        jax.ShapeDtypeStruct((rows, hd * dims.ck), BF16),
        jax.ShapeDtypeStruct((rows, hd * dims.cv), F32),
        jax.ShapeDtypeStruct((hd * dims.ck + 16, dims.cv), BF16),
        jax.ShapeDtypeStruct((hd * dims.ck, dims.cv), F32),
        jax.ShapeDtypeStruct((hd * dims.ck, dims.cv), F32),
        jax.ShapeDtypeStruct((hd * dims.ck, dims.cv), F32),
    ]


def slot_sequence(dims, slot):
    return lax.rem(lax.axis_index("fs") + dims.fs_size - slot, dims.fs_size)


def columns_of(row, width):
    return dot(row, jnp.ones((1, width), row.dtype), ((0,), (0,)), precision=HIGH if row.dtype == F32 else None)


def local_part(dims, slot, acc, low_rank, init, up, up_wide, bias, retain, query_gain, outs):
    q_out, reach_out, inside_out, send_out, state_out, decay_out, begin_out = outs
    hd, rows, ck, cv = dims.heads, dims.rows, dims.ck, dims.cv
    gain = jnp.concatenate([query_gain[...], query_gain[...]], axis=1)
    up_wide[...] = up[...].astype(F32)
    retain_columns = jnp.transpose(retain[...])
    head_lane = lax.broadcasted_iota(jnp.int32, retain_columns.shape, 1)
    row_id = lax.broadcasted_iota(jnp.int32, (rows, rows), 0)
    col_id = lax.broadcasted_iota(jnp.int32, (rows, rows), 1)
    same_block = row_id // BLK == col_id // BLK
    lower = row_id >= col_id
    summing = jnp.where(same_block & lower, 1.0, 0.0).astype(BF16)
    blocks = rows // BLK
    first = lax.axis_index("sp") == 0
    head0 = dims.first_head()
    sequence = slot_sequence(dims, slot)
    send_out[hd * ck :, :] = jnp.zeros((16, cv), BF16)
    for h in range(hd):
        q = acc[:, h * dims.ca : (h + 1) * dims.ca].astype(BF16).astype(F32)
        q_out[:, h * dims.ca : (h + 1) * dims.ca] = rms_halves(q, gain).astype(BF16)
    logs = []
    for h in range(hd):
        head = head0 + h
        up_head = up_wide[pl.ds(head, dims.rank, stride=dims.all_heads), :].astype(BF16)
        pre = dot(low_rank, up_head) + bias[pl.ds(head, 1), :]
        gate = jnp.minimum(pre, 0.0) - jnp.log1p(jnp.exp(-jnp.abs(pre)))
        kept = jnp.sum(jnp.where(head_lane == head, retain_columns, 0.0), axis=1, keepdims=True)
        logs.append(gate / TAU + kept)
    log_decay = jnp.concatenate(logs, axis=1)
    running = jnp.zeros_like(log_decay)
    left = log_decay
    for _ in range(3):
        term = left.astype(BF16)
        running = running + dot(summing, term)
        left = left - term.astype(F32)
    finals = [running[(b + 1) * BLK - 1 : (b + 1) * BLK, :] for b in range(blocks)]
    pivots = [running[b * BLK + BLK // 2 : b * BLK + BLK // 2 + 1, :] for b in range(blocks)]
    at = hd * dims.ca
    queries = acc[:, at : at + hd * ck].astype(BF16).astype(F32) * ck ** (-0.5)
    keys = acc[:, at + hd * ck : at + 2 * hd * ck].astype(BF16).astype(F32)
    q_edge, q_piv, k_piv, k_end, reach, faded = [], [], [], [], [], [None] * blocks
    before = jnp.zeros_like(finals[0])
    for b in range(blocks):
        here = slice(b * BLK, (b + 1) * BLK)
        run, q, k = running[here], queries[here], keys[here]
        q_edge.append(q * jnp.exp(run))
        q_piv.append((q * jnp.exp(run - pivots[b])).astype(BF16))
        k_piv.append((k * jnp.exp(pivots[b] - run)).astype(BF16))
        k_end.append(k * jnp.exp(finals[b] - run))
        reach.append((q_edge[b] * jnp.exp(before)).astype(BF16))
        reach_out[here, :] = reach[b]
        before = before + finals[b]
    later = jnp.zeros_like(finals[0])
    for b in range(blocks - 1, -1, -1):
        faded[b] = (k_end[b] * jnp.exp(later)).astype(BF16)
        later = later + finals[b]
    faded_rows = jnp.concatenate(faded, axis=0)
    decay = jnp.exp(before)
    for h in range(hd):
        of = slice(h * ck, (h + 1) * ck)
        at = hd * (dims.ca + 2 * ck) + h * cv
        vl = acc[:, at : at + cv].astype(BF16)
        for b in range(blocks):
            here = slice(b * BLK, (b + 1) * BLK)
            own = dot(q_piv[b][:, of], k_piv[b][:, of], ((1,), (1,)))
            own = jnp.where(lower[:BLK, :BLK], own, 0.0).astype(BF16)
            result = dot(own, vl[here])
            gap = jnp.zeros_like(finals[0][:, of])
            for c in range(b - 1, -1, -1):
                edge = (k_end[c][:, of] * jnp.exp(gap)).astype(BF16)
                across = dot(q_edge[b][:, of].astype(BF16), edge, ((1,), (1,)))
                result = result + dot(across.astype(BF16), vl[c * BLK : (c + 1) * BLK])
                gap = gap + finals[c][:, of]
            inside_out[here, h * cv : (h + 1) * cv] = result
        state = dot(faded_rows[:, of], vl, ((0,), (0,)))
        columns = columns_of(decay[:, of], cv)
        begin = init[pl.ds((sequence * hd + h) * ck, ck), :]
        begin = jnp.where(first, begin, 0.0)
        begin_out[of, :] = begin
        state = state + columns * begin
        state_out[of, :] = state
        decay_out[of, :] = columns
        send_out[of, :] = state.astype(BF16)
        at = hd * ck + h
        send_out[at : at + 1, :ck] = decay[:, of].astype(BF16)


def rest_work(dims, slot, values, gain, weights, consts):
    layout = (dims.ca // 128, dims.ck // 128, dims.ck // 128, dims.cv // 128)
    raw = gain is not None
    n_out, n_in = len(slot_outputs(dims)), 1 + len(weights) + len(consts)
    args = (values, *weights, *consts) + ((gain,) if raw else ())

    def body(*refs):
        inputs, refs = refs[:n_in], refs[n_in:]
        tok, raws, consts_v = inputs[0], inputs[1 : 1 + len(weights)], inputs[1 + len(weights) :]
        if raw:
            gain_ref, refs = refs[0], refs[1:]
            outs, normed, (acc, w_out, wide, up_wide) = refs[:n_out], refs[n_out], refs[n_out + 1 :]
            normed[...] = rms(tok[...].astype(F32), gain_ref[...]).astype(BF16)
        else:
            outs, (acc, w_out, wide, up_wide) = refs[:n_out], refs[n_out:]
            normed = tok
        acc[...] = projected(normed, raws, layout, dims, w_out, wide)
        down, init, up, bias, retain, query_gain = consts_v
        low = dot(normed[...], down[...], ((1,), (1,))).astype(BF16)
        local_part(dims, slot, acc, low, init, up, up_wide, bias, retain, query_gain, outs)

    outs = slot_outputs(dims) + ([jax.ShapeDtypeStruct(values.shape, BF16)] if raw else [])
    scratch = work_scratch(dims, weights) + [pltpu.VMEM(consts[2].shape, F32)]
    return call(body, 4, 18, args, [whole(a.shape) for a in args], outs, scratch)


def linger(x):
    def body(x_ref, out):
        out[...] = x_ref[...]

    return call(body, LINGER_US, 1, (x,), [whole(x.shape)], jax.ShapeDtypeStruct(x.shape, x.dtype), [])


def combine(dims, bit, state, decay, prefix, prefix_decay, received):
    hd, ck, cv = dims.heads, dims.ck, dims.cv
    begun = prefix_decay is not None

    def body(*refs):
        if begun:
            st, dec, pre, pre_dec, rec, send_out, st_out, dec_out, pre_out, pre_dec_out = refs
        else:
            st, dec, pre, rec, send_out, st_out, dec_out, pre_out, pre_dec_out = refs
        upper = lax.rem(lax.axis_index("sp") // bit, 2) == 1
        send_out[hd * ck :, :] = jnp.zeros((16, cv), BF16)
        for h in range(hd):
            at = slice(h * ck, (h + 1) * ck)
            other = rec[at, :].astype(F32)
            other_row = rec[hd * ck + h : hd * ck + h + 1, :ck]
            other_dec = columns_of(other_row, cv)
            mine, mine_dec = st[at, :], dec[at, :]
            earlier = jnp.where(upper, other, mine)
            late = jnp.where(upper, mine, other)
            total = earlier * jnp.where(upper, mine_dec, other_dec) + late
            st_out[at, :] = total
            send_out[at, :] = total.astype(BF16)
            both = mine_dec * other_dec
            dec_out[at, :] = both
            if bit * 4 < dims.sp_size:
                send_out[hd * ck + h : hd * ck + h + 1, :ck] = jnp.transpose(both[:, :128])[:1, :].astype(BF16)
            if begun:
                pre_out[at, :] = pre[at, :] + jnp.where(upper, pre_dec[at, :] * other, 0.0)
                pre_dec_out[at, :] = jnp.where(upper, pre_dec[at, :] * other_dec, pre_dec[at, :])
            else:
                pre_out[at, :] = jnp.where(upper, other, pre[at, :])
                pre_dec_out[at, :] = jnp.where(upper, other_dec, 1.0)

    full = jax.ShapeDtypeStruct((hd * ck, cv), F32)
    args = (state, decay, prefix) + ((prefix_decay,) if begun else ()) + (received,)
    return call(
        body,
        2,
        6,
        args,
        [whole(a.shape) for a in args],
        [jax.ShapeDtypeStruct((hd * ck + 16, cv), BF16), full, full, full, full],
        [],
    )


def attend(dims, kv_blocks, q_unit, mix_gain, diff_lambda):
    hd, rows, ca, va = dims.heads, dims.rows, dims.ca, dims.va
    count = len(kv_blocks)
    scale = (ca // 2) ** (-0.5)

    def body(*refs):
        kvs = refs[:count]
        q_ref, mix_ref, lam_ref, out = refs[count:]
        place = lax.axis_index("sp")
        head0 = dims.first_head()
        lane = lax.broadcasted_iota(jnp.int32, (rows, ca), 1)
        row_id = lax.rem(lax.broadcasted_iota(jnp.int32, (2 * rows, rows), 0), rows)
        col_id = lax.broadcasted_iota(jnp.int32, (2 * rows, rows), 1)
        allowed = row_id // BLK >= col_id // BLK
        lam_lane = lax.broadcasted_iota(jnp.int32, lam_ref.shape, 1)
        for h in range(hd):
            q = q_ref[:, h * ca : (h + 1) * ca]
            zero = jnp.zeros_like(q)
            pair = jnp.concatenate([jnp.where(lane < ca // 2, q, zero), jnp.where(lane < ca // 2, zero, q)], axis=0)
            scores = []
            for m in range(count):
                s = dot(pair, kvs[m][:rows, h * ca : (h + 1) * ca], ((1,), (1,))) * scale
                if m == 0:
                    s = jnp.where(allowed, s, -jnp.inf)
                else:
                    s = jnp.where(jnp.bitwise_xor(place, m) < place, s, -jnp.inf)
                scores.append(s)
            top = jnp.max(functools.reduce(jnp.maximum, scores), axis=1, keepdims=True)
            total = jnp.zeros((2 * rows, rows), F32)
            sums = jnp.zeros((2 * rows, va), F32)
            for m in range(count):
                raised = jnp.exp(scores[m] - top)
                total = total + raised
                sums = sums + dot(raised.astype(BF16), kvs[m][rows : 2 * rows, h * va : (h + 1) * va])
            ratio = sums / jnp.sum(total, axis=1, keepdims=True)
            lam = jnp.sum(jnp.where(lam_lane == head0 + h, lam_ref[...], 0.0), axis=1, keepdims=True)
            diff = ratio[:rows] - lam * ratio[rows:]
            out[:, h * va : (h + 1) * va] = rms(diff, mix_ref[...]).astype(BF16)

    args = (*kv_blocks, q_unit, mix_gain, diff_lambda)
    out = jax.ShapeDtypeStruct((rows, hd * va), BF16)
    return call(body, 1.5, 8, args, [whole(a.shape) for a in args], out, [])


def recall(dims, bit, reach, inside, prefix, prefix_decay, received, state_gain):
    hd, rows, ck, cv = dims.heads, dims.rows, dims.ck, dims.cv

    def body(reach_ref, inside_ref, pre, pre_dec, rec, sg_ref, out):
        upper = lax.rem(lax.axis_index("sp") // bit, 2) == 1
        for h in range(hd):
            at, wide = slice(h * ck, (h + 1) * ck), slice(h * cv, (h + 1) * cv)
            enter = pre[at, :] + jnp.where(upper, pre_dec[at, :] * rec[at, :].astype(F32), 0.0)
            raw = inside_ref[:, wide] + dot(reach_ref[:, at], enter.astype(BF16))
            out[:, wide] = rms(raw, sg_ref[...]).astype(BF16)

    args = (reach, inside, prefix, prefix_decay, received, state_gain)
    out = jax.ShapeDtypeStruct((rows, hd * cv), BF16)
    return call(body, 1, 6, args, [whole(a.shape) for a in args], out, [])


def project_out(dims, pieces, weights, start, last):
    rows, cols = dims.rows, weights[0].shape[1]
    count = len(pieces)
    used = sorted({which for _, which, _, _ in pieces})

    def body(*refs):
        parts, mats, out = refs[:count], dict(zip(used, refs[count : count + len(used)])), refs[-1]
        fs, tp = lax.axis_index("fs"), lax.axis_index("tp")
        total = refs[count + len(used)][...] if start is not None else jnp.zeros((rows, cols), F32)
        for ref, (_, which, j, step) in zip(parts, pieces):
            owner = lax.rem(fs + j, dims.fs_size) * dims.tp_size + lax.rem(tp + step, dims.tp_size)
            size = ref.shape[1]
            at = pl.multiple_of(owner * size, size)
            total = total + dot(ref[...], mats[which][pl.ds(at, size), :])
        out[...] = total.astype(out.dtype)

    args = [p[0] for p in pieces] + [weights[w] for w in used] + ([] if start is None else [start])
    out = jax.ShapeDtypeStruct((rows, cols), BF16 if last else F32)
    return call(body, 1, 6, args, [whole(a.shape) for a in args], out, [])


def swap(x, axis, bit, size):
    return lax.ppermute(x, axis, [(i, i ^ bit) for i in range(size)])


def shift(x, axis, by, size):
    return lax.ppermute(x, axis, [(i, (i + by) % size) for i in range(size)])


def low_bit(m):
    return m & -m


def body(
    tokens,
    norm_gain,
    query_attend,
    key_attend,
    value_attend,
    query_linear,
    key_linear,
    value_linear,
    decay_down,
    decay_up,
    decay_bias,
    log_retain,
    query_gain,
    key_gain,
    diff_lambda,
    mix_gain,
    state_gain,
    init_state,
    output_attend,
    output_linear,
):
    fs_size, tp_size, sp_size = (lax.axis_size(a) for a in ("fs", "tp", "sp"))
    dims = Dims(tokens, query_attend, value_attend, key_linear, value_linear, decay_up)
    rows = dims.rows

    def flat(w):
        d, h, c = w.shape
        parts = c // 128
        return w.reshape(d, h, parts, 128).transpose(0, 2, 1, 3).reshape(d * parts * h, 128)

    own = tokens[0]
    retain_own = log_retain[0].T
    gain = norm_gain.reshape(1, -1)
    kg = key_gain.reshape(-1, key_gain.shape[-1])
    up = decay_up.reshape(-1, decay_up.shape[-1])
    init = init_state.reshape(-1, dims.cv)
    token_slots = [own] + [shift(own, "fs", j, fs_size) for j in range(1, fs_size)]
    retains = [retain_own] + [shift(retain_own, "fs", j, fs_size) for j in range(1, fs_size)]

    def keys_of_all(kv):
        blocks = [kv]
        for m in range(1, sp_size):
            blocks.append(swap(blocks[m - low_bit(m)], "sp", low_bit(m), sp_size))
        return blocks

    def entering(send, state, decay, prefix):
        prefix_decay, bit = None, 1
        while True:
            received = swap(send, "sp", bit, sp_size)
            if bit * 2 >= sp_size:
                return bit, prefix, prefix_decay, received
            send, state, decay, prefix, prefix_decay = combine(
                dims, bit, state, decay, prefix, prefix_decay, received
            )
            bit *= 2

    kv_weights = [flat(w) for w in (key_attend, value_attend)]
    rest_weights = [flat(w) for w in (query_attend, query_linear, key_linear, value_linear)]
    blocks, outs, states = [], [], []
    for j in range(fs_size):
        consts = (decay_down.T, init, up, decay_bias, retains[j], query_gain.reshape(1, -1))
        if j == 0:
            kv, normed = keys_work(dims, own, linger(gain), kv_weights, kg)
            out = rest_work(dims, j, normed, None, rest_weights, consts)
        else:
            *out, normed = rest_work(dims, j, token_slots[j], gain, rest_weights, consts)
            (kv,) = keys_work(dims, normed, None, kv_weights, kg)
        blocks.append(keys_of_all(kv))
        outs.append(out)
        states.append(entering(*out[3:]))

    mix, sg, lam = mix_gain.reshape(1, -1), state_gain.reshape(1, -1), diff_lambda.reshape(1, -1)
    weights = (output_attend, output_linear)
    early, late, last = [], [], []
    for j in range(fs_size):
        q_unit, reach, inside = outs[j][:3]
        bit, *entered = states[j]
        for which in range(2):
            if which == 0:
                value = attend(dims, blocks[j], q_unit, mix, lam)
            else:
                value = recall(dims, bit, reach, inside, *entered, sg)
            if j:
                value = shift(value, "fs", -j, fs_size)
            arrived = [value]
            arrived += [shift(value, "tp", -i, tp_size) for i in range(1, tp_size)]
            groups = [early] * tp_size if j else [late] + [last] * (tp_size - 1)
            for i, group in enumerate(groups):
                group.append((arrived[i], which, j, i))
    total = None
    groups = [(n, g) for n, g in (("early", early), ("late", late), ("last", last)) if g]
    for name, group in groups:
        total = project_out(dims, group, weights, total, name == groups[-1][0])
    return total.reshape(1, rows, -1)


def solution(mesh):
    heads = P(None, ("fs", "tp"), None)
    positions = P(("grp", "fs"), "sp", None)
    in_specs = (
        positions,
        P(),
        heads,
        heads,
        heads,
        heads,
        heads,
        heads,
        P(),
        P(),
        P(),
        positions,
        P(),
        P(),
        P(),
        P(),
        P(),
        P("grp", ("fs", "tp"), None, None),
        P(None, "tp"),
        P(None, "tp"),
    )
    out_specs = P(("grp", "fs"), "sp", "tp")

    return jax.shard_map(body, mesh=mesh, in_specs=in_specs, out_specs=out_specs, check_vma=False)
```

time: 60.4 us -> 71.6 us (1.19)
  the two profiles are of different devices: /device:TPU:0 before, /device:TPU:31 now
where the time goes in v3:
time: 71.6 us; the launch traced here: 70.3 us
  waiting for transfers between devices  29.7 us (41%)
  Pallas kernels  16.7 us (23%)
  starting transfers between devices  12.1 us (17%)
  local copies, waits for them, and re-layouts  11.6 us (16%)
    ppermute x10, waiting for transfers between devices, swap(): return lax.ppermute(x, axis, [(i, i ^ bit) for i in range(size)])  17.6 us
    pallas_call x14, Pallas kernels, call(): pl.pallas_call(body, in_specs=in_specs, out_specs=specs, out_shape=outs,...  16.7 us
    ppermute x8, waiting for transfers between devices, shift(): return lax.ppermute(x, axis, [(i, (i + by) % size) for i in range(size)])  12.1 us
    unnamed x58, local copies, waits for them, and re-layouts  11.6 us
    ppermute x8, starting transfers between devices, shift(): return lax.ppermute(x, axis, [(i, (i + by) % size) for i in range(size)])  7.8 us
    ppermute x10, starting transfers between devices, swap(): return lax.ppermute(x, axis, [(i, i ^ bit) for i in range(size)])  4.26 us
  transfers between devices with their start and end apart: 18, of which 9 were waited for; matrix products, arithmetic and copies ran while one was open for 0% of the time, Pallas kernels for 17%

profile of v3, /device:TPU:31, one launch (start us, length us, event | category | flops | bytes accessed | tf_op | source)
XLA Modules:
  0.0 70.3 jit_solution(8708125066874856178)
XLA Ops:
  0.3 1.2 %collective-permute-start.8 = (f32[8,128]{1,0:T(8,128)}, f32[8,128]{1,0:T(8,128)S(1)}, u32[]{:S(2)}, u32[]{:S(2)}) collective-permute-start(f32[8,128]{1,0:T(8,128)} %bitcast.48), channel_id=1, source_target_pairs={{0,2},{2,0},{1,3},{3,1},{4,6},{6,4},{5,7},{7,5},{8,10},{10,8},{9,1... | collective-permute-start | bytes 12296 | tf_op jit(solution)/shard_map/ppermute | solution.py:456
  1.5 11.6 %collective-permute-done.8.refs_9_ = f32[8,128]{1,0:T(8,128)S(1)} collective-permute-done((f32[8,128]{1,0:T(8,128)}, f32[8,128]{1,0:T(8,128)S(1)}, u32[]{:S(2)}, u32[]{:S(2)}) %collective-permute-start.8) | collective-permute-done | bytes 4128 | tf_op jit(solution)/shard_map/ppermute | solution.py:456
  13.1 1.6 %copy-done.2 = bf16[2048,2,256]{2,1,0:T(2,128)(2,1)S(1)} copy-done((bf16[2048,2,256]{2,1,0:T(2,128)(2,1)S(1)}, bf16[2048,2,256]{2,1,0:T(2,128)(2,1)}, u32[]{:S(2)}) %copy-start.2) | copy-done | bytes 2097176
  14.7 1.2 %copy-done.4 = bf16[2048,2,128]{2,1,0:T(2,128)(2,1)S(1)} copy-done((bf16[2048,2,128]{2,1,0:T(2,128)(2,1)S(1)}, bf16[2048,2,128]{2,1,0:T(2,128)(2,1)}, u32[]{:S(2)}) %copy-start.4) | copy-done | bytes 1048600
  15.9 1.2 %copy-done.6 = bf16[2048,2,128]{2,1,0:T(2,128)(2,1)S(1)} copy-done((bf16[2048,2,128]{2,1,0:T(2,128)(2,1)S(1)}, bf16[2048,2,128]{2,1,0:T(2,128)(2,1)}, u32[]{:S(2)}) %copy-start.6) | copy-done | bytes 1048600
  17.2 1.2 %copy-done.8 = bf16[2048,2,128]{2,1,0:T(2,128)(2,1)S(1)} copy-done((bf16[2048,2,128]{2,1,0:T(2,128)(2,1)S(1)}, bf16[2048,2,128]{2,1,0:T(2,128)(2,1)}, u32[]{:S(2)}) %copy-start.8) | copy-done | bytes 1048600
  18.4 1.0 %copy-done.12 = f32[2,2,128,256]{3,2,1,0:T(8,128)S(1)} copy-done((f32[2,2,128,256]{3,2,1,0:T(8,128)S(1)}, f32[2,2,128,256]{3,2,1,0:T(8,128)}, u32[]{:S(2)}) %copy-start.12) | copy-done | bytes 524312
  23.2 4.0 %shard_map.196 = (bf16[128,256]{1,0:T(8,128)(2,1)S(1)}, bf16[128,256]{1,0:T(8,128)(2,1)S(1)}, f32[128,512]{1,0:T(8,128)S(1)}, bf16[272,256]{1,0:T(8,128)(2,1)S(1...) custom-call(bf16[128,2048]{1,0:T(8,128)(2,1)S(1)} %collective-permut, ...), custom_call_target="tpu_custom_call" | custom-call | flops 800000000 | tf_op jit(solution)/shard_map/pallas_call | solution.py:111
  27.5 0.9 %copy-done.10 = bf16[2048,2,128]{2,1,0:T(2,128)(2,1)S(1)} copy-done((bf16[2048,2,128]{2,1,0:T(2,128)(2,1)S(1)}, bf16[2048,2,128]{2,1,0:T(2,128)(2,1)}, u32[]{:S(2)}) %copy-start.10) | copy-done | bytes 1048600
  28.9 1.3 %shard_map.191 = (bf16[256,256]{1,0:T(8,128)(2,1)S(1)}, bf16[128,2048]{1,0:T(8,128)(2,1)S(1)}) custom-call(bf16[128,2048]{1,0:T(8,128)(2,1)S(1)} %bitcast.39, bf16[4096,128]{1,0:T(8,128)(2,1)S(1)} %bitcast.32, bf16[4096,128]{1,0:T(8,128)(2,1)S(1)} %bitcast.34, f32[16,64]{1,0:T(8,128)S(1)} %bitcast.44, f32[1,2048]{1,0:T(1,128)S(1)} %shard_map.190.refs_4_), custom_call_target="tpu_custom_call" | custom-call | flops 400000000 | tf_op jit(solution)/shard_map/pallas_call | solution.py:111
  30.2 1.2 %shard_map.197.refs_0_ = bf16[256,256]{1,0:T(8,128)(2,1)S(1)} custom-call(bf16[128,2048]{1,0:T(8,128)(2,1)S(1)} %get-tuple-element.40.refs_0_, bf16[4096,128]{1,0:T(8,128)(2,1)S(1)} %bitcast.33, bf16[4096,128]{1,0:T(8,128)(2,1)S(1)} %bitcast.35, f32[16,64]{1,0:T(8,128)S(1)} %bitcast.45), custom_call_target="tpu_custom_call" | custom-call | flops 400000000 | tf_op jit(solution)/shard_map/pallas_call | solution.py:111
  31.6 1.0 %shard_map.199 = (bf16[272,256]{1,0:T(8,128)(2,1)S(1)}, f32[256,256]{1,0:T(8,128)}, f32[256,256]{1,0:T(8,128)}, f32[256,256]{1,0:T(8,128)S(1)}, f32[256,256]{1,0:T(8,128)S(1)}) custom-call(f32[256,256]{1,0:T(8,128)S(1)} %get-tuple-element.44.refs_0_, f32[256,256]{1,0:T(8,128)S(1)} %get-tuple-element.45.refs_1_, f32[256,256]{1,0:T(8,128)S(1)} %get-tuple-element.46.refs_2_, ...), custom_call_target="tpu_custom_call" | custom-call | flops 400000000 | tf_op jit(solution)/shard_map/pallas_call | solution.py:111
  32.6 2.3 %collective-permute-start.15 = (bf16[272,256]{1,0:T(8,128)(2,1)S(1)}, bf16[272,256]{1,0:T(8,128)(2,1)S(1)}, u32[]{:S(2)}, u32[]{:S(2)}) collective-permute-start(bf16[272,256]{1,0:T(8,128)(2,1)S(1)} %get-tuple-element.50), channel_id=1, source_target_pairs={{0,8},{4,12},{8,0},{12,4},{1,9},{5,13},{9,1},{13,5},{2,10},{6,14},... | collective-permute-start | bytes 417800 | tf_op jit(solution)/shard_map/ppermute | solution.py:452
  35.0 3.7 %shard_map.192 = (bf16[128,256]{1,0:T(8,128)(2,1)S(1)}, bf16[128,256]{1,0:T(8,128)(2,1)S(1)}, f32[128,512]{1,0:T(8,128)S(1)}, bf16[272,256]{1,0:T(8,128)(2,1)S(1...) custom-call(bf16[128,2048]{1,0:T(8,128)(2,1)S(1)} %get-tuple-element.29.refs_0_, ...), custom_call_target="tpu_custom_call" | custom-call | flops 800000000 | tf_op jit(solution)/shard_map/pallas_call | solution.py:111
  39.0 1.3 %collective-permute-start.9 = (bf16[256,256]{1,0:T(8,128)(2,1)S(1)}, bf16[256,256]{1,0:T(8,128)(2,1)S(1)}, u32[]{:S(2)}, u32[]{:S(2)}) collective-permute-start(bf16[256,256]{1,0:T(8,128)(2,1)S(1)} %shard_map.197.refs_0_), channel_id=1, source_target_pairs={{0,4},{4,0},{8,12},{12,8},{1,5},{5,1},{9,13},{13,9},{2,6},{6,2},{1... | collective-permute-start | bytes 393224 | tf_op jit(solution)/shard_map/ppermute | solution.py:452
  40.3 3.2 %collective-permute-done.10.refs_2_ = bf16[256,256]{1,0:T(8,128)(2,1)S(1)} collective-permute-done((bf16[256,256]{1,0:T(8,128)(2,1)S(1)}, bf16[256,256]{1,0:T(8,128)(2,1)S(1)}, u32[]{:S(2)}, u32[]{:S(2)}) %collective-permute-start.10) | collective-permute-done | bytes 131104 | tf_op jit(solution)/shard_map/ppermute | solution.py:452
  43.5 5.1 %collective-permute-done.15.rec = bf16[272,256]{1,0:T(8,128)(2,1)S(1)} collective-permute-done((bf16[272,256]{1,0:T(8,128)(2,1)S(1)}, bf16[272,256]{1,0:T(8,128)(2,1)S(1)}, u32[]{:S(2)}, u32[]{:S(2)}) %collective-permute-start.15) | collective-permute-done | bytes 139296 | tf_op jit(solution)/shard_map/ppermute | solution.py:452
  49.5 1.0 %shard_map.194 = (bf16[272,256]{1,0:T(8,128)(2,1)S(1)}, f32[256,256]{1,0:T(8,128)}, f32[256,256]{1,0:T(8,128)}, f32[256,256]{1,0:T(8,128)S(1)}, f32[256,256]{1,0:T(8,128)S(1)}) custom-call(f32[256,256]{1,0:T(8,128)S(1)} %get-tuple-element.33.refs_0_, f32[256,256]{1,0:T(8,128)S(1)} %get-tuple-element.34.refs_1_, f32[256,256]{1,0:T(8,128)S(1)} %get-tuple-element.35.refs_2_, ...), custom_call_target="tpu_custom_call" | custom-call | flops 400000000 | tf_op jit(solution)/shard_map/pallas_call | solution.py:111
  50.5 1.7 %collective-permute-done.1.refs_2_ = bf16[256,256]{1,0:T(8,128)(2,1)S(1)} collective-permute-done((bf16[256,256]{1,0:T(8,128)(2,1)S(1)}, bf16[256,256]{1,0:T(8,128)(2,1)S(1)}, u32[]{:S(2)}, u32[]{:S(2)}) %collective-permute-start.1) | collective-permute-done | bytes 131104 | tf_op jit(solution)/shard_map/ppermute | solution.py:452
  52.2 2.8 %collective-permute-done.9.refs_1_ = bf16[256,256]{1,0:T(8,128)(2,1)S(1)} collective-permute-done((bf16[256,256]{1,0:T(8,128)(2,1)S(1)}, bf16[256,256]{1,0:T(8,128)(2,1)S(1)}, u32[]{:S(2)}, u32[]{:S(2)}) %collective-permute-start.9) | collective-permute-done | bytes 131104 | tf_op jit(solution)/shard_map/ppermute | solution.py:452
  55.0 4.5 %collective-permute-done.11.refs_3_ = bf16[256,256]{1,0:T(8,128)(2,1)S(1)} collective-permute-done((bf16[256,256]{1,0:T(8,128)(2,1)S(1)}, bf16[256,256]{1,0:T(8,128)(2,1)S(1)}, u32[]{:S(2)}, u32[]{:S(2)}) %collective-permute-start.11) | collective-permute-done | bytes 131104 | tf_op jit(solution)/shard_map/ppermute | solution.py:452
  61.1 2.1 %collective-permute-start.17 = (bf16[128,512]{1,0:T(8,128)(2,1)S(1)}, bf16[128,512]{1,0:T(8,128)(2,1)S(1)}, u32[]{:S(2)}, u32[]{:S(2)}) collective-permute-start(bf16[128,512]{1,0:T(8,128)(2,1)S(1)} %collective-permute-done.16.refs_2_), channel_id=1, source_target_pairs={{0,1},{1,0},{2,3},{3,2},{4,5},{5,4},{6,7},{7,6},{8,9},{9,8},{10,11... | collective-permute-start | bytes 393224 | tf_op jit(solution)/shard_map/ppermute | solution.py:456
  64.0 3.1 %collective-permute-start.13 = (bf16[128,256]{1,0:T(8,128)(2,1)S(1)}, bf16[128,256]{1,0:T(8,128)(2,1)S(1)}, u32[]{:S(2)}, u32[]{:S(2)}) collective-permute-start(bf16[128,256]{1,0:T(8,128)(2,1)S(1)} %collective-permute-done.12.refs_0_), channel_id=1, source_target_pairs={{0,1},{1,0},{2,3},{3,2},{4,5},{5,4},{6,7},{7,6},{8,9},{9,8},{10,11... | collective-permute-start | bytes 196616 | tf_op jit(solution)/shard_map/ppermute | solution.py:456
  69.2 1.1 %shard_map.203 = bf16[128,1024]{1,0:T(8,128)(2,1)} custom-call(bf16[128,256]{1,0:T(8,128)(2,1)S(1)} %collective-permute-done.3.refs_0_, bf16[128,512]{1,0:T(8,128)(2,1)S(1)} %collective-permute-done.6.refs_1_, bf16[1024,1024]{1,0:T(8,128)(2,1)S(1)} %copy-done.1, bf16[2048,1024]{1,0:T(8,128)(2,1)S(1)} %copy-done, f32[128,1024]{1,0:T(8,128)S(1)} %shard_map.202.refs_4_), custom_call_target="tpu_custom_call" | custom-call | flops 200000000 | tf_op jit(solution)/shard_map/pallas_call | solution.py:111
  (84 shorter events, 10.5 us)
Async XLA Ops:
  0.0 13.1 %collective-permute-start.7 = (bf16[128,2048]{1,0:T(8,128)(2,1)}, bf16[128,2048]{1,0:T(8,128)(2,1)S(1)}, u32[]{:S(2)}, u32[]{:S(2)}) collective-permute-start(bf16[128,2048]{1,0:T(8,128)(2,1)} %bitcast.38), channel_id=1, source_target_pairs={{0,2},{2,0},{1,3},{3,1},{4,6},{6,4},{5,7},{7,5},{8,10},{10,8},{9,1... | collective-permute-start | bytes 1572872 | tf_op jit(solution)/shard_map/ppermute | solution.py:456
  0.3 12.9 %collective-permute-start.8 = (f32[8,128]{1,0:T(8,128)}, f32[8,128]{1,0:T(8,128)S(1)}, u32[]{:S(2)}, u32[]{:S(2)}) collective-permute-start(f32[8,128]{1,0:T(8,128)} %bitcast.48), channel_id=1, source_target_pairs={{0,2},{2,0},{1,3},{3,1},{4,6},{6,4},{5,7},{7,5},{8,10},{10,8},{9,1... | collective-permute-start | bytes 12296 | tf_op jit(solution)/shard_map/ppermute | solution.py:456
  27.2 4.3 %collective-permute-start.14 = (bf16[272,256]{1,0:T(8,128)(2,1)S(1)}, bf16[272,256]{1,0:T(8,128)(2,1)S(1)}, u32[]{:S(2)}, u32[]{:S(2)}) collective-permute-start(bf16[272,256]{1,0:T(8,128)(2,1)S(1)} %get-tuple-element.47), channel_id=1, source_target_pairs={{0,4},{4,0},{8,12},{12,8},{1,5},{5,1},{9,13},{13,9},{2,6},{6,2},{1... | collective-permute-start | bytes 417800 | tf_op jit(solution)/shard_map/ppermute | solution.py:452
  28.8 6.1 %copy-start.16 = (bf16[2048,32]{0,1:T(8,128)(2,1)S(1)}, bf16[2048,32]{0,1:T(8,128)(2,1)}, u32[]{:S(2)}) copy-start(bf16[2048,32]{0,1:T(8,128)(2,1)} %param.28) | copy-start | bytes 393220
  31.4 12.1 %collective-permute-start.10 = (bf16[256,256]{1,0:T(8,128)(2,1)S(1)}, bf16[256,256]{1,0:T(8,128)(2,1)S(1)}, u32[]{:S(2)}, u32[]{:S(2)}) collective-permute-start(bf16[256,256]{1,0:T(8,128)(2,1)S(1)} %shard_map.197.refs_0_), channel_id=1, source_target_pairs={{0,8},{4,12},{8,0},{12,4},{1,9},{5,13},{9,1},{13,5},{2,10},{6,14},... | collective-permute-start | bytes 393224 | tf_op jit(solution)/shard_map/ppermute | solution.py:452
  32.6 16.0 %collective-permute-start.15 = (bf16[272,256]{1,0:T(8,128)(2,1)S(1)}, bf16[272,256]{1,0:T(8,128)(2,1)S(1)}, u32[]{:S(2)}, u32[]{:S(2)}) collective-permute-start(bf16[272,256]{1,0:T(8,128)(2,1)S(1)} %get-tuple-element.50), channel_id=1, source_target_pairs={{0,8},{4,12},{8,0},{12,4},{1,9},{5,13},{9,1},{13,5},{2,10},{6,14},... | collective-permute-start | bytes 417800 | tf_op jit(solution)/shard_map/ppermute | solution.py:452
  35.0 13.6 %copy-start.24 = (f32[256]{0:T(256)S(1)}, f32[256]{0:T(256)}, u32[]{:S(2)}) copy-start(f32[256]{0:T(256)} %param.36) | copy-start | bytes 3076
  35.0 33.0 %copy-start.1 = (bf16[1024,1024]{1,0:T(8,128)(2,1)S(1)}, bf16[1024,1024]{1,0:T(8,128)(2,1)}, u32[]{:S(2)}) copy-start(bf16[1024,1024]{1,0:T(8,128)(2,1)} %refs_2_.3) | copy-start | bytes 6291460
  38.7 20.8 %copy-start.27 = (f32[128]{0:T(128)S(1)}, f32[128]{0:T(128)}, u32[]{:S(2)}) copy-start(f32[128]{0:T(128)} %param.35) | copy-start | bytes 1540
  38.7 20.8 %copy-start.28 = (f32[8]{0:T(128)S(1)}, f32[8]{0:T(128)}, u32[]{:S(2)}) copy-start(f32[8]{0:T(128)} %param.34) | copy-start | bytes 100
  38.8 10.7 %collective-permute-start.4 = (bf16[272,256]{1,0:T(8,128)(2,1)S(1)}, bf16[272,256]{1,0:T(8,128)(2,1)S(1)}, u32[]{:S(2)}, u32[]{:S(2)}) collective-permute-start(bf16[272,256]{1,0:T(8,128)(2,1)S(1)} %get-tuple-element.36), channel_id=1, source_target_pairs={{0,4},{4,0},{8,12},{12,8},{1,5},{5,1},{9,13},{13,9},{2,6},{6,2},{1... | collective-permute-start | bytes 417800 | tf_op jit(solution)/shard_map/ppermute | solution.py:452
  39.0 13.2 %collective-permute-start.1 = (bf16[256,256]{1,0:T(8,128)(2,1)S(1)}, bf16[256,256]{1,0:T(8,128)(2,1)S(1)}, u32[]{:S(2)}, u32[]{:S(2)}) collective-permute-start(bf16[256,256]{1,0:T(8,128)(2,1)S(1)} %get-tuple-element.28.refs_0_), channel_id=1, source_target_pairs={{0,8},{4,12},{8,0},{12,4},{1,9},{5,13},{9,1},{13,5},{2,10},{6,14},... | collective-permute-start | bytes 393224 | tf_op jit(solution)/shard_map/ppermute | solution.py:452
  39.0 16.0 %collective-permute-start.9 = (bf16[256,256]{1,0:T(8,128)(2,1)S(1)}, bf16[256,256]{1,0:T(8,128)(2,1)S(1)}, u32[]{:S(2)}, u32[]{:S(2)}) collective-permute-start(bf16[256,256]{1,0:T(8,128)(2,1)S(1)} %shard_map.197.refs_0_), channel_id=1, source_target_pairs={{0,4},{4,0},{8,12},{12,8},{1,5},{5,1},{9,13},{13,9},{2,6},{6,2},{1... | collective-permute-start | bytes 393224 | tf_op jit(solution)/shard_map/ppermute | solution.py:452
  43.5 16.0 %collective-permute-start.11 = (bf16[256,256]{1,0:T(8,128)(2,1)S(1)}, bf16[256,256]{1,0:T(8,128)(2,1)S(1)}, u32[]{:S(2)}, u32[]{:S(2)}) collective-permute-start(bf16[256,256]{1,0:T(8,128)(2,1)S(1)} %collective-permute-done.10.refs_2_), channel_id=1, source_target_pairs={{0,4},{4,0},{8,12},{12,8},{1,5},{5,1},{9,13},{13,9},{2,6},{6,2},{1... | collective-permute-start | bytes 393224 | tf_op jit(solution)/shard_map/ppermute | solution.py:452
  48.9 12.2 %collective-permute-start.16 = (bf16[128,512]{1,0:T(8,128)(2,1)S(1)}, bf16[128,512]{1,0:T(8,128)(2,1)S(1)}, u32[]{:S(2)}, u32[]{:S(2)}) collective-permute-start(bf16[128,512]{1,0:T(8,128)(2,1)S(1)} %shard_map.200), channel_id=1, source_target_pairs={{0,2},{2,0},{1,3},{3,1},{4,6},{6,4},{5,7},{7,5},{8,10},{10,8},{9,1... | collective-permute-start | bytes 393224 | tf_op jit(solution)/shard_map/ppermute | solution.py:456
  49.5 18.6 %copy-start = (bf16[2048,1024]{1,0:T(8,128)(2,1)S(1)}, bf16[2048,1024]{1,0:T(8,128)(2,1)}, u32[]{:S(2)}) copy-start(bf16[2048,1024]{1,0:T(8,128)(2,1)} %refs_3_.3) | copy-start | bytes 12582916
  50.5 12.8 %collective-permute-start.5 = (bf16[272,256]{1,0:T(8,128)(2,1)S(1)}, bf16[272,256]{1,0:T(8,128)(2,1)S(1)}, u32[]{:S(2)}, u32[]{:S(2)}) collective-permute-start(bf16[272,256]{1,0:T(8,128)(2,1)S(1)} %get-tuple-element.39), channel_id=1, source_target_pairs={{0,8},{4,12},{8,0},{12,4},{1,9},{5,13},{9,1},{13,5},{2,10},{6,14},... | collective-permute-start | bytes 417800 | tf_op jit(solution)/shard_map/ppermute | solution.py:452
  52.2 14.8 %collective-permute-start = (bf16[256,256]{1,0:T(8,128)(2,1)S(1)}, bf16[256,256]{1,0:T(8,128)(2,1)S(1)}, u32[]{:S(2)}, u32[]{:S(2)}) collective-permute-start(bf16[256,256]{1,0:T(8,128)(2,1)S(1)} %get-tuple-element.28.refs_0_), channel_id=1, source_target_pairs={{0,4},{4,0},{8,12},{12,8},{1,5},{5,1},{9,13},{13,9},{2,6},{6,2},{1... | collective-permute-start | bytes 393224 | tf_op jit(solution)/shard_map/ppermute | solution.py:452
  55.0 12.0 %collective-permute-start.2 = (bf16[256,256]{1,0:T(8,128)(2,1)S(1)}, bf16[256,256]{1,0:T(8,128)(2,1)S(1)}, u32[]{:S(2)}, u32[]{:S(2)}) collective-permute-start(bf16[256,256]{1,0:T(8,128)(2,1)S(1)} %collective-permute-done.1.refs_2_), channel_id=1, source_target_pairs={{0,4},{4,0},{8,12},{12,8},{1,5},{5,1},{9,13},{13,9},{2,6},{6,2},{1... | collective-permute-start | bytes 393224 | tf_op jit(solution)/shard_map/ppermute | solution.py:452
  60.5 3.5 %collective-permute-start.12 = (bf16[128,256]{1,0:T(8,128)(2,1)S(1)}, bf16[128,256]{1,0:T(8,128)(2,1)S(1)}, u32[]{:S(2)}, u32[]{:S(2)}) collective-permute-start(bf16[128,256]{1,0:T(8,128)(2,1)S(1)} %shard_map.198), channel_id=1, source_target_pairs={{0,2},{2,0},{1,3},{3,1},{4,6},{6,4},{5,7},{7,5},{8,10},{10,8},{9,1... | collective-permute-start | bytes 196616 | tf_op jit(solution)/shard_map/ppermute | solution.py:456
  61.1 6.9 %collective-permute-start.17 = (bf16[128,512]{1,0:T(8,128)(2,1)S(1)}, bf16[128,512]{1,0:T(8,128)(2,1)S(1)}, u32[]{:S(2)}, u32[]{:S(2)}) collective-permute-start(bf16[128,512]{1,0:T(8,128)(2,1)S(1)} %collective-permute-done.16.refs_2_), channel_id=1, source_target_pairs={{0,1},{1,0},{2,3},{3,2},{4,5},{5,4},{6,7},{7,6},{8,9},{9,8},{10,11... | collective-permute-start | bytes 393224 | tf_op jit(solution)/shard_map/ppermute | solution.py:456
  63.6 5.7 %collective-permute-start.6 = (bf16[128,512]{1,0:T(8,128)(2,1)S(1)}, bf16[128,512]{1,0:T(8,128)(2,1)S(1)}, u32[]{:S(2)}, u32[]{:S(2)}) collective-permute-start(bf16[128,512]{1,0:T(8,128)(2,1)S(1)} %shard_map.195.refs_1_), channel_id=1, source_target_pairs={{0,1},{1,0},{2,3},{3,2},{4,5},{5,4},{6,7},{7,6},{8,9},{9,8},{10,11... | collective-permute-start | bytes 393224 | tf_op jit(solution)/shard_map/ppermute | solution.py:456
  64.0 4.1 %collective-permute-start.13 = (bf16[128,256]{1,0:T(8,128)(2,1)S(1)}, bf16[128,256]{1,0:T(8,128)(2,1)S(1)}, u32[]{:S(2)}, u32[]{:S(2)}) collective-permute-start(bf16[128,256]{1,0:T(8,128)(2,1)S(1)} %collective-permute-done.12.refs_0_), channel_id=1, source_target_pairs={{0,1},{1,0},{2,3},{3,2},{4,5},{5,4},{6,7},{7,6},{8,9},{9,8},{10,11... | collective-permute-start | bytes 196616 | tf_op jit(solution)/shard_map/ppermute | solution.py:456
  67.9 1.3 %collective-permute-start.3 = (bf16[128,256]{1,0:T(8,128)(2,1)S(1)}, bf16[128,256]{1,0:T(8,128)(2,1)S(1)}, u32[]{:S(2)}, u32[]{:S(2)}) collective-permute-start(bf16[128,256]{1,0:T(8,128)(2,1)S(1)} %shard_map.193.refs_0_), channel_id=1, source_target_pairs={{0,1},{1,0},{2,3},{3,2},{4,5},{5,4},{6,7},{7,6},{8,9},{9,8},{10,11... | collective-permute-start | bytes 196616 | tf_op jit(solution)/shard_map/ppermute | solution.py:456
  (23 other events, 62.8 us)

commit v4 on v3

--- a/solution.py
+++ b/solution.py
@@ -175,9 +175,7 @@
     kv = jax.ShapeDtypeStruct((2 * dims.rows, dims.heads * dims.ca), BF16)
     normed = jax.ShapeDtypeStruct(values.shape, BF16)
     outs = [kv] + ([normed] if raw else [])
-    return call(
-        body, 2, 12, args, [whole(a.shape) for a in args], outs, work_scratch(dims, weights)
-    )
+    return call(body, 2, 12, args, [whole(a.shape) for a in args], outs, work_scratch(dims, weights))
 
 
 def slot_outputs(dims):
@@ -288,42 +286,49 @@
         send_out[at : at + 1, :ck] = decay[:, of].astype(BF16)
 
 
-def rest_work(dims, slot, values, gain, weights, consts):
+def rest_work(dims, slot, values, gain, weights, consts, after):
     layout = (dims.ca // 128, dims.ck // 128, dims.ck // 128, dims.cv // 128)
     raw = gain is not None
-    n_out, n_in = len(slot_outputs(dims)), 1 + len(weights) + len(consts)
-    args = (values, *weights, *consts) + ((gain,) if raw else ())
+    n_out, n_in, n_v = len(slot_outputs(dims)), len(values) + len(weights) + len(consts), len(values)
+    args = (*values, *weights, *consts, *after) + ((gain,) if raw else ())
 
     def body(*refs):
-        inputs, refs = refs[:n_in], refs[n_in:]
-        tok, raws, consts_v = inputs[0], inputs[1 : 1 + len(weights)], inputs[1 + len(weights) :]
+        inputs, refs = refs[:n_in], refs[n_in + len(after) :]
+        toks, raws, consts_v = inputs[:n_v], inputs[n_v : n_v + len(weights)], inputs[n_v + len(weights) :]
         if raw:
             gain_ref, refs = refs[0], refs[1:]
             outs, normed, (acc, w_out, wide, up_wide) = refs[:n_out], refs[n_out], refs[n_out + 1 :]
-            normed[...] = rms(tok[...].astype(F32), gain_ref[...]).astype(BF16)
+            for i, tok in enumerate(toks):
+                size = tok.shape[0]
+                at = pl.multiple_of(lax.rem(lax.axis_index("tp") + i, n_v) * size, size) if n_v > 1 else 0
+                normed[pl.ds(at, size), :] = rms(tok[...].astype(F32), gain_ref[...]).astype(BF16)
         else:
             outs, (acc, w_out, wide, up_wide) = refs[:n_out], refs[n_out:]
-            normed = tok
+            normed = toks[0]
         acc[...] = projected(normed, raws, layout, dims, w_out, wide)
         down, init, up, bias, retain, query_gain = consts_v
         low = dot(normed[...], down[...], ((1,), (1,))).astype(BF16)
         local_part(dims, slot, acc, low, init, up, up_wide, bias, retain, query_gain, outs)
 
-    outs = slot_outputs(dims) + ([jax.ShapeDtypeStruct(values.shape, BF16)] if raw else [])
+    outs = slot_outputs(dims) + ([jax.ShapeDtypeStruct((dims.rows, dims.model), BF16)] if raw else [])
     scratch = work_scratch(dims, weights) + [pltpu.VMEM(consts[2].shape, F32)]
     return call(body, 4, 18, args, [whole(a.shape) for a in args], outs, scratch)
 
 
-def linger(x):
-    def body(x_ref, out):
-        out[...] = x_ref[...]
-
-    return call(body, LINGER_US, 1, (x,), [whole(x.shape)], jax.ShapeDtypeStruct(x.shape, x.dtype), [])
+def own_part(dims, tokens):
+    size = dims.rows // dims.tp_size
+
+    def body(tok, out):
+        at = pl.multiple_of(lax.axis_index("tp") * size, size)
+        out[...] = tok[pl.ds(at, size), :]
+
+    out = jax.ShapeDtypeStruct((size, dims.model), BF16)
+    return call(body, LINGER_US, 2, (tokens,), [whole(tokens.shape)], out, [])
 
 
 def combine(dims, bit, state, decay, prefix, prefix_decay, received):
     hd, ck, cv = dims.heads, dims.ck, dims.cv
-    begun = prefix_decay is not None
+    begun, more = prefix_decay is not None, bit * 4 < dims.sp_size
 
     def body(*refs):
         if begun:
@@ -331,7 +336,8 @@
         else:
             st, dec, pre, rec, send_out, st_out, dec_out, pre_out, pre_dec_out = refs
         upper = lax.rem(lax.axis_index("sp") // bit, 2) == 1
-        send_out[hd * ck :, :] = jnp.zeros((16, cv), BF16)
+        if more:
+            send_out[hd * ck :, :] = jnp.zeros((16, cv), BF16)
         for h in range(hd):
             at = slice(h * ck, (h + 1) * ck)
             other = rec[at, :].astype(F32)
@@ -345,7 +351,7 @@
             send_out[at, :] = total.astype(BF16)
             both = mine_dec * other_dec
             dec_out[at, :] = both
-            if bit * 4 < dims.sp_size:
+            if more:
                 send_out[hd * ck + h : hd * ck + h + 1, :ck] = jnp.transpose(both[:, :128])[:1, :].astype(BF16)
             if begun:
                 pre_out[at, :] = pre[at, :] + jnp.where(upper, pre_dec[at, :] * other, 0.0)
@@ -362,7 +368,7 @@
         6,
         args,
         [whole(a.shape) for a in args],
-        [jax.ShapeDtypeStruct((hd * ck + 16, cv), BF16), full, full, full, full],
+        [jax.ShapeDtypeStruct((hd * ck + (16 if more else 0), cv), BF16), full, full, full, full],
         [],
     )
 
@@ -456,6 +462,12 @@
     return lax.ppermute(x, axis, [(i, (i + by) % size) for i in range(size)])
 
 
+def shift_both(x, j, i, fs_size, tp_size):
+    places = [(f, t) for f in range(fs_size) for t in range(tp_size)]
+    perm = [(f * tp_size + t, (f - j) % fs_size * tp_size + (t - i) % tp_size) for f, t in places]
+    return lax.ppermute(x, ("fs", "tp"), perm)
+
+
 def low_bit(m):
     return m & -m
 
@@ -497,7 +509,11 @@
     kg = key_gain.reshape(-1, key_gain.shape[-1])
     up = decay_up.reshape(-1, decay_up.shape[-1])
     init = init_state.reshape(-1, dims.cv)
-    token_slots = [own] + [shift(own, "fs", j, fs_size) for j in range(1, fs_size)]
+    mine = own_part(dims, own)
+    token_slots = [(own,)]
+    for j in range(1, fs_size):
+        part = shift(mine, "fs", j, fs_size)
+        token_slots.append((part, *(shift(part, "tp", -i, tp_size) for i in range(1, tp_size))))
     retains = [retain_own] + [shift(retain_own, "fs", j, fs_size) for j in range(1, fs_size)]
 
     def keys_of_all(kv):
@@ -522,19 +538,16 @@
     blocks, outs, states = [], [], []
     for j in range(fs_size):
         consts = (decay_down.T, init, up, decay_bias, retains[j], query_gain.reshape(1, -1))
-        if j == 0:
-            kv, normed = keys_work(dims, own, linger(gain), kv_weights, kg)
-            out = rest_work(dims, j, normed, None, rest_weights, consts)
-        else:
-            *out, normed = rest_work(dims, j, token_slots[j], gain, rest_weights, consts)
-            (kv,) = keys_work(dims, normed, None, kv_weights, kg)
+        after = () if j else (mine,)
+        *out, normed = rest_work(dims, j, token_slots[j], gain, rest_weights, consts, after)
+        (kv,) = keys_work(dims, normed, None, kv_weights, kg)
         blocks.append(keys_of_all(kv))
         outs.append(out)
         states.append(entering(*out[3:]))
 
     mix, sg, lam = mix_gain.reshape(1, -1), state_gain.reshape(1, -1), diff_lambda.reshape(1, -1)
     weights = (output_attend, output_linear)
-    early, late, last = [], [], []
+    early, late = [], []
     for j in range(fs_size):
         q_unit, reach, inside = outs[j][:3]
         bit, *entered = states[j]
@@ -543,15 +556,19 @@
                 value = attend(dims, blocks[j], q_unit, mix, lam)
             else:
                 value = recall(dims, bit, reach, inside, *entered, sg)
+            arrived = [value]
             if j:
-                value = shift(value, "fs", -j, fs_size)
-            arrived = [value]
-            arrived += [shift(value, "tp", -i, tp_size) for i in range(1, tp_size)]
-            groups = [early] * tp_size if j else [late] + [last] * (tp_size - 1)
-            for i, group in enumerate(groups):
-                group.append((arrived[i], which, j, i))
+                arrived = [shift(value, "fs", -j, fs_size)]
+            for i in range(1, tp_size):
+                if j and which == 0:
+                    arrived.append(shift_both(value, j, i, fs_size, tp_size))
+                else:
+                    arrived.append(shift(arrived[0], "tp", -i, tp_size))
+            for i in range(tp_size):
+                soon = i == 0 and (j == 0 or which == 1)
+                (early if soon else late).append((arrived[i], which, j, i))
     total = None
-    groups = [(n, g) for n, g in (("early", early), ("late", late), ("last", last)) if g]
+    groups = [("early", early), ("late", late)]
     for name, group in groups:
         total = project_out(dims, group, weights, total, name == groups[-1][0])
     return total.reshape(1, rows, -1)

time: 71.6 us -> 67.2 us (0.939)
  the two profiles are of different devices: /device:TPU:31 before, /device:TPU:0 now
where the time goes in v4:
time: 67.2 us; the launch traced here: 67.1 us
  waiting for transfers between devices  30 us (45%)
  starting transfers between devices  19.2 us (29%)
  Pallas kernels  16.5 us (25%)
  local copies, waits for them, and re-layouts  1.13 us (2%)
    ppermute x10, waiting for transfers between devices, swap(): return lax.ppermute(x, axis, [(i, i ^ bit) for i in range(size)])  18.2 us
    pallas_call x13, Pallas kernels, call(): pl.pallas_call(body, in_specs=in_specs, out_specs=specs, out_shape=outs,...  16.5 us
    ppermute x10, starting transfers between devices, swap(): return lax.ppermute(x, axis, [(i, i ^ bit) for i in range(size)])  10.4 us
    ppermute x8, waiting for transfers between devices, shift(): return lax.ppermute(x, axis, [(i, (i + by) % size) for i in range(size)])  9.7 us
    ppermute x8, starting transfers between devices, shift(): return lax.ppermute(x, axis, [(i, (i + by) % size) for i in range(size)])  7.56 us
    ppermute x1, waiting for transfers between devices, shift_both(): return lax.ppermute(x, ('fs', 'tp'), perm)  2.09 us
  transfers between devices with their start and end apart: 19, of which 11 were waited for; matrix products, arithmetic and copies ran while one was open for 0% of the time, Pallas kernels for 17%

profile of v4, /device:TPU:0, one launch (start us, length us, event | category | flops | bytes accessed | tf_op | source)
XLA Modules:
  0.0 67.1 jit_solution(5207305553114426128)
XLA Ops:
  0.0 1.0 %copy-done.10 = bf16[1,128,2048]{2,1,0:T(8,128)(2,1)S(1)} copy-done((bf16[1,128,2048]{2,1,0:T(8,128)(2,1)S(1)}, bf16[1,128,2048]{2,1,0:T(8,128)(2,1)}, u32[]{:S(2)}) %copy-start.10) | copy-done | bytes 524312
  1.2 3.0 %collective-permute-start.7 = (bf16[64,2048]{1,0:T(8,128)(2,1)S(1)}, bf16[64,2048]{1,0:T(8,128)(2,1)S(1)}, u32[]{:S(2)}, u32[]{:S(2)}) collective-permute-start(bf16[64,2048]{1,0:T(8,128)(2,1)S(1)} %shard_map.190.refs_11_), channel_id=1, source_target_pairs={{0,2},{2,0},{1,3},{3,1},{4,6},{6,4},{5,7},{7,5},{8,10},{10,8},{9,1... | collective-permute-start | bytes 786440 | tf_op jit(solution)/shard_map/ppermute | solution.py:462
  4.2 6.3 %collective-permute-done.7.refs_0_ = bf16[64,2048]{1,0:T(8,128)(2,1)S(1)} collective-permute-done((bf16[64,2048]{1,0:T(8,128)(2,1)S(1)}, bf16[64,2048]{1,0:T(8,128)(2,1)S(1)}, u32[]{:S(2)}, u32[]{:S(2)}) %collective-permute-start.7) | collective-permute-done | bytes 262176 | tf_op jit(solution)/shard_map/ppermute | solution.py:462
  10.5 1.7 %collective-permute-start.9 = (f32[8,128]{1,0:T(8,128)S(1)}, f32[8,128]{1,0:T(8,128)S(1)}, u32[]{:S(2)}, u32[]{:S(2)}) collective-permute-start(f32[8,128]{1,0:T(8,128)S(1)} %bitcast.50), channel_id=1, source_target_pairs={{0,2},{2,0},{1,3},{3,1},{4,6},{6,4},{5,7},{7,5},{8,10},{10,8},{9,1... | collective-permute-start | bytes 12296 | tf_op jit(solution)/shard_map/ppermute | solution.py:462
  12.2 1.9 %collective-permute-done.9.refs_10_ = f32[8,128]{1,0:T(8,128)S(1)} collective-permute-done((f32[8,128]{1,0:T(8,128)S(1)}, f32[8,128]{1,0:T(8,128)S(1)}, u32[]{:S(2)}, u32[]{:S(2)}) %collective-permute-start.9) | collective-permute-done | bytes 4128 | tf_op jit(solution)/shard_map/ppermute | solution.py:462
  14.2 3.9 %shard_map.196 = (bf16[128,256]{1,0:T(8,128)(2,1)S(1)}, bf16[128,256]{1,0:T(8,128)(2,1)S(1)}, f32[128,512]{1,0:T(8,128)S(1)}, bf16[272,256]{1,0:T(8,128)(2,1)S(1...) custom-call(bf16[64,2048]{1,0:T(8,128)(2,1)S(1)} %collective-permute, ...), custom_call_target="tpu_custom_call" | custom-call | flops 800000000 | tf_op jit(solution)/shard_map/pallas_call | solution.py:111
  18.2 1.9 %collective-permute-start.15 = (bf16[272,256]{1,0:T(8,128)(2,1)S(1)}, bf16[272,256]{1,0:T(8,128)(2,1)S(1)}, u32[]{:S(2)}, u32[]{:S(2)}) collective-permute-start(bf16[272,256]{1,0:T(8,128)(2,1)S(1)} %get-tuple-element.45), channel_id=1, source_target_pairs={{0,4},{4,0},{8,12},{12,8},{1,5},{5,1},{9,13},{13,9},{2,6},{6,2},{1... | collective-permute-start | bytes 417800 | tf_op jit(solution)/shard_map/ppermute | solution.py:458
  20.1 3.9 %shard_map.191 = (bf16[128,256]{1,0:T(8,128)(2,1)S(1)}, bf16[128,256]{1,0:T(8,128)(2,1)S(1)}, f32[128,512]{1,0:T(8,128)S(1)}, bf16[272,256]{1,0:T(8,128)(2,1)S(1...) custom-call(bf16[128,2048]{1,0:T(8,128)(2,1)S(1)} %bitcast.41, ...), custom_call_target="tpu_custom_call" | custom-call | flops 800000000 | tf_op jit(solution)/shard_map/pallas_call | solution.py:111
  24.2 1.2 %shard_map.192.refs_0_ = bf16[256,256]{1,0:T(8,128)(2,1)S(1)} custom-call(bf16[128,2048]{1,0:T(8,128)(2,1)S(1)} %get-tuple-element.27.refs_0_, bf16[4096,128]{1,0:T(8,128)(2,1)S(1)} %bitcast.32, bf16[4096,128]{1,0:T(8,128)(2,1)S(1)} %bitcast.34, f32[16,64]{1,0:T(8,128)S(1)} %bitcast.46), custom_call_target="tpu_custom_call" | custom-call | flops 400000000 | tf_op jit(solution)/shard_map/pallas_call | solution.py:111
  25.4 2.9 %collective-permute-start.1 = (bf16[256,256]{1,0:T(8,128)(2,1)S(1)}, bf16[256,256]{1,0:T(8,128)(2,1)S(1)}, u32[]{:S(2)}, u32[]{:S(2)}) collective-permute-start(bf16[256,256]{1,0:T(8,128)(2,1)S(1)} %shard_map.192.refs_0_), channel_id=1, source_target_pairs={{0,8},{4,12},{8,0},{12,4},{1,9},{5,13},{9,1},{13,5},{2,10},{6,14},... | collective-permute-start | bytes 393224 | tf_op jit(solution)/shard_map/ppermute | solution.py:458
  29.5 1.5 %collective-permute-done.4.refs_3_ = bf16[272,256]{1,0:T(8,128)(2,1)S(1)} collective-permute-done((bf16[272,256]{1,0:T(8,128)(2,1)S(1)}, bf16[272,256]{1,0:T(8,128)(2,1)S(1)}, u32[]{:S(2)}, u32[]{:S(2)}) %collective-permute-start.4) | collective-permute-done | bytes 139296 | tf_op jit(solution)/shard_map/ppermute | solution.py:458
  32.0 1.7 %collective-permute-start.5 = (bf16[256,256]{1,0:T(8,128)(2,1)S(1)}, bf16[256,256]{1,0:T(8,128)(2,1)S(1)}, u32[]{:S(2)}, u32[]{:S(2)}) collective-permute-start(bf16[256,256]{1,0:T(8,128)(2,1)S(1)} %get-tuple-element.37), channel_id=1, source_target_pairs={{0,8},{4,12},{8,0},{12,4},{1,9},{5,13},{9,1},{13,5},{2,10},{6,14},... | collective-permute-start | bytes 393224 | tf_op jit(solution)/shard_map/ppermute | solution.py:458
  33.7 1.2 %shard_map.197.refs_0_ = bf16[256,256]{1,0:T(8,128)(2,1)S(1)} custom-call(bf16[128,2048]{1,0:T(8,128)(2,1)S(1)} %get-tuple-element.38.refs_0_, bf16[4096,128]{1,0:T(8,128)(2,1)S(1)} %bitcast.33, bf16[4096,128]{1,0:T(8,128)(2,1)S(1)} %bitcast.35, f32[16,64]{1,0:T(8,128)S(1)} %bitcast.47), custom_call_target="tpu_custom_call" | custom-call | flops 400000000 | tf_op jit(solution)/shard_map/pallas_call | solution.py:111
  34.9 1.2 %collective-permute-start.11 = (bf16[256,256]{1,0:T(8,128)(2,1)S(1)}, bf16[256,256]{1,0:T(8,128)(2,1)S(1)}, u32[]{:S(2)}, u32[]{:S(2)}) collective-permute-start(bf16[256,256]{1,0:T(8,128)(2,1)S(1)} %shard_map.197.refs_0_), channel_id=1, source_target_pairs={{0,8},{4,12},{8,0},{12,4},{1,9},{5,13},{9,1},{13,5},{2,10},{6,14},... | collective-permute-start | bytes 393224 | tf_op jit(solution)/shard_map/ppermute | solution.py:458
  36.5 9.1 %collective-permute-done.16.rec = bf16[256,256]{1,0:T(8,128)(2,1)S(1)} collective-permute-done((bf16[256,256]{1,0:T(8,128)(2,1)S(1)}, bf16[256,256]{1,0:T(8,128)(2,1)S(1)}, u32[]{:S(2)}, u32[]{:S(2)}) %collective-permute-start.16) | collective-permute-done | bytes 131104 | tf_op jit(solution)/shard_map/ppermute | solution.py:458
  45.9 1.7 %collective-permute-start.17 = (bf16[128,512]{1,0:T(8,128)(2,1)S(1)}, bf16[128,512]{1,0:T(8,128)(2,1)S(1)}, u32[]{:S(2)}, u32[]{:S(2)}) collective-permute-start(bf16[128,512]{1,0:T(8,128)(2,1)S(1)} %shard_map.200), channel_id=1, source_target_pairs={{0,2},{2,0},{1,3},{3,1},{4,6},{6,4},{5,7},{7,5},{8,10},{10,8},{9,1... | collective-permute-start | bytes 393224 | tf_op jit(solution)/shard_map/ppermute | solution.py:462
  48.4 1.2 %collective-permute-start.10 = (bf16[256,256]{1,0:T(8,128)(2,1)S(1)}, bf16[256,256]{1,0:T(8,128)(2,1)S(1)}, u32[]{:S(2)}, u32[]{:S(2)}) collective-permute-start(bf16[256,256]{1,0:T(8,128)(2,1)S(1)} %shard_map.197.refs_0_), channel_id=1, source_target_pairs={{0,4},{4,0},{8,12},{12,8},{1,5},{5,1},{9,13},{13,9},{2,6},{6,2},{1... | collective-permute-start | bytes 393224 | tf_op jit(solution)/shard_map/ppermute | solution.py:458
  52.1 1.9 %collective-permute-done.2.refs_3_ = bf16[256,256]{1,0:T(8,128)(2,1)S(1)} collective-permute-done((bf16[256,256]{1,0:T(8,128)(2,1)S(1)}, bf16[256,256]{1,0:T(8,128)(2,1)S(1)}, u32[]{:S(2)}, u32[]{:S(2)}) %collective-permute-start.2) | collective-permute-done | bytes 131104 | tf_op jit(solution)/shard_map/ppermute | solution.py:458
  55.0 1.8 %collective-permute-done.10.refs_1_ = bf16[256,256]{1,0:T(8,128)(2,1)S(1)} collective-permute-done((bf16[256,256]{1,0:T(8,128)(2,1)S(1)}, bf16[256,256]{1,0:T(8,128)(2,1)S(1)}, u32[]{:S(2)}, u32[]{:S(2)}) %collective-permute-start.10) | collective-permute-done | bytes 131104 | tf_op jit(solution)/shard_map/ppermute | solution.py:458
  56.8 2.1 %collective-permute-done.12.refs_3_ = bf16[256,256]{1,0:T(8,128)(2,1)S(1)} collective-permute-done((bf16[256,256]{1,0:T(8,128)(2,1)S(1)}, bf16[256,256]{1,0:T(8,128)(2,1)S(1)}, u32[]{:S(2)}, u32[]{:S(2)}) %collective-permute-start.12) | collective-permute-done | bytes 131104 | tf_op jit(solution)/shard_map/ppermute | solution.py:458
  59.8 1.2 %collective-permute-start.14 = (bf16[128,256]{1,0:T(8,128)(2,1)S(1)}, bf16[128,256]{1,0:T(8,128)(2,1)S(1)}, u32[]{:S(2)}, u32[]{:S(2)}) collective-permute-start(bf16[128,256]{1,0:T(8,128)(2,1)S(1)} %shard_map.198), channel_id=1, source_target_pairs={{0,3},{1,2},{2,1},{3,0},{4,7},{5,6},{6,5},{7,4},{8,11},{9,10},{10,... | collective-permute-start | bytes 196616 | tf_op jit(solution)/shard_map/ppermute | solution.py:468
  62.1 2.1 %collective-permute-done.14.refs_3_ = bf16[128,256]{1,0:T(8,128)(2,1)S(1)} collective-permute-done((bf16[128,256]{1,0:T(8,128)(2,1)S(1)}, bf16[128,256]{1,0:T(8,128)(2,1)S(1)}, u32[]{:S(2)}, u32[]{:S(2)}) %collective-permute-start.14) | collective-permute-done | bytes 65568 | tf_op jit(solution)/shard_map/ppermute | solution.py:468
  64.2 1.5 %collective-permute-done.13.refs_2_ = bf16[128,256]{1,0:T(8,128)(2,1)S(1)} collective-permute-done((bf16[128,256]{1,0:T(8,128)(2,1)S(1)}, bf16[128,256]{1,0:T(8,128)(2,1)S(1)}, u32[]{:S(2)}, u32[]{:S(2)}) %collective-permute-start.13) | collective-permute-done | bytes 65568 | tf_op jit(solution)/shard_map/ppermute | solution.py:462
  65.7 1.4 %shard_map.202 = bf16[128,1024]{1,0:T(8,128)(2,1)} custom-call(bf16[128,256]{1,0:T(8,128)(2,1)S(1)} %collective-permute-done.3.refs_0_, bf16[128,512]{1,0:T(8,128)(2,1)S(1)} %collective-permute-done.6.refs_1_, bf16[128,256]{1,0:T(8,128)(2,1)S(1)} %collective-permute-done.13.refs_2_, bf16[128,256]{1,0:T(8,128)(2,1)S(1)} %collective-permute-done.14.refs_3_, ...), custom_call_target="tpu_custom_call" | custom-call | flops 200000000 | tf_op jit(solution)/shard_map/pallas_call | solution.py:111
  (69 shorter events, 9.2 us)
Async XLA Ops:
  1.2 9.3 %collective-permute-start.7 = (bf16[64,2048]{1,0:T(8,128)(2,1)S(1)}, bf16[64,2048]{1,0:T(8,128)(2,1)S(1)}, u32[]{:S(2)}, u32[]{:S(2)}) collective-permute-start(bf16[64,2048]{1,0:T(8,128)(2,1)S(1)} %shard_map.190.refs_11_), channel_id=1, source_target_pairs={{0,2},{2,0},{1,3},{3,1},{4,6},{6,4},{5,7},{7,5},{8,10},{10,8},{9,1... | collective-permute-start | bytes 786440 | tf_op jit(solution)/shard_map/ppermute | solution.py:462
  10.5 3.6 %collective-permute-start.8 = (bf16[64,2048]{1,0:T(8,128)(2,1)S(1)}, bf16[64,2048]{1,0:T(8,128)(2,1)S(1)}, u32[]{:S(2)}, u32[]{:S(2)}) collective-permute-start(bf16[64,2048]{1,0:T(8,128)(2,1)S(1)} %collective-permute-done.7.refs_0_), channel_id=1, source_target_pairs={{0,1},{1,0},{2,3},{3,2},{4,5},{5,4},{6,7},{7,6},{8,9},{9,8},{10,11... | collective-permute-start | bytes 786440 | tf_op jit(solution)/shard_map/ppermute | solution.py:462
  10.5 3.6 %collective-permute-start.9 = (f32[8,128]{1,0:T(8,128)S(1)}, f32[8,128]{1,0:T(8,128)S(1)}, u32[]{:S(2)}, u32[]{:S(2)}) collective-permute-start(f32[8,128]{1,0:T(8,128)S(1)} %bitcast.50), channel_id=1, source_target_pairs={{0,2},{2,0},{1,3},{3,1},{4,6},{6,4},{5,7},{7,5},{8,10},{10,8},{9,1... | collective-permute-start | bytes 12296 | tf_op jit(solution)/shard_map/ppermute | solution.py:462
  18.2 10.1 %collective-permute-start.15 = (bf16[272,256]{1,0:T(8,128)(2,1)S(1)}, bf16[272,256]{1,0:T(8,128)(2,1)S(1)}, u32[]{:S(2)}, u32[]{:S(2)}) collective-permute-start(bf16[272,256]{1,0:T(8,128)(2,1)S(1)} %get-tuple-element.45), channel_id=1, source_target_pairs={{0,4},{4,0},{8,12},{12,8},{1,5},{5,1},{9,13},{13,9},{2,6},{6,2},{1... | collective-permute-start | bytes 417800 | tf_op jit(solution)/shard_map/ppermute | solution.py:458
  24.0 7.0 %collective-permute-start.4 = (bf16[272,256]{1,0:T(8,128)(2,1)S(1)}, bf16[272,256]{1,0:T(8,128)(2,1)S(1)}, u32[]{:S(2)}, u32[]{:S(2)}) collective-permute-start(bf16[272,256]{1,0:T(8,128)(2,1)S(1)} %get-tuple-element.34), channel_id=1, source_target_pairs={{0,4},{4,0},{8,12},{12,8},{1,5},{5,1},{9,13},{13,9},{2,6},{6,2},{1... | collective-permute-start | bytes 417800 | tf_op jit(solution)/shard_map/ppermute | solution.py:458
  25.4 22.2 %collective-permute-start.1 = (bf16[256,256]{1,0:T(8,128)(2,1)S(1)}, bf16[256,256]{1,0:T(8,128)(2,1)S(1)}, u32[]{:S(2)}, u32[]{:S(2)}) collective-permute-start(bf16[256,256]{1,0:T(8,128)(2,1)S(1)} %shard_map.192.refs_0_), channel_id=1, source_target_pairs={{0,8},{4,12},{8,0},{12,4},{1,9},{5,13},{9,1},{13,5},{2,10},{6,14},... | collective-permute-start | bytes 393224 | tf_op jit(solution)/shard_map/ppermute | solution.py:458
  29.4 16.3 %collective-permute-start.16 = (bf16[256,256]{1,0:T(8,128)(2,1)S(1)}, bf16[256,256]{1,0:T(8,128)(2,1)S(1)}, u32[]{:S(2)}, u32[]{:S(2)}) collective-permute-start(bf16[256,256]{1,0:T(8,128)(2,1)S(1)} %get-tuple-element.48), channel_id=1, source_target_pairs={{0,8},{4,12},{8,0},{12,4},{1,9},{5,13},{9,1},{13,5},{2,10},{6,14},... | collective-permute-start | bytes 393224 | tf_op jit(solution)/shard_map/ppermute | solution.py:458
  30.9 14.7 %copy-start.16 = (f32[256]{0:T(256)S(1)}, f32[256]{0:T(256)}, u32[]{:S(2)}) copy-start(f32[256]{0:T(256)} %param.36) | copy-start | bytes 3076
  32.0 16.5 %collective-permute-start.5 = (bf16[256,256]{1,0:T(8,128)(2,1)S(1)}, bf16[256,256]{1,0:T(8,128)(2,1)S(1)}, u32[]{:S(2)}, u32[]{:S(2)}) collective-permute-start(bf16[256,256]{1,0:T(8,128)(2,1)S(1)} %get-tuple-element.37), channel_id=1, source_target_pairs={{0,8},{4,12},{8,0},{12,4},{1,9},{5,13},{9,1},{13,5},{2,10},{6,14},... | collective-permute-start | bytes 393224 | tf_op jit(solution)/shard_map/ppermute | solution.py:458
  33.7 20.3 %copy-start.19 = (f32[128]{0:T(128)S(1)}, f32[128]{0:T(128)}, u32[]{:S(2)}) copy-start(f32[128]{0:T(128)} %param.35) | copy-start | bytes 1540
  33.7 20.3 %copy-start.20 = (f32[8]{0:T(128)S(1)}, f32[8]{0:T(128)}, u32[]{:S(2)}) copy-start(f32[8]{0:T(128)} %param.34) | copy-start | bytes 100
  33.7 27.8 %copy-start.1 = (bf16[1024,1024]{1,0:T(8,128)(2,1)S(1)}, bf16[1024,1024]{1,0:T(8,128)(2,1)}, u32[]{:S(2)}) copy-start(bf16[1024,1024]{1,0:T(8,128)(2,1)} %refs_5_.1) | copy-start | bytes 6291460
  34.9 15.7 %collective-permute-start.11 = (bf16[256,256]{1,0:T(8,128)(2,1)S(1)}, bf16[256,256]{1,0:T(8,128)(2,1)S(1)}, u32[]{:S(2)}, u32[]{:S(2)}) collective-permute-start(bf16[256,256]{1,0:T(8,128)(2,1)S(1)} %shard_map.197.refs_0_), channel_id=1, source_target_pairs={{0,8},{4,12},{8,0},{12,4},{1,9},{5,13},{9,1},{13,5},{2,10},{6,14},... | collective-permute-start | bytes 393224 | tf_op jit(solution)/shard_map/ppermute | solution.py:458
  36.2 15.4 %collective-permute-start = (bf16[256,256]{1,0:T(8,128)(2,1)S(1)}, bf16[256,256]{1,0:T(8,128)(2,1)S(1)}, u32[]{:S(2)}, u32[]{:S(2)}) collective-permute-start(bf16[256,256]{1,0:T(8,128)(2,1)S(1)} %shard_map.192.refs_0_), channel_id=1, source_target_pairs={{0,4},{4,0},{8,12},{12,8},{1,5},{5,1},{9,13},{13,9},{2,6},{6,2},{1... | collective-permute-start | bytes 393224 | tf_op jit(solution)/shard_map/ppermute | solution.py:458
  45.6 15.9 %copy-start = (bf16[2048,1024]{1,0:T(8,128)(2,1)S(1)}, bf16[2048,1024]{1,0:T(8,128)(2,1)}, u32[]{:S(2)}) copy-start(bf16[2048,1024]{1,0:T(8,128)(2,1)} %refs_6_.1) | copy-start | bytes 12582916
  45.9 5.7 %collective-permute-start.17 = (bf16[128,512]{1,0:T(8,128)(2,1)S(1)}, bf16[128,512]{1,0:T(8,128)(2,1)S(1)}, u32[]{:S(2)}, u32[]{:S(2)}) collective-permute-start(bf16[128,512]{1,0:T(8,128)(2,1)S(1)} %shard_map.200), channel_id=1, source_target_pairs={{0,2},{2,0},{1,3},{3,1},{4,6},{6,4},{5,7},{7,5},{8,10},{10,8},{9,1... | collective-permute-start | bytes 393224 | tf_op jit(solution)/shard_map/ppermute | solution.py:462
  47.6 6.4 %collective-permute-start.2 = (bf16[256,256]{1,0:T(8,128)(2,1)S(1)}, bf16[256,256]{1,0:T(8,128)(2,1)S(1)}, u32[]{:S(2)}, u32[]{:S(2)}) collective-permute-start(bf16[256,256]{1,0:T(8,128)(2,1)S(1)} %collective-permute-done.1.refs_2_), channel_id=1, source_target_pairs={{0,4},{4,0},{8,12},{12,8},{1,5},{5,1},{9,13},{13,9},{2,6},{6,2},{1... | collective-permute-start | bytes 393224 | tf_op jit(solution)/shard_map/ppermute | solution.py:458
  48.4 8.4 %collective-permute-start.10 = (bf16[256,256]{1,0:T(8,128)(2,1)S(1)}, bf16[256,256]{1,0:T(8,128)(2,1)S(1)}, u32[]{:S(2)}, u32[]{:S(2)}) collective-permute-start(bf16[256,256]{1,0:T(8,128)(2,1)S(1)} %shard_map.197.refs_0_), channel_id=1, source_target_pairs={{0,4},{4,0},{8,12},{12,8},{1,5},{5,1},{9,13},{13,9},{2,6},{6,2},{1... | collective-permute-start | bytes 393224 | tf_op jit(solution)/shard_map/ppermute | solution.py:458
  50.6 8.3 %collective-permute-start.12 = (bf16[256,256]{1,0:T(8,128)(2,1)S(1)}, bf16[256,256]{1,0:T(8,128)(2,1)S(1)}, u32[]{:S(2)}, u32[]{:S(2)}) collective-permute-start(bf16[256,256]{1,0:T(8,128)(2,1)S(1)} %collective-permute-done.11.refs_2_), channel_id=1, source_target_pairs={{0,4},{4,0},{8,12},{12,8},{1,5},{5,1},{9,13},{13,9},{2,6},{6,2},{1... | collective-permute-start | bytes 393224 | tf_op jit(solution)/shard_map/ppermute | solution.py:458
  51.5 10.5 %collective-permute-start.6 = (bf16[128,512]{1,0:T(8,128)(2,1)S(1)}, bf16[128,512]{1,0:T(8,128)(2,1)S(1)}, u32[]{:S(2)}, u32[]{:S(2)}) collective-permute-start(bf16[128,512]{1,0:T(8,128)(2,1)S(1)} %shard_map.195.refs_1_), channel_id=1, source_target_pairs={{0,1},{1,0},{2,3},{3,2},{4,5},{5,4},{6,7},{7,6},{8,9},{9,8},{10,11... | collective-permute-start | bytes 393224 | tf_op jit(solution)/shard_map/ppermute | solution.py:462
  51.6 14.1 %collective-permute-start.18 = (bf16[128,512]{1,0:T(8,128)(2,1)S(1)}, bf16[128,512]{1,0:T(8,128)(2,1)S(1)}, u32[]{:S(2)}, u32[]{:S(2)}) collective-permute-start(bf16[128,512]{1,0:T(8,128)(2,1)S(1)} %collective-permute-done.17.refs_2_), channel_id=1, source_target_pairs={{0,1},{1,0},{2,3},{3,2},{4,5},{5,4},{6,7},{7,6},{8,9},{9,8},{10,11... | collective-permute-start | bytes 393224 | tf_op jit(solution)/shard_map/ppermute | solution.py:462
  54.9 7.2 %collective-permute-start.3 = (bf16[128,256]{1,0:T(8,128)(2,1)S(1)}, bf16[128,256]{1,0:T(8,128)(2,1)S(1)}, u32[]{:S(2)}, u32[]{:S(2)}) collective-permute-start(bf16[128,256]{1,0:T(8,128)(2,1)S(1)} %shard_map.193.refs_0_), channel_id=1, source_target_pairs={{0,1},{1,0},{2,3},{3,2},{4,5},{5,4},{6,7},{7,6},{8,9},{9,8},{10,11... | collective-permute-start | bytes 196616 | tf_op jit(solution)/shard_map/ppermute | solution.py:462
  59.8 4.3 %collective-permute-start.14 = (bf16[128,256]{1,0:T(8,128)(2,1)S(1)}, bf16[128,256]{1,0:T(8,128)(2,1)S(1)}, u32[]{:S(2)}, u32[]{:S(2)}) collective-permute-start(bf16[128,256]{1,0:T(8,128)(2,1)S(1)} %shard_map.198), channel_id=1, source_target_pairs={{0,3},{1,2},{2,1},{3,0},{4,7},{5,6},{6,5},{7,4},{8,11},{9,10},{10,... | collective-permute-start | bytes 196616 | tf_op jit(solution)/shard_map/ppermute | solution.py:468
  61.1 4.6 %collective-permute-start.13 = (bf16[128,256]{1,0:T(8,128)(2,1)S(1)}, bf16[128,256]{1,0:T(8,128)(2,1)S(1)}, u32[]{:S(2)}, u32[]{:S(2)}) collective-permute-start(bf16[128,256]{1,0:T(8,128)(2,1)S(1)} %shard_map.198), channel_id=1, source_target_pairs={{0,2},{2,0},{1,3},{3,1},{4,6},{6,4},{5,7},{7,5},{8,10},{10,8},{9,1... | collective-permute-start | bytes 196616 | tf_op jit(solution)/shard_map/ppermute | solution.py:462
  (16 other events, 165.4 us)
